TPU v7x, 128 devices: a whole 4x4x4 slice. The times are simulated.
128 devices in a mesh: kv: 16 (over z, y), tp: 8 (over x, core).
Axes of the slice: x: 4, y: 4, z: 4, core: 2. Of those that a mesh axis runs over, the one named last changes fastest.
Arguments:
- residual_entries: bfloat16 [1024, 4096], P(None, ('kv', 'tp')), may hold values from -6 to 6
- fresh_extents: int32 [128], replicated, may hold values from 1 to 8, 512 in all
- memory_matrix: float32 [128, 16, 128, 128], P('kv', 'tp'), may hold values from -3 to 3
- initial_rescale_vector: float32 [4096], P('kv'), may hold values from 0.1 to 1.9
- probe_matrix: bfloat16 [4096, 2048], P('kv', 'tp'), may hold values from -0.09375 to 0.09375
- retain_matrix: bfloat16 [4096, 2048], P('kv', 'tp'), may hold values from -0.09375 to 0.09375
- content_matrix: bfloat16 [4096, 2048], P('kv', 'tp'), may hold values from -0.09375 to 0.09375
- result_switch_matrix: bfloat16 [4096, 2048], P('kv', 'tp'), may hold values from -0.09375 to 0.09375
- retain_lower_limit: float32 [2048], P('tp'), may hold values from 0 to 0.9
- extra_shrink_log: float32 [1024, 16], P('kv', 'tp'), may hold values from -0.7 to 0
- lane_result_rescale: float32 [128], replicated, may hold values from 0.1 to 1.9
- result_matrix: bfloat16 [2048, 4096], P('tp', 'kv'), may hold values from -0.125 to 0.125
- later_rescale_vector: float32 [4096], P(('kv', 'tp')), may hold values from 0.1 to 1.9
- mixer_switch_matrix: bfloat16 [4096, 11008], P(None, ('kv', 'tp')), may hold values from -0.09375 to 0.09375
- widening_matrix: bfloat16 [4096, 11008], P(None, ('kv', 'tp')), may hold values from -0.09375 to 0.09375
- narrowing_matrix: bfloat16 [11008, 4096], P(('kv', 'tp')), may hold values from -0.21875 to 0.21875
Outputs:
- mixed: bfloat16 [1024, 4096], P(None, ('kv', 'tp'))
- new_state: float32 [128, 16, 128, 128], P('kv', 'tp')
Inputs may be any that keep to these rules, and one draw needn't show every extreme that they name: `fresh_extents`: the lengths sum to exactly 512.
All inputs are finite; a program needn't handle non-finite values.
Results may differ from a plain program's by a relative error of at most 0.022.
Values may be sent and summed in bfloat16 or wider, within the bound.
A program may use at most 64 MiB of HBM per device.

v0:
```python
import functools

import jax
import jax.numpy as jnp
from jax import lax
from jax.sharding import Mesh
from jax.sharding import PartitionSpec as P

D = 4096
HEAD = 128
FRESH_PLACES = 8
KV = ("kv_0", "kv_1")
TP = ("tp_0", "tp_1")
KV_TP = ("kv_0", "kv_1", "tp_0", "tp_1")


epsilon = 1e-06


def joined_along(pieces, dim):
    pieces = jnp.moveaxis(pieces, 0, dim)
    shape = pieces.shape
    return pieces.reshape(*shape[:dim], shape[dim] * shape[dim + 1], *shape[dim + 2 :])


def copy_for_each(x, axis):
    devices = lax.axis_size(axis)
    return lax.all_to_all(jnp.broadcast_to(x[None], (devices, *x.shape)), axis, 0, 0, tiled=True)


def gather_directly(x, axis, dim):
    return joined_along(copy_for_each(x, axis), dim)


def split_up(x, dim, devices):
    before, after = (x.shape[:dim], x.shape[dim + 1 :])
    return jnp.moveaxis(x.reshape(*before, devices, -1, *after), dim, 0)


def sum_at_owner(x, axis, dim):
    devices = lax.axis_size(axis)
    pieces = lax.all_to_all(split_up(x, dim, devices), axis, 0, 0, tiled=True)
    return jnp.sum(pieces, axis=0)


def own_rows(terms, axes):
    total = terms.astype(jnp.bfloat16)
    for axis in axes:
        total = lax.psum_scatter(total, axis, scatter_dimension=0, tiled=True)
    return total.astype(jnp.float32)


def sent_and_summed(x, axis, dim):
    devices = lax.axis_size(axis)
    pieces = lax.all_to_all(split_up(x, dim, devices), axis, 0, 0, tiled=True)
    return jnp.sum(pieces.astype(jnp.float32), axis=0)


def one_axis_at_a_time(x, axes):
    return functools.reduce(lax.psum, axes, x)


def sum_in_two_steps(x, axes, dim):
    far, near = axes
    pieces = split_up(x, dim, lax.axis_size(far))
    nearer = sent_and_summed(pieces, near, dim + 1)
    arrived = lax.all_to_all(
        nearer.astype(jnp.bfloat16), far, split_axis=0, concat_axis=0, tiled=True
    )
    return arrived.astype(jnp.float32).sum(axis=0)


def local(
    residual_entries,
    fresh_extents,
    memory_matrix,
    initial_rescale_vector,
    probe_matrix,
    retain_matrix,
    content_matrix,
    result_switch_matrix,
    retain_lower_limit,
    extra_shrink_log,
    lane_result_rescale,
    result_matrix,
    later_rescale_vector,
    mixer_switch_matrix,
    widening_matrix,
    narrowing_matrix,
):
    sequences_per_device = memory_matrix.shape[0]
    heads_per_device = memory_matrix.shape[1]
    rows_dev = sequences_per_device * FRESH_PLACES
    all_rows = residual_entries.shape[0]
    kv_index = lax.axis_index(KV)
    tokens_wide = residual_entries.astype(jnp.float32)
    columns = gather_directly(residual_entries, TP, 1)
    col_wide = columns.astype(jnp.float32)
    own_squares = sum_at_owner(jnp.sum(col_wide * col_wide, axis=1), KV, 0)
    first_scale = lax.rsqrt(own_squares / D + epsilon)
    scaled = (columns.astype(jnp.float32) * initial_rescale_vector).astype(jnp.bfloat16)
    projected = (
        own_rows(
            jnp.concatenate(
                [
                    jnp.dot(scaled, weight, preferred_element_type=jnp.float32)
                    for weight in (
                        probe_matrix,
                        retain_matrix,
                        content_matrix,
                        result_switch_matrix,
                    )
                ],
                axis=1,
            ),
            KV,
        )
        * first_scale[:, None]
    )
    width_dev = probe_matrix.shape[1]
    shape_four = (sequences_per_device, FRESH_PLACES, heads_per_device, HEAD)
    z_query = projected[:, :width_dev]
    z_forget = projected[:, width_dev : 2 * width_dev].reshape(shape_four)
    z_input = projected[:, 2 * width_dev : 3 * width_dev].reshape(shape_four)
    z_outgate = projected[:, 3 * width_dev :]
    own_lengths = lax.dynamic_slice_in_dim(
        fresh_extents, kv_index * sequences_per_device, sequences_per_device
    )
    living = jnp.arange(FRESH_PLACES, dtype=jnp.int32)[None, :] < own_lengths[:, None]
    query = jax.nn.silu(z_query).reshape(shape_four)
    bounds = retain_lower_limit.reshape(heads_per_device, HEAD)
    retain_factor = bounds + (1.0 - bounds) * jax.nn.sigmoid(z_forget)
    shrink_exponent = jnp.log(retain_factor) + extra_shrink_log.reshape(
        sequences_per_device, FRESH_PLACES, heads_per_device, 1
    )
    decays = jnp.where(living[:, :, None, None], jnp.exp(shrink_exponent), 1.0)
    key_gate = jnp.where(living[:, :, None, None], 1.0 - retain_factor, 0.0)
    carried = memory_matrix
    outputs = []
    for position in range(FRESH_PLACES):
        carried = (
            decays[:, position, :, :, None] * carried
            + key_gate[:, position, :, :, None] * z_input[:, position, :, None, :]
        )
        outputs.append(
            jnp.einsum(
                "bhd,bhdv->bhv", query[:, position], carried, precision=lax.Precision.HIGHEST
            )
        )
    heads_out = jnp.stack(outputs, axis=1)
    heads_out = (
        heads_out
        * lax.rsqrt(jnp.mean(heads_out * heads_out, axis=-1, keepdims=True) + epsilon)
        * lane_result_rescale
    )
    normed = jnp.where(
        living.reshape(rows_dev)[:, None],
        heads_out.reshape(rows_dev, width_dev) * jax.nn.silu(z_outgate),
        0.0,
    ).astype(jnp.bfloat16)
    head_partial = jnp.dot(
        gather_directly(normed, KV, 0), result_matrix, preferred_element_type=jnp.float32
    ).astype(jnp.bfloat16)
    attended = sent_and_summed(head_partial, TP, 1)
    residual = (tokens_wide + attended).astype(jnp.bfloat16)
    resid_wide = residual.astype(jnp.float32)
    resid_squares = one_axis_at_a_time(jnp.sum(resid_wide * resid_wide, axis=1), KV_TP)
    second_in = (
        resid_wide * later_rescale_vector * lax.rsqrt(resid_squares / D + epsilon)[:, None]
    ).astype(jnp.bfloat16)
    live_rows = (
        jnp.arange(FRESH_PLACES, dtype=jnp.int32)[None, :] < fresh_extents[:, None]
    ).reshape(all_rows)
    piece = lax.all_gather(second_in, KV_TP, axis=1, tiled=True)
    gated = jnp.dot(piece, mixer_switch_matrix, preferred_element_type=jnp.float32)
    upward = jnp.dot(piece, widening_matrix, preferred_element_type=jnp.float32)
    hidden = (jax.nn.silu(gated) * upward).astype(jnp.bfloat16)
    mixer_terms = sum_in_two_steps(
        jnp.dot(hidden, narrowing_matrix, preferred_element_type=jnp.float32).astype(jnp.bfloat16),
        (("kv_0", "kv_1", "tp_0"), "tp_1"),
        1,
    )
    mixed = jnp.where(live_rows[:, None], resid_wide + mixer_terms, 0.0).astype(jnp.bfloat16)
    return (mixed, carried)


def solution(mesh):
    torus = Mesh(mesh.devices.reshape(4, 4, 4, 2), ("kv_0", "kv_1", "tp_0", "tp_1"))
    placed = (
        P(None, KV_TP),
        P(),
        P(KV, TP, None, None),
        P(KV),
        P(KV, TP),
        P(KV, TP),
        P(KV, TP),
        P(KV, TP),
        P(TP),
        P(KV, TP),
        P(),
        P(TP, KV),
        P(KV_TP),
        P(None, KV_TP),
        P(None, KV_TP),
        P(KV_TP, None),
    )
    return jax.shard_map(
        local,
        mesh=torus,
        in_specs=placed,
        out_specs=(P(None, KV_TP), P(KV, TP, None, None)),
        check_vma=False,
    )
```

profile of v0, /device:TPU:1, one launch (start us, length us, event | category | flops | bytes accessed | tf_op | source)
XLA Modules:
  0.0 364.8 jit_solution(14487172462540239422)
XLA Ops:
  7.2 1.0 broadcast_in_dim.67
  8.2 14.9 %all_to_all.34 = bf16[8,1024,32]{1,2,0:T(8,128)(2,1)S(1)} all-to-all(bf16[8,1024,32]{1,2,0:T(8,128)(2,1)S(1)} %broadcast_in_dim.67), channel_id=1, replica_groups=mesh['kv_0'=4,'kv_1'=4,'tp_0'=4,'tp_1'=2] {'tp_0','tp_1'}, dimensions={0} | all-to-all | bytes 1048576 | tf_op jit(solution)/shard_map/all_to_all | solution.py:28
  23.1 0.8 fusion.1
  24.0 1.2 convolution_convert_fusion.2
  25.2 1.2 convolution_convert_fusion.3
  26.5 0.3 convolution_convert_fusion.4
  26.8 0.3 convolution_convert_fusion.5
  27.2 1.5 pad_maximum_fusion
  28.8 30.9 %reduce-scatter.5.cloned.1.call-done = bf16[256,1024]{0,1:T(8,128)(2,1)} async-done(((bf16[1024,1024]{0,1:T(8,128)(2,1)}), bf16[256,1024]{0,1:T(8,128)(2,1)}) %reduce-scatter.5.cloned.1.call-update) | async-done | bytes 524304 | tf_op jit(solution)/shard_map/reduce_scatter | solution.py:49
  59.7 2.0 copy.335
  61.9 0.1 multiply_reduce_fusion
  62.0 0.7 all_to_all.22
  62.7 5.0 %all-to-all-start.1 = ((f32[16,1,64]{2,1,0:T(1,128)}), f32[16,1,64]{2,1,0:T(1,128)S(1)}, u32[]{:S(2)}, u32[]{:S(2)}) async-start(f32[16,1,64]{2,1,0:T(1,128)} %all_to_all.22), calls=%async_computation.2 | async-start | bytes 16384 | tf_op jit(solution)/shard_map/all_to_all | solution.py:42
  68.0 6.1 %all-to-all-done.1 = f32[16,1,64]{2,1,0:T(1,128)S(1)} async-done(((f32[16,1,64]{2,1,0:T(1,128)}), f32[16,1,64]{2,1,0:T(1,128)S(1)}, u32[]{:S(2)}, u32[]{:S(2)}) %all-to-all-start.1) | async-done | bytes 4128 | tf_op jit(solution)/shard_map/all_to_all | solution.py:42
  74.1 7.5 %reduce-scatter.7.cloned.1.call-done = bf16[64,1024]{1,0:T(8,128)(2,1)} async-done(((bf16[256,1024]{1,0:T(8,128)(2,1)}), bf16[64,1024]{1,0:T(8,128)(2,1)}) %reduce-scatter.7.cloned.1.call-update) | async-done | bytes 131088 | tf_op jit(solution)/shard_map/reduce_scatter | solution.py:49
  81.6 1.0 convert_multiply_fusion
  82.8 0.1 exponential_select_fusion
  82.9 0.1 fusion.52
  83.0 4.7 %multiply_add_fusion = (f32[8,2,128,128]{3,2,1,0:T(8,128)S(1)}, f32[8,2,128,128]{3,2,1,0:T(8,128)S(1)}) fusion(f32[8,2,128]{2,1,0:T(2,128)S(1)} %bitcast.181, f32[8,2,128]{2,1,0:T(2,128)S(1)} %bitcast.205, f32[8,2,128]{2,1,0:T(2,128)S(1)} %bitcast.204, f32[8,2,128]{2,1,0:T(2,128)S(1)} %bitcast.179, f32[8,2,128]{2,1,0:T(2,128)S(1)} %bitcast.201, ...), kind=kLoop, calls=%fused_computation.13 | loop fusion | flops 6291456 | bytes 3342336 | tf_op jit(solution)/shard_map/add | solution.py:142
  87.7 3.1 fusion.5
  90.8 2.1 fusion.24
  92.9 1.4 fusion.4
  94.3 1.0 fusion.45
  95.3 3.0 fusion.3
  98.4 2.1 fusion.23
  100.5 1.4 fusion.2
  101.9 1.0 fusion.40
  103.0 0.1 multiply_reduce_fusion.1
  103.3 13.9 %all_to_all.35 = bf16[16,64,256]{2,1,0:T(8,128)(2,1)S(1)} all-to-all(bf16[16,64,256]{2,1,0:T(8,128)(2,1)S(1)} %broadcast_in_dim.71), channel_id=1, replica_groups=mesh['kv_0'=4,'kv_1'=4,'tp_0'=4,'tp_1'=2] {'kv_0','kv_1'}, dimensions={0} | all-to-all | bytes 1048576 | tf_op jit(solution)/shard_map/all_to_all | solution.py:28
  117.2 0.3 convolution_convert_fusion.1
  117.6 17.8 %all_to_all.36 = bf16[8,1024,32]{1,2,0:T(8,128)(2,1)S(1)} all-to-all(bf16[8,1024,32]{1,2,0:T(8,128)(2,1)S(1)} %bitcast.146), channel_id=1, replica_groups=mesh['kv_0'=4,'kv_1'=4,'tp_0'=4,'tp_1'=2] {'tp_0','tp_1'}, dimensions={0} | all-to-all | bytes 1048576 | tf_op jit(solution)/shard_map/all_to_all | solution.py:55
  135.6 6.8 %psum.28 = f32[1024]{0:T(1024)S(1)} all-reduce(f32[1024]{0:T(1024)S(1)} %get-tuple-element.2), channel_id=1, replica_groups=mesh['kv_0'=4,'kv_1'=4,'tp_0'=4,'tp_1'=2] {'kv_0'}, use_global_device_ids=true, to_apply=%region_7.8 | all-reduce | flops 1024 | bytes 8192 | tf_op jit(solution)/shard_map/psum | solution.py:60
  142.4 6.5 %psum.29 = f32[1024]{0:T(1024)S(1)} all-reduce(f32[1024]{0:T(1024)S(1)} %psum.28), channel_id=1, replica_groups=mesh['kv_0'=4,'kv_1'=4,'tp_0'=4,'tp_1'=2] {'kv_1'}, use_global_device_ids=true, to_apply=%region_8.9 | all-reduce | flops 1024 | bytes 8192 | tf_op jit(solution)/shard_map/psum | solution.py:60
  148.9 6.9 %psum.30 = f32[1024]{0:T(1024)S(1)} all-reduce(f32[1024]{0:T(1024)S(1)} %psum.29), channel_id=1, replica_groups=mesh['kv_0'=4,'kv_1'=4,'tp_0'=4,'tp_1'=2] {'tp_0'}, use_global_device_ids=true, to_apply=%region_9.10 | all-reduce | flops 1024 | bytes 8192 | tf_op jit(solution)/shard_map/psum | solution.py:60
  155.8 9.2 %psum.31 = f32[1024]{0:T(1024)S(1)} all-reduce(f32[1024]{0:T(1024)S(1)} %psum.30), channel_id=1, replica_groups=mesh['kv_0'=4,'kv_1'=4,'tp_0'=4,'tp_1'=2] {'tp_1'}, use_global_device_ids=true, to_apply=%region_10.11 | all-reduce | flops 1024 | bytes 8192 | tf_op jit(solution)/shard_map/psum | solution.py:60
  165.0 0.7 fusion.27
  165.8 65.2 %all-gather.2.cloned.1.call-done = bf16[1024,4096]{0,1:T(8,128)(2,1)} async-done(((bf16[1024,32]{0,1:T(8,128)(2,1)}), bf16[1024,4096]{0,1:T(8,128)(2,1)}) %all-gather.2.cloned.1.call-update) | async-done | bytes 8388624 | tf_op jit(solution)/shard_map/all_gather | solution.py:174
  231.0 5.0 %fusion.55 = f32[1024,86]{0,1:T(8,128)S(1)} fusion(bf16[1024,4096]{0,1:T(8,128)(2,1)} %all-gather.2.cloned.1.call-done, bf16[4096,86]{0,1:T(8,128)(2,1)} %param.29), kind=kOutput, calls=%fused_computation.111 | convolution fusion | flops 721420288 | bytes 9445376 | tf_op jit(solution)/shard_map/dot_general | solution.py:175
  236.0 10.9 %convolution_convert_fusion = bf16[1024,4096]{1,0:T(8,128)(2,1)} fusion(bf16[86,4096]{1,0:T(8,128)(2,1)S(1)} %copy-done, bf16[1024,4096]{0,1:T(8,128)(2,1)} %all-gather.2.cloned.1.call-done, bf16[4096,86]{0,1:T(8,128)(2,1)S(1)} %copy-done.4, f32[1024,86]{0,1:T(8,128)S(1)} %fusion.55), kind=kOutput, calls=%fused_computation.1 | convolution fusion | flops 1447563264 | bytes 18538496 | tf_op jit(solution)/shard_map/dot_general | solution.py:179
  246.9 11.9 %copy.292 = bf16[1024,4096]{0,1:T(8,128)(2,1)} copy(bf16[1024,4096]{1,0:T(8,128)(2,1)} %convolution_convert_fusion) | data formatting | bytes 16777216 | tf_op jit(solution)/shard_map/convert_element_type | solution.py:179
  258.8 8.5 %copy.293 = bf16[2,64,1024,32]{2,3,1,0:T(8,128)(2,1)} copy(bf16[2,64,1024,32]{2,3,0,1:T(8,128)(2,1)} %bitcast.144) | data formatting | bytes 16777216 | tf_op jit(solution)/shard_map/transpose | solution.py:37
  267.3 18.4 %all_to_all.37 = bf16[2,64,1024,32]{2,3,1,0:T(8,128)(2,1)} all-to-all(bf16[2,64,1024,32]{2,3,1,0:T(8,128)(2,1)} %copy.293), channel_id=1, replica_groups=mesh['kv_0'=4,'kv_1'=4,'tp_0'=4,'tp_1'=2] {'tp_1'}, dimensions={0} | all-to-all | bytes 16777216 | tf_op jit(solution)/shard_map/all_to_all | solution.py:55
  285.7 9.1 %reduce_sum.71 = bf16[64,1024,32]{1,2,0:T(8,128)(2,1)} reduce(bf16[2,64,1024,32]{2,3,1,0:T(8,128)(2,1)} %all_to_all.37, bf16[]{:T(256)} %constant.41.clone.1), dimensions={0}, to_apply=%region_11.12 | reduce | flops 2097152 | bytes 12582914 | tf_op jit(solution)/shard_map/reduce_sum | solution.py:56
  294.8 6.5 %all-to-all-start.5 = ((bf16[64,1024,32]{1,2,0:T(8,128)(2,1)}), bf16[64,1024,32]{1,2,0:T(8,128)(2,1)}, u32[]{:S(2)}, u32[]{:S(2)}) async-start(bf16[64,1024,32]{1,2,0:T(8,128)(2,1)} %reduce_sum.71), calls=%async_computation.6 | async-start | bytes 8388608 | tf_op jit(solution)/shard_map/all_to_all | solution.py:67
  301.4 0.1 lt.50
  301.5 53.2 %all-to-all-done.5 = bf16[64,1024,32]{1,2,0:T(8,128)(2,1)} async-done(((bf16[64,1024,32]{1,2,0:T(8,128)(2,1)}), bf16[64,1024,32]{1,2,0:T(8,128)(2,1)}, u32[]{:S(2)}, u32[]{:S(2)}) %all-to-all-start.5) | async-done | bytes 4194336 | tf_op jit(solution)/shard_map/all_to_all | solution.py:67
  354.6 3.0 convert_reduce_fusion
  357.7 0.6 fusion.30
  (69 shorter events, 1.2 us)
Async XLA Ops:
  7.2 228.8 %copy-start = (bf16[86,4096]{1,0:T(8,128)(2,1)S(1)}, bf16[86,4096]{1,0:T(8,128)(2,1)}, u32[]{:S(2)}) copy-start(bf16[86,4096]{1,0:T(8,128)(2,1)} %param.31) | copy-start | bytes 2113540
  7.2 19.3 %copy-start.6 = (bf16[256,256]{1,0:T(8,128)(2,1)S(1)}, bf16[256,256]{1,0:T(8,128)(2,1)}, u32[]{:S(2)}) copy-start(bf16[256,256]{1,0:T(8,128)(2,1)} %param.21) | copy-start | bytes 393220
  7.2 19.6 %copy-start.7 = (bf16[256,256]{1,0:T(8,128)(2,1)S(1)}, bf16[256,256]{1,0:T(8,128)(2,1)}, u32[]{:S(2)}) copy-start(bf16[256,256]{1,0:T(8,128)(2,1)} %param.20) | copy-start | bytes 393220
  7.2 52.5 %reduce-scatter.5.cloned.1.call-start = ((), (), s32[]{:S(2)}) async-start(), calls=%async_computation.8 | async-start | bytes 2621440 | tf_op jit(solution)/shard_map/reduce_scatter | solution.py:49
  27.2 34.6 %copy-start.12 = (s32[128]{0:T(128)S(1)}, s32[128]{0:T(128)}, u32[]{:S(2)}) copy-start(s32[128]{0:T(128)} %param.17) | copy-start | bytes 1540
  27.2 34.7 %copy-start.9 = (f32[256]{0:T(256)S(1)}, f32[256]{0:T(256)}, u32[]{:S(2)}) copy-start(f32[256]{0:T(256)} %param.24) | copy-start | bytes 3076
  27.2 40.6 %copy-start.13 = (f32[128]{0:T(128)S(1)}, f32[128]{0:T(128)}, u32[]{:S(2)}) copy-start(f32[128]{0:T(128)} %param.26) | copy-start | bytes 1540
  27.2 40.6 %copy-start.10 = (f32[64,2]{0,1:T(2,128)S(1)}, f32[64,2]{0,1:T(2,128)}, u32[]{:S(2)}) copy-start(f32[64,2]{0,1:T(2,128)} %param.25) | copy-start | bytes 1540
  27.2 55.8 %copy-start.2 = (f32[8,2,128,128]{3,2,1,0:T(8,128)S(1)}, f32[8,2,128,128]{3,2,1,0:T(8,128)}, u32[]{:S(2)}) copy-start(f32[8,2,128,128]{3,2,1,0:T(8,128)} %param.18) | copy-start | bytes 3145732
  28.8 52.8 %reduce-scatter.7.cloned.1.call-start = ((), (), s32[]{:S(2)}) async-start(), calls=%async_computation.10 | async-start | bytes 655360 | tf_op jit(solution)/shard_map/reduce_scatter | solution.py:49
  62.7 11.4 %all-to-all-start.1 = ((f32[16,1,64]{2,1,0:T(1,128)}), f32[16,1,64]{2,1,0:T(1,128)S(1)}, u32[]{:S(2)}, u32[]{:S(2)}) async-start(f32[16,1,64]{2,1,0:T(1,128)} %all_to_all.22), calls=%async_computation.2 | async-start | bytes 16384 | tf_op jit(solution)/shard_map/all_to_all | solution.py:42
  67.7 163.2 %all-gather.2.cloned.1.call-start = ((), (), s32[]{:S(2)}) async-start(), calls=%async_computation.9 | async-start | bytes 8454144 | tf_op jit(solution)/shard_map/all_gather | solution.py:174
  87.7 14.2 %copy-start.3 = (f32[8,2,128,128]{3,2,1,0:T(8,128)}, f32[8,2,128,128]{3,2,1,0:T(8,128)S(1)}, u32[]{:S(2)}) copy-start(f32[8,2,128,128]{3,2,1,0:T(8,128)S(1)} %get-tuple-element.4) | copy-start | bytes 3145732
  95.3 21.9 %copy-start.8 = (bf16[256,256]{1,0:T(8,128)(2,1)S(1)}, bf16[256,256]{1,0:T(8,128)(2,1)}, u32[]{:S(2)}) copy-start(bf16[256,256]{1,0:T(8,128)(2,1)} %param.27) | copy-start | bytes 393220
  98.3 37.2 %copy-start.5 = (bf16[1024,32]{0,1:T(8,128)(2,1)S(1)}, bf16[1024,32]{0,1:T(8,128)(2,1)}, u32[]{:S(2)}) copy-start(bf16[1024,32]{0,1:T(8,128)(2,1)} %param.16) | copy-start | bytes 196612
  100.5 64.5 %copy-start.11 = (f32[32]{0:T(128)S(1)}, f32[32]{0:T(128)}, u32[]{:S(2)}) copy-start(f32[32]{0:T(128)} %param.28) | copy-start | bytes 388
  165.8 70.2 %copy-start.4 = (bf16[4096,86]{0,1:T(8,128)(2,1)S(1)}, bf16[4096,86]{0,1:T(8,128)(2,1)}, u32[]{:S(2)}) copy-start(bf16[4096,86]{0,1:T(8,128)(2,1)} %param.30) | copy-start | bytes 2113540
  294.8 59.9 %all-to-all-start.5 = ((bf16[64,1024,32]{1,2,0:T(8,128)(2,1)}), bf16[64,1024,32]{1,2,0:T(8,128)(2,1)}, u32[]{:S(2)}, u32[]{:S(2)}) async-start(bf16[64,1024,32]{1,2,0:T(8,128)(2,1)} %reduce_sum.71), calls=%async_computation.6 | async-start | bytes 8388608 | tf_op jit(solution)/shard_map/all_to_all | solution.py:67
  301.3 57.0 %copy-start.1 = (bf16[86,4096]{1,0:T(8,128)(2,1)S(1)}, bf16[86,4096]{1,0:T(8,128)(2,1)}, u32[]{:S(2)}) copy-start(bf16[86,4096]{1,0:T(8,128)(2,1)} %param.31) | copy-start | bytes 2113540
Sparse Core Ops, SparseCore 0:
  28.9 30.7 reduce-scatter.4
  62.6 18.9 reduce-scatter.6
  165.9 65.0 all-gather.1
where the time goes:
time: 367 us; the launch traced here: 365 us
  waiting for transfers between devices  163 us (44%)
  blocking collectives  94.5 us (26%)
  matrix products  34.5 us (9%)
  local copies, waits for them, and re-layouts  24.8 us (7%)
  other arithmetic  22.3 us (6%)
  between operations  14.2 us (4%)
  starting transfers between devices  11.6 us (3%)
    all_gather x1, waiting for transfers between devices, local(): piece = lax.all_gather(second_in, KV_TP, axis=1, tiled=True)  65.2 us
    all_to_all x1, waiting for transfers between devices, sum_in_two_steps(): lax.all_to_all(nearer.astype(jnp.bfloat16), far, split_axis=0, concat_axi...  53.2 us
    reduce_scatter x2, waiting for transfers between devices, own_rows(): total = lax.psum_scatter(total, axis, scatter_dimension=0, tiled=True)  38.3 us
    all_to_all x2, blocking collectives, sent_and_summed(): pieces = lax.all_to_all(split_up(x, dim, devices), axis, 0, 0, tiled=True)  36.3 us
    psum x4, blocking collectives, one_axis_at_a_time(): return functools.reduce(lax.psum, axes, x)  29.4 us
    all_to_all x2, blocking collectives, copy_for_each(): lax.all_to_all(jnp.broadcast_to(x[None], (devices, *x.shape)), axis, 0, 0...  28.8 us
    dot_general x8, matrix products, local(): jnp.einsum('bhd,bhdv->bhv', query[:, position], carried, precision=lax.Pr...  15.1 us
    convert_element_type x1, local copies, waits for them, and re-layouts, local(): jnp.dot(hidden, narrowing_matrix, preferred_element_type=jnp.float32)  11.9 us
  transfers between devices with their start and end apart: 5, of which 5 were waited for; matrix products, arithmetic and copies ran while one was open for 0% of the time, Pallas kernels for 0%

commit v1 on v0

--- a/solution.py
+++ b/solution.py
@@ -3,6 +3,8 @@
 import jax
 import jax.numpy as jnp
 from jax import lax
+from jax.experimental import pallas as pl
+from jax.experimental.pallas import tpu as pltpu
 from jax.sharding import Mesh
 from jax.sharding import PartitionSpec as P
 
@@ -68,6 +70,430 @@
         nearer.astype(jnp.bfloat16), far, split_axis=0, concat_axis=0, tiled=True
     )
     return arrived.astype(jnp.float32).sum(axis=0)
+
+
+MESH = pl.DeviceIdType.MESH
+EPS = 1e-06
+F32 = jnp.float32
+BF = jnp.bfloat16
+PARTS = ((0, 3, "xyz"), (3, 3, "yzx"), (6, 2, "zxy"))
+
+
+def my_position():
+    return dict(
+        z=lax.axis_index("kv_0"),
+        y=lax.axis_index("kv_1"),
+        x=lax.axis_index("tp_0"),
+        c=lax.axis_index("tp_1"),
+    )
+
+
+def device_at(at, **moved):
+    there = dict(at, **moved)
+    return (there["z"], there["y"], there["x"], there["c"])
+
+
+def plane_offsets():
+    return [(dz, dy) for dz in range(4) for dy in range(4) if dz or dy]
+
+
+def line_offsets():
+    return [(dx, dc) for dx in range(4) for dc in range(2) if dx or dc]
+
+
+def plane_peer(at, dz, dy):
+    return device_at(at, z=(at["z"] + dz) % 4, y=(at["y"] + dy) % 4)
+
+
+def line_peer(at, dx, dc):
+    return device_at(at, x=(at["x"] + dx) % 4, c=(at["c"] + dc) % 2)
+
+
+def meet(peers):
+    barrier = pltpu.get_barrier_semaphore()
+    for peer in peers:
+        pl.semaphore_signal(barrier, inc=1, device_id=peer, device_id_type=MESH)
+    pl.semaphore_wait(barrier, len(peers))
+
+
+def send(src, dst, sems, i, peer):
+    copy = pltpu.make_async_remote_copy(
+        src_ref=src,
+        dst_ref=dst,
+        send_sem=sems[0].at[i],
+        recv_sem=sems[1].at[i],
+        device_id=peer,
+        device_id_type=MESH,
+    )
+    copy.start()
+    return copy
+
+
+def row_of(column, rows):
+    eye = lax.broadcasted_iota(jnp.int32, (rows, 128), 0) == lax.broadcasted_iota(
+        jnp.int32, (rows, 128), 1
+    )
+    return jnp.sum(jnp.where(eye, column, 0.0), axis=0, keepdims=True)
+
+
+def column_of(row, rows):
+    eye = lax.broadcasted_iota(jnp.int32, (rows, 128), 0) == lax.broadcasted_iota(
+        jnp.int32, (rows, 128), 1
+    )
+    return jnp.sum(jnp.where(eye, row, 0.0), axis=1, keepdims=True)
+
+
+def halves(length):
+    return pl.ds(0, length // 2), pl.ds(length // 2, length - length // 2)
+
+
+def gather_phase(at, bufs, phase, sems, base):
+    first = []
+    for p, (_, _, order) in enumerate(PARTS):
+        axis = order[phase]
+        pre = tuple(at[a] for a in order[:phase:-1])
+        m = at[axis]
+        up, down = (m + 1) % 4, (m + 3) % 4
+        own = bufs[p].at[(*pre, m)]
+        i = base + 4 * p
+        first.append((
+            send(own, own, sems, i, device_at(at, **{axis: up})),
+            send(own, own, sems, i + 1, device_at(at, **{axis: down})),
+        ))
+    second = []
+    for p, (_, _, order) in enumerate(PARTS):
+        axis = order[phase]
+        pre = tuple(at[a] for a in order[:phase:-1])
+        m = at[axis]
+        up, down = (m + 1) % 4, (m + 3) % 4
+        lo, hi = halves(bufs[p].shape[len(pre) + 1])
+        i = base + 4 * p
+        first[p][0].wait_recv()
+        from_down = bufs[p].at[(*pre, down, lo)]
+        a = send(from_down, from_down, sems, i + 2, device_at(at, **{axis: up}))
+        first[p][1].wait_recv()
+        from_up = bufs[p].at[(*pre, up, hi)]
+        b = send(from_up, from_up, sems, i + 3, device_at(at, **{axis: down}))
+        second.append((a, b))
+    for p in range(3):
+        for copy in first[p]:
+            copy.wait_send()
+        for copy in second[p]:
+            copy.wait()
+
+
+def add_into(ref, idx, terms):
+    total = ref[idx].astype(F32)
+    for term in terms:
+        total = total + term.astype(F32)
+    ref[idx] = total.astype(BF)
+
+
+def reduce_phase(at, bufs, phase, one_up, one_down, two_up, two_down, sems, base):
+    early = []
+    for p, (_, _, order) in enumerate(PARTS):
+        axis = order[phase]
+        pre = tuple(at[a] for a in order[:phase:-1])
+        m = at[axis]
+        up, down, far = (m + 1) % 4, (m + 3) % 4, (m + 2) % 4
+        to_up, to_down = device_at(at, **{axis: up}), device_at(at, **{axis: down})
+        lo, hi = halves(bufs[p].shape[len(pre) + 1])
+        i = base + 6 * p
+        early.append((
+            send(bufs[p].at[(*pre, far, lo)], one_up[p], sems, i, to_up),
+            send(bufs[p].at[(*pre, far, hi)], one_down[p], sems, i + 1, to_down),
+            send(bufs[p].at[(*pre, up, hi)], two_up[p].at[hi], sems, i + 2, to_up),
+            send(bufs[p].at[(*pre, down, lo)], two_down[p].at[lo], sems, i + 3, to_down),
+        ))
+    late = []
+    for p, (_, _, order) in enumerate(PARTS):
+        axis = order[phase]
+        pre = tuple(at[a] for a in order[:phase:-1])
+        m = at[axis]
+        up, down = (m + 1) % 4, (m + 3) % 4
+        to_up, to_down = device_at(at, **{axis: up}), device_at(at, **{axis: down})
+        lo, hi = halves(bufs[p].shape[len(pre) + 1])
+        i = base + 6 * p
+        early[p][0].wait_recv()
+        add_into(bufs[p], (*pre, up, lo), [one_up[p][...]])
+        a = send(bufs[p].at[(*pre, up, lo)], two_up[p].at[lo], sems, i + 4, to_up)
+        early[p][1].wait_recv()
+        add_into(bufs[p], (*pre, down, hi), [one_down[p][...]])
+        b = send(bufs[p].at[(*pre, down, hi)], two_down[p].at[hi], sems, i + 5, to_down)
+        late.append((a, b))
+    for p, (_, _, order) in enumerate(PARTS):
+        axis = order[phase]
+        pre = tuple(at[a] for a in order[:phase:-1])
+        for copy in early[p][2:]:
+            copy.wait_recv()
+        for copy in late[p]:
+            copy.wait_recv()
+        for copy in (*early[p], *late[p]):
+            copy.wait_send()
+        add_into(bufs[p], (*pre, at[axis]), [two_up[p][...], two_down[p][...]])
+
+
+def mixer_kernel(
+    normed_ref, packed_ref, x_ref, result_ref, gain_ref, gate_ref, wide_ref, narrow_ref,
+    out_ref,
+    heads, partial, arrived, gains, residual_ref, squares, squares_sum, squares_line,
+    weights, narrow, total, ga, gb, gc,
+    *rest,
+):
+    (pa, pb, pc), rest = rest[:3], rest[3:]
+    receive, rest = rest[:36], rest[36:]
+    ypack, yarrive, sends, recvs = rest
+    sems = (sends, recvs)
+    at = my_position()
+    kv = 4 * at["z"] + at["y"]
+    tp = 2 * at["x"] + at["c"]
+    planes, lines = plane_offsets(), line_offsets()
+    meet([plane_peer(at, *d) for d in planes] + [line_peer(at, *d) for d in lines])
+
+    copies = [
+        send(normed_ref, heads.at[kv], sems, i, plane_peer(at, *d)) for i, d in enumerate(planes)
+    ]
+    gain_copies = [
+        send(gain_ref, gains.at[tp], sems, 15 + i, line_peer(at, *d)) for i, d in enumerate(lines)
+    ]
+    partner = line_peer(at, 0, 1)
+    zeros = jnp.zeros((256, 128 - 86), BF)
+
+    def widen(k, carry):
+        rows = pl.ds(pl.multiple_of(k * 256, 256), 256)
+        weights[0, k] = jnp.concatenate(
+            [gate_ref[rows, :], zeros, wide_ref[rows, :], zeros], axis=1
+        )
+        cols = rows
+        narrow[0, :, cols] = jnp.concatenate(
+            [narrow_ref[:, cols], jnp.zeros((128 - 86, 256), BF)], axis=0
+        )
+        return carry
+
+    lax.fori_loop(0, 16, widen, 0)
+    weight_copy = send(weights.at[0], weights.at[1], sems, 22, partner)
+    narrow_copy = send(narrow.at[0], narrow.at[1], sems, 23, partner)
+    heads[pl.ds(kv, 1)] = normed_ref[...][None]
+    gains[pl.ds(tp, 1)] = gain_ref[...][None]
+
+    place = packed_ref[0:1, :]
+
+    def chosen(start, rows):
+        want = lax.broadcasted_iota(jnp.int32, (rows, 1024), 0) + start
+        return jnp.where(want == place, 1.0, 0.0).astype(BF)
+
+    own_rows = jnp.dot(chosen(64 * tp, 64), x_ref[...], preferred_element_type=F32)
+
+    for copy in copies:
+        copy.wait()
+    all_heads = heads[...].reshape(1024, 256)
+    for part in range(2):
+        live = jnp.dot(chosen(256 * part, 256), all_heads, preferred_element_type=F32).astype(BF)
+        partial[4 * part : 4 * part + 4] = (
+            jnp.dot(live, result_ref[...], preferred_element_type=F32)
+            .astype(BF)
+            .reshape(4, 64, 256)
+        )
+    copies = []
+    for i, (dx, dc) in enumerate(lines):
+        peer = line_peer(at, dx, dc)
+        copies.append(
+            send(partial.at[2 * peer[2] + peer[3]], arrived.at[i], sems, 24 + i, peer)
+        )
+    for copy in gain_copies:
+        copy.wait()
+    gain = jnp.concatenate([gains[t, 0:1, 0:32] for t in range(8)], axis=1)
+    attended = partial[tp].astype(F32)
+    for i, copy in enumerate(copies):
+        copy.wait()
+        attended = attended + arrived[i].astype(F32)
+    residual = (own_rows + attended).astype(BF).astype(F32)
+    residual_ref[...] = residual
+    own_squares = jnp.sum(residual * residual, axis=1, keepdims=True)
+    squares[0] = jnp.broadcast_to(row_of(own_squares, 64), (8, 128))
+    square_copies = [
+        send(squares.at[0], squares.at[1 + i], sems, 31 + i, plane_peer(at, *d))
+        for i, d in enumerate(planes)
+    ]
+    tile = (residual * gain).astype(BF)
+    blocks = [tile[16 * i : 16 * i + 16, 128 * h : 128 * h + 128] for h in range(2) for i in range(4)]
+    bufs = (ga, gb, gc)
+    for p, (start, count, order) in enumerate(PARTS):
+        idx = tuple(at[a] for a in order[::-1])
+        for b in range(count):
+            bufs[p][(*idx, b)] = blocks[start + b]
+    gather_phase(at, bufs, 0, sems, 46)
+    gather_phase(at, bufs, 1, sems, 58)
+    for copy in square_copies:
+        copy.wait()
+    own_sum = jnp.sum(squares[...], axis=0)
+    squares_sum[...] = own_sum
+    squares_line[pl.ds(at["x"], 1)] = own_sum[None]
+    line_copies = [
+        send(squares_sum, squares_line.at[at["x"]], sems, 82 + dx - 1, line_peer(at, dx, 0))
+        for dx in (1, 2, 3)
+    ]
+    gather_phase(at, bufs, 2, sems, 70)
+    for copy in line_copies:
+        copy.wait()
+    weight_copy.wait()
+    narrow_copy.wait()
+
+    def rows_at(zz, yy):
+        a, b, c = ga[zz, yy], gb[:, zz, yy], gc[yy, :, zz]
+        v = jnp.concatenate([a, b, c], axis=1)
+        return jnp.concatenate(
+            [v[:, 0:4].reshape(256, 128), v[:, 4:8].reshape(256, 128)], axis=1
+        )
+
+    def widening(k, carry):
+        lhs = rows_at(k // 4, k % 4)
+        for core in range(2):
+            term = jnp.dot(lhs, weights[core, k], preferred_element_type=F32)
+
+            @pl.when(k == 0)
+            def _():
+                total[core] = term
+
+            @pl.when(k > 0)
+            def _():
+                total[core] += term
+
+        return carry
+
+    lax.fori_loop(0, 16, widening, 0)
+    scale = lax.rsqrt(
+        jnp.concatenate([column_of(squares_line[g, 0:1, :], 64) for g in range(4)], axis=0)
+        / 4096
+        + EPS
+    )
+    hidden = []
+    for core in range(2):
+        gated = total[core, :, 0:128] * scale
+        upward = total[core, :, 128:256] * scale
+        hidden.append((gated * jax.nn.sigmoid(gated) * upward).astype(BF))
+    hidden = jnp.concatenate(hidden, axis=1)
+    pbufs = (pa, pb, pc)
+
+    def narrowing(k, carry):
+        cols = pl.ds(pl.multiple_of(k * 256, 256), 256)
+        rhs = jnp.concatenate([narrow[0, :, cols], narrow[1, :, cols]], axis=0)
+        term = jnp.dot(hidden, rhs, preferred_element_type=F32).astype(BF)
+        v = jnp.concatenate(
+            [term[:, 0:128].reshape(4, 4, 16, 128), term[:, 128:256].reshape(4, 4, 16, 128)], axis=1
+        )
+        zz, yy = k // 4, k % 4
+        pa[zz, yy] = v[:, 0:3]
+        pb[:, zz, yy] = v[:, 3:6]
+        pc[yy, :, zz] = v[:, 6:8]
+        return carry
+
+    lax.fori_loop(0, 16, narrowing, 0)
+    for n, phase in enumerate((2, 1, 0)):
+        r = receive[12 * n : 12 * n + 12]
+        reduce_phase(at, pbufs, phase, r[0:3], r[3:6], r[6:9], r[9:12], sems, 85 + 18 * n)
+    sums = []
+    for p, (start, count, order) in enumerate(PARTS):
+        idx = tuple(at[a] for a in order[::-1])
+        for b in range(count):
+            sums.append(pbufs[p][(*idx, b)].astype(F32))
+    mixed = []
+    for h in range(2):
+        for i in range(4):
+            res = residual_ref[16 * i : 16 * i + 16, 128 * h : 128 * h + 128]
+            mixed.append((res + sums[4 * h + i]).astype(BF))
+    for t in range(8):
+        h, lane = t // 4, 32 * (t % 4)
+        ypack[t] = jnp.concatenate(
+            [mixed[4 * h + i][:, lane : lane + 32] for i in range(4)], axis=1
+        )
+    copies = []
+    for i, (dx, dc) in enumerate(lines):
+        peer = line_peer(at, dx, dc)
+        copies.append(
+            send(ypack.at[2 * peer[2] + peer[3]], yarrive.at[tp], sems, 139 + i, peer)
+        )
+    yarrive[pl.ds(tp, 1)] = ypack[pl.ds(tp, 1)]
+    for copy in copies:
+        copy.wait()
+    out_ref[...] = yarrive[...]
+
+
+def mixer(normed, packed, x, result, gain, gate, wide, narrow):
+    vmem = pl.BlockSpec(memory_space=pltpu.VMEM)
+    counts = [count for _, count, _ in PARTS]
+    boxes = [pltpu.VMEM((4, 4, 4, count, 16, 128), BF) for count in counts]
+    receive = []
+    for phase in (2, 1, 0):
+        lead = (4,) * phase
+        shapes = [(*lead, count, 16, 128) for count in counts]
+        low = [pltpu.VMEM((s[0] // 2, *s[1:]), BF) for s in shapes]
+        high = [pltpu.VMEM((s[0] - s[0] // 2, *s[1:]), BF) for s in shapes]
+        full = [pltpu.VMEM(s, BF) for s in shapes]
+        receive += low + high + full + full
+    return pl.pallas_call(
+        mixer_kernel,
+        out_shape=jax.ShapeDtypeStruct((8, 16, 128), BF),
+        in_specs=[vmem] * 8,
+        out_specs=vmem,
+        scratch_shapes=[
+            pltpu.VMEM((16, 64, 256), BF),
+            pltpu.VMEM((8, 64, 256), BF),
+            pltpu.VMEM((7, 64, 256), BF),
+            pltpu.VMEM((8, 8, 128), F32),
+            pltpu.VMEM((64, 256), F32),
+            pltpu.VMEM((16, 8, 128), F32),
+            pltpu.VMEM((8, 128), F32),
+            pltpu.VMEM((4, 8, 128), F32),
+            pltpu.VMEM((2, 16, 256, 256), BF),
+            pltpu.VMEM((2, 128, 4096), BF),
+            pltpu.VMEM((2, 256, 256), F32),
+            *boxes,
+            *boxes,
+            *receive,
+            pltpu.VMEM((8, 16, 128), BF),
+            pltpu.VMEM((8, 16, 128), BF),
+            pltpu.SemaphoreType.DMA((146,)),
+            pltpu.SemaphoreType.DMA((146,)),
+        ],
+        compiler_params=pltpu.CompilerParams(
+            collective_id=0, has_side_effects=True, vmem_limit_bytes=48 * 1024 * 1024
+        ),
+        name="mixer",
+    )(normed, packed, x, result, gain, gate, wide, narrow)
+
+
+def spread_kernel(packed_ref, mixed_ref, out_ref):
+    place = packed_ref[0:1, :]
+    total = jnp.zeros((1024, 32), F32)
+    j = lax.broadcasted_iota(jnp.int32, (128, 1024), 0)
+    rows = 64 * (j // 16) + j % 16
+    for a in range(4):
+        chosen = jnp.where(rows + 16 * a == place, 1.0, 0.0).astype(BF)
+        piece = mixed_ref[...].reshape(128, 128)[:, 32 * a : 32 * a + 32]
+        total = total + lax.dot_general(
+            chosen, piece, (((0,), (0,)), ((), ())), preferred_element_type=F32
+        )
+    out_ref[...] = total.astype(BF)
+
+
+def spread(packed, mixed):
+    vmem = pl.BlockSpec(memory_space=pltpu.VMEM)
+    return pl.pallas_call(
+        spread_kernel,
+        out_shape=jax.ShapeDtypeStruct((1024, 32), BF),
+        in_specs=[vmem] * 2,
+        out_specs=vmem,
+        name="spread",
+    )(packed, mixed)
+
+
+def places_of_live_rows(lengths):
+    order = jnp.arange(128, dtype=jnp.int32)
+    starts = jnp.sum(jnp.where(order[:, None] < order[None, :], lengths[:, None], 0), axis=0)
+    slot = jnp.arange(FRESH_PLACES, dtype=jnp.int32)[None, :]
+    place = jnp.where(slot < lengths[:, None], starts[:, None] + slot, -1)
+    return jnp.broadcast_to(place.reshape(1, 1024), (8, 1024))
 
 
 def local(
@@ -158,30 +584,19 @@
         heads_out.reshape(rows_dev, width_dev) * jax.nn.silu(z_outgate),
         0.0,
     ).astype(jnp.bfloat16)
-    head_partial = jnp.dot(
-        gather_directly(normed, KV, 0), result_matrix, preferred_element_type=jnp.float32
-    ).astype(jnp.bfloat16)
-    attended = sent_and_summed(head_partial, TP, 1)
-    residual = (tokens_wide + attended).astype(jnp.bfloat16)
-    resid_wide = residual.astype(jnp.float32)
-    resid_squares = one_axis_at_a_time(jnp.sum(resid_wide * resid_wide, axis=1), KV_TP)
-    second_in = (
-        resid_wide * later_rescale_vector * lax.rsqrt(resid_squares / D + epsilon)[:, None]
-    ).astype(jnp.bfloat16)
-    live_rows = (
-        jnp.arange(FRESH_PLACES, dtype=jnp.int32)[None, :] < fresh_extents[:, None]
-    ).reshape(all_rows)
-    piece = lax.all_gather(second_in, KV_TP, axis=1, tiled=True)
-    gated = jnp.dot(piece, mixer_switch_matrix, preferred_element_type=jnp.float32)
-    upward = jnp.dot(piece, widening_matrix, preferred_element_type=jnp.float32)
-    hidden = (jax.nn.silu(gated) * upward).astype(jnp.bfloat16)
-    mixer_terms = sum_in_two_steps(
-        jnp.dot(hidden, narrowing_matrix, preferred_element_type=jnp.float32).astype(jnp.bfloat16),
-        (("kv_0", "kv_1", "tp_0"), "tp_1"),
-        1,
-    )
-    mixed = jnp.where(live_rows[:, None], resid_wide + mixer_terms, 0.0).astype(jnp.bfloat16)
-    return (mixed, carried)
+    packed = places_of_live_rows(fresh_extents)
+    gain = jnp.broadcast_to(jnp.pad(later_rescale_vector, (0, 96))[None], (8, 128))
+    mixed = mixer(
+        normed,
+        packed,
+        columns,
+        result_matrix,
+        gain,
+        mixer_switch_matrix,
+        widening_matrix,
+        narrowing_matrix,
+    )
+    return (spread(packed, mixed), carried)
 
 
 def solution(mesh):

time: 367 us -> 221 us (0.60)
  waiting for transfers between devices: 163 us -> 40.4 us
  Pallas kernels: 0 us -> 87.4 us
  blocking collectives: 94.5 us -> 15 us
  other arithmetic: 22.3 us -> 9.85 us
  local copies, waits for them, and re-layouts: 24.8 us -> 14.3 us
  starting transfers between devices: 11.6 us -> 5.09 us
    pallas_call x0 -> x2, Pallas kernels: none -> 87.4 us  [the longest x1 85.4 us: mixer(): pl.pallas_call(mixer_kernel, out_shape=jax.ShapeDtypeStruct((8, 16, 128),...]
    all_gather x1 -> x0, waiting for transfers between devices: 65.2 us -> none  [local(): piece = lax.all_gather(second_in, KV_TP, axis=1, tiled=True)]
    all_to_all x1 -> x0, waiting for transfers between devices: 53.2 us -> none  [sum_in_two_steps(): lax.all_to_all(nearer.astype(jnp.bfloat16), far, split_axis=0, concat_axi...]
    all_to_all x2 -> x0, blocking collectives: 36.3 us -> none  [sent_and_summed(): pieces = lax.all_to_all(split_up(x, dim, devices), axis, 0, 0, tiled=True)]
    psum x4 -> x0, blocking collectives: 29.4 us -> none  [one_axis_at_a_time(): return functools.reduce(lax.psum, axes, x)]
    dot_general x8, matrix products: 15.1 us -> 32.1 us  [local(): jnp.einsum('bhd,bhdv->bhv', query[:, position], carried, precision=lax.Pr...]
    dot_general x3 -> x0, matrix products: 16.3 us -> none  [the longest x1 10.9 us: local(): jnp.dot(hidden, narrowing_matrix, preferred_element_type=jnp.float32)]
    all_to_all x2 -> x1, blocking collectives: 28.8 us -> 15 us  [copy_for_each(): lax.all_to_all(jnp.broadcast_to(x[None], (devices, *x.shape)), axis, 0, 0...]
  transfers between devices with their start and end apart: 5 -> 3, of which waited for: 5 -> 3; matrix products, arithmetic and copies ran while one was open for 0% -> 2% of each run, Pallas kernels for 0% -> 0%
where the time goes in v1:
time: 221 us; the launch traced here: 220 us
  Pallas kernels  87.4 us (40%)
  waiting for transfers between devices  40.4 us (18%)
  matrix products  33.5 us (15%)
  blocking collectives  15 us (7%)
  between operations  14.4 us (7%)
  local copies, waits for them, and re-layouts  14.3 us (6%)
  other arithmetic  9.85 us (4%)
  starting transfers between devices  5.09 us (2%)
    pallas_call x1, Pallas kernels, mixer(): pl.pallas_call(mixer_kernel, out_shape=jax.ShapeDtypeStruct((8, 16, 128),...  85.4 us
    reduce_scatter x2, waiting for transfers between devices, own_rows(): total = lax.psum_scatter(total, axis, scatter_dimension=0, tiled=True)  39 us
    dot_general x8, matrix products, local(): jnp.einsum('bhd,bhdv->bhv', query[:, position], carried, precision=lax.Pr...  32.1 us
    all_to_all x1, blocking collectives, copy_for_each(): lax.all_to_all(jnp.broadcast_to(x[None], (devices, *x.shape)), axis, 0, 0...  15 us
    unnamed x37, local copies, waits for them, and re-layouts  7.62 us
    all_to_all x1, starting transfers between devices, sum_at_owner(): pieces = lax.all_to_all(split_up(x, dim, devices), axis, 0, 0, tiled=True)  5.01 us
    add x1, other arithmetic, local(): decays[:, position, :, :, None] * carried  4.68 us
  transfers between devices with their start and end apart: 3, of which 3 were waited for; matrix products, arithmetic and copies ran while one was open for 2% of the time, Pallas kernels for 0%

profile of v1, /device:TPU:1, one launch (start us, length us, event | category | flops | bytes accessed | tf_op | source)
XLA Modules:
  0.0 220.0 jit_solution(13238824748063568407)
XLA Ops:
  7.2 0.9 broadcast_in_dim.81
  8.2 15.0 %all_to_all.14 = bf16[8,1024,32]{1,2,0:T(8,128)(2,1)S(1)} all-to-all(bf16[8,1024,32]{1,2,0:T(8,128)(2,1)S(1)} %broadcast_in_dim.81), channel_id=1, replica_groups=mesh['kv_0'=4,'kv_1'=4,'tp_0'=4,'tp_1'=2] {'tp_0','tp_1'}, dimensions={0} | all-to-all | bytes 1048576 | tf_op jit(solution)/shard_map/all_to_all | solution.py:30
  23.2 0.9 multiply_convert_fusion
  24.1 0.4 convolution_convert_fusion
  24.5 0.4 convolution_convert_fusion.1
  24.9 0.4 convolution_convert_fusion.2
  25.2 0.4 convolution_convert_fusion.3
  25.6 1.6 pad_maximum_fusion
  27.3 0.6 copy-done.14
  28.0 30.1 %reduce-scatter.3.cloned.1.call-done = bf16[256,1024]{1,0:T(8,128)(2,1)} async-done(((bf16[1024,1024]{1,0:T(8,128)(2,1)}), bf16[256,1024]{1,0:T(8,128)(2,1)}) %reduce-scatter.3.cloned.1.call-update) | async-done | bytes 524304 | tf_op jit(solution)/shard_map/reduce_scatter | solution.py:51
  58.2 0.1 select_reduce_fusion
  58.3 0.1 add_select_fusion
  58.4 0.1 multiply_reduce_fusion
  58.6 0.7 all_to_all.10
  59.2 5.0 %all-to-all-start.1 = ((f32[16,1,64]{2,1,0:T(1,128)}), f32[16,1,64]{2,1,0:T(1,128)S(1)}, u32[]{:S(2)}, u32[]{:S(2)}) async-start(f32[16,1,64]{2,1,0:T(1,128)} %all_to_all.10), calls=%async_computation.3 | async-start | bytes 16384 | tf_op jit(solution)/shard_map/all_to_all | solution.py:44
  64.3 0.6 broadcast_bitcast_fusion
  64.9 0.6 lt.71
  65.5 0.7 select_n.31
  66.2 0.7 copy.52.gate_ref
  66.9 1.6 copy.53.wide_ref
  68.5 0.5 pad.4
  69.0 0.2 copy.51.x_ref
  69.2 1.4 all-to-all-done.1
  70.6 8.9 %reduce-scatter.5.cloned.1.call-done = bf16[64,1024]{1,0:T(8,128)(2,1)} async-done(((bf16[256,1024]{1,0:T(8,128)(2,1)}), bf16[64,1024]{1,0:T(8,128)(2,1)}) %reduce-scatter.5.cloned.1.call-update) | async-done | bytes 131088 | tf_op jit(solution)/shard_map/reduce_scatter | solution.py:51
  79.5 1.1 convert_multiply_fusion
  80.7 0.6 copy-done.7
  81.3 0.1 exponential_select_fusion
  81.4 0.1 fusion.21
  81.5 2.6 %convolution_bitcast_fusion.7 = f32[8,1,2,128]{3,1,2,0:T(1,128)S(1)} fusion(f32[8,2,128,128]{3,2,1,0:T(8,128)} %param.18, f32[8,2,128]{2,1,0:T(2,128)S(1)} %bitcast.148, f32[8,2,128]{2,1,0:T(2,128)S(1)} %bitcast.164, f32[8,2,128]{2,1,0:T(2,128)S(1)} %bitcast.156, f32[8,8,2,128]{3,1,2,0:T(8,128)S(1)} %get-tuple-element.12), kind=kOutput, calls=%fused_computation.12 | convolution fusion | flops 3932160 | bytes 1089536 | tf_op jit(solution)/shard_map/bhd,bhdv->bhv/dot_general | solution.py:572
  84.2 2.7 %convolution_bitcast_fusion.6 = f32[8,1,2,128]{3,1,2,0:T(1,128)} fusion(f32[8,2,128,128]{3,2,1,0:T(8,128)S(1)} %copy-done.5, f32[8,2,128]{2,1,0:T(2,128)S(1)} %bitcast.193, f32[8,2,128]{2,1,0:T(2,128)S(1)} %bitcast.228, f32[8,2,128]{2,1,0:T(2,128)S(1)} %bitcast.221, f32[8,2,128]{2,1,0:T(2,128)S(1)} %bitcast.149, f32[8,2,128]{2,1,0:T(2,128)S(1)} %bitcast.165, ...), kind=kOutput, calls=%fused_computation.11 | convolution fusion | flops 4718592 | bytes 1114112 | tf_op jit(solution)/shard_map/bhd,bhdv->bhv/dot_general | solution.py:572
  86.9 3.6 %convolution_bitcast_fusion.5 = f32[8,1,2,128]{3,1,2,0:T(1,128)} fusion(f32[8,2,128]{2,1,0:T(2,128)S(1)} %bitcast.187, f32[8,2,128]{2,1,0:T(2,128)S(1)} %bitcast.235, f32[8,2,128]{2,1,0:T(2,128)S(1)} %bitcast.215, f32[8,2,128,128]{3,2,1,0:T(8,128)S(1)} %copy-done.5, f32[8,2,128]{2,1,0:T(2,128)S(1)} %bitcast.194, f32[8,2,128]{2,1,0:T(2,128)S(1)} %bitcast.229, ...), kind=kOutput, calls=%fused_computation.10 | convolution fusion | flops 5505024 | bytes 1138688 | tf_op jit(solution)/shard_map/bhd,bhdv->bhv/dot_general | solution.py:572
  90.5 4.2 %convolution_bitcast_fusion.4 = f32[8,1,2,128]{3,1,2,0:T(1,128)} fusion(f32[8,8,2,128]{3,1,2,0:T(8,128)S(1)} %get-tuple-element.12, f32[8,2,128]{2,1,0:T(2,128)S(1)} %bitcast.182, f32[8,2,128]{2,1,0:T(2,128)S(1)} %bitcast.241, f32[8,2,128]{2,1,0:T(2,128)S(1)} %bitcast.210, f32[8,2,128]{2,1,0:T(2,128)S(1)} %bitcast.188, f32[8,2,128]{2,1,0:T(2,128)S(1)} %bitcast.236, ...), kind=kOutput, calls=%fused_computation.9 | convolution fusion | flops 6291456 | bytes 1163264 | tf_op jit(solution)/shard_map/bhd,bhdv->bhv/dot_general | solution.py:572
  94.7 5.5 %convolution_bitcast_fusion.3 = f32[8,1,2,128]{3,1,2,0:T(1,128)} fusion(f32[8,2,128]{2,1,0:T(2,128)S(1)} %bitcast.178, f32[8,2,128]{2,1,0:T(2,128)S(1)} %bitcast.246, f32[8,2,128]{2,1,0:T(2,128)S(1)} %bitcast.206, f32[8,8,2,128]{3,1,2,0:T(8,128)S(1)} %get-tuple-element.12, f32[8,2,128]{2,1,0:T(2,128)S(1)} %bitcast.183, f32[8,2,128]{2,1,0:T(2,128)S(1)} %bitcast.242, ...), kind=kOutput, calls=%fused_computation.8 | convolution fusion | flops 7077888 | bytes 1187840 | tf_op jit(solution)/shard_map/bhd,bhdv->bhv/dot_general | solution.py:572
  100.1 6.0 %convolution_bitcast_fusion.2 = f32[8,1,2,128]{3,1,2,0:T(1,128)} fusion(f32[8,2,128]{2,1,0:T(2,128)S(1)} %bitcast.175, f32[8,2,128]{2,1,0:T(2,128)S(1)} %bitcast.250, f32[8,2,128]{2,1,0:T(2,128)S(1)} %bitcast.203, f32[8,2,128]{2,1,0:T(2,128)S(1)} %bitcast.179, f32[8,2,128]{2,1,0:T(2,128)S(1)} %bitcast.247, f32[8,2,128]{2,1,0:T(2,128)S(1)} %bitcast.207, ...), kind=kOutput, calls=%fused_computation.7 | convolution fusion | flops 7864320 | bytes 1212416 | tf_op jit(solution)/shard_map/bhd,bhdv->bhv/dot_general | solution.py:572
  106.1 6.5 %convolution_bitcast_fusion.1 = f32[8,1,2,128]{3,1,2,0:T(1,128)} fusion(f32[8,2,128]{2,1,0:T(2,128)S(1)} %bitcast.173, f32[8,2,128]{2,1,0:T(2,128)S(1)} %bitcast.253, f32[8,2,128]{2,1,0:T(2,128)S(1)} %bitcast.201, f32[8,2,128]{2,1,0:T(2,128)S(1)} %bitcast.176, f32[8,2,128]{2,1,0:T(2,128)S(1)} %bitcast.251, f32[8,2,128]{2,1,0:T(2,128)S(1)} %bitcast.204, ...), kind=kOutput, calls=%fused_computation.6 | convolution fusion | flops 8650752 | bytes 1236992 | tf_op jit(solution)/shard_map/bhd,bhdv->bhv/dot_general | solution.py:572
  112.7 4.7 %multiply_add_fusion = f32[8,2,128,128]{3,2,1,0:T(8,128)S(1)} fusion(f32[8,2,128]{2,1,0:T(2,128)S(1)} %bitcast.172, f32[8,2,128]{2,1,0:T(2,128)S(1)} %bitcast.255, f32[8,2,128]{2,1,0:T(2,128)S(1)} %bitcast.200, f32[8,2,128]{2,1,0:T(2,128)S(1)} %bitcast.174, f32[8,2,128]{2,1,0:T(2,128)S(1)} %bitcast.254, f32[8,2,128]{2,1,0:T(2,128)S(1)} %bitcast.202, ...), kind=kLoop, calls=%fused_computation.13 | loop fusion | flops 6291456 | bytes 2293760 | tf_op jit(solution)/shard_map/add | solution.py:568
  117.4 1.0 copy-done.6
  118.3 1.0 convolution_bitcast_fusion
  119.3 0.9 stack.35
  120.2 0.1 multiply_reduce_fusion.1
  120.3 0.9 fusion.20.normed_ref
  121.2 0.7 broadcast_in_dim.79.packed_ref
  121.9 0.6 broadcast_in_dim.85.gain_ref
  122.6 0.9 copy-done.4
  123.5 85.4 %mixer.1.mixed_ref = bf16[8,16,128]{2,1,0:T(8,128)(2,1)S(1)} custom-call(bf16[64,256]{1,0:T(8,128)(2,1)S(1)} %fusion.20.normed_ref, s32[8,1024]{1,0:T(8,128)S(1)} %broadcast_in_dim.79.packed_ref, bf16[1024,256]{1,0:T(8,128)(2,1)S(1)} %copy.51.x_ref, bf16[256,256]{1,0:T(8,128)(2,1)S(1)} %copy-done.4, f32[8,128]{1,0:T(8,128)S(1)} %broadcast_in_dim.85.gain_ref, ...), custom_call_target="tpu_custom_call" | custom-call | tf_op jit(solution)/shard_map/mixer/pallas_call | solution.py:434
  208.9 0.6 copy-done.3
  209.5 2.0 spread.1
  211.5 1.7 copy.54
  (43 shorter events, 0.5 us)
Async XLA Ops:
  7.2 17.0 %copy-start = (bf16[256,256]{1,0:T(8,128)(2,1)S(1)}, bf16[256,256]{1,0:T(8,128)(2,1)}, u32[]{:S(2)}) copy-start(bf16[256,256]{1,0:T(8,128)(2,1)} %param.23) | copy-start | bytes 393220
  7.2 17.3 %copy-start.9 = (bf16[256,256]{1,0:T(8,128)(2,1)S(1)}, bf16[256,256]{1,0:T(8,128)(2,1)}, u32[]{:S(2)}) copy-start(bf16[256,256]{1,0:T(8,128)(2,1)} %param.22) | copy-start | bytes 393220
  7.2 51.0 %reduce-scatter.3.cloned.1.call-start = ((), (), s32[]{:S(2)}) async-start(), calls=%async_computation.4 | async-start | bytes 2621440 | tf_op jit(solution)/shard_map/reduce_scatter | solution.py:51
  8.2 16.7 %copy-start.10 = (bf16[256,256]{1,0:T(8,128)(2,1)S(1)}, bf16[256,256]{1,0:T(8,128)(2,1)}, u32[]{:S(2)}) copy-start(bf16[256,256]{1,0:T(8,128)(2,1)} %param.21) | copy-start | bytes 393220
  23.2 2.0 copy-start.11
  27.2 0.7 copy-start.14
  27.2 31.1 %copy-start.12 = (f32[256]{0:T(256)S(1)}, f32[256]{0:T(256)}, u32[]{:S(2)}) copy-start(f32[256]{0:T(256)} %param.24) | copy-start | bytes 3076
  27.2 37.0 %copy-start.15 = (f32[128]{0:T(128)S(1)}, f32[128]{0:T(128)}, u32[]{:S(2)}) copy-start(f32[128]{0:T(128)} %param.26) | copy-start | bytes 1540
  27.2 37.6 %copy-start.13 = (f32[64,2]{0,1:T(2,128)S(1)}, f32[64,2]{0,1:T(2,128)}, u32[]{:S(2)}) copy-start(f32[64,2]{0,1:T(2,128)} %param.25) | copy-start | bytes 1540
  27.2 39.0 %copy-start.8 = (bf16[4096,86]{0,1:T(8,128)(2,1)S(1)}, bf16[4096,86]{0,1:T(8,128)(2,1)}, u32[]{:S(2)}) copy-start(bf16[4096,86]{0,1:T(8,128)(2,1)} %param.29) | copy-start | bytes 2113540
  27.3 52.3 %reduce-scatter.5.cloned.1.call-start = ((), (), s32[]{:S(2)}) async-start(), calls=%async_computation.5 | async-start | bytes 655360 | tf_op jit(solution)/shard_map/reduce_scatter | solution.py:51
  58.4 10.1 %copy-start.16 = (f32[32]{0:T(128)S(1)}, f32[32]{0:T(128)}, u32[]{:S(2)}) copy-start(f32[32]{0:T(128)} %param.28) | copy-start | bytes 388
  59.2 11.4 %all-to-all-start.1 = ((f32[16,1,64]{2,1,0:T(1,128)}), f32[16,1,64]{2,1,0:T(1,128)S(1)}, u32[]{:S(2)}, u32[]{:S(2)}) async-start(f32[16,1,64]{2,1,0:T(1,128)} %all_to_all.10), calls=%async_computation.3 | async-start | bytes 16384 | tf_op jit(solution)/shard_map/all_to_all | solution.py:44
  79.5 4.6 %copy-start.5 = (f32[8,2,128,128]{3,2,1,0:T(8,128)S(1)}, f32[8,2,128,128]{3,2,1,0:T(8,128)}, u32[]{:S(2)}) copy-start(f32[8,2,128,128]{3,2,1,0:T(8,128)} %param.18) | copy-start | bytes 3145732
  80.6 0.7 copy-start.7
  112.6 9.9 %copy-start.1 = (bf16[86,4096]{1,0:T(8,128)(2,1)S(1)}, bf16[86,4096]{1,0:T(8,128)(2,1)}, u32[]{:S(2)}) copy-start(bf16[86,4096]{1,0:T(8,128)(2,1)} %narrow_ref.1) | copy-start | bytes 2113540
  117.3 1.0 copy-start.6
  121.9 86.9 %copy-start.2 = (s32[8,1024]{1,0:T(8,128)}, s32[8,1024]{1,0:T(8,128)S(1)}, u32[]{:S(2)}) copy-start(s32[8,1024]{1,0:T(8,128)S(1)} %broadcast_in_dim.79.packed_ref) | copy-start | bytes 98308
  122.6 0.9 copy-start.4
  208.9 0.6 copy-start.3
Sparse Core Ops, SparseCore 0:
  27.4 30.7 reduce-scatter.2
  60.6 18.9 reduce-scatter.4

commit v2 on v1

v2 whole, which is shorter than its diff:
```python
import jax
import jax.numpy as jnp
from jax import lax
from jax.experimental import pallas as pl
from jax.experimental.pallas import tpu as pltpu
from jax.sharding import Mesh
from jax.sharding import PartitionSpec as P

KV = ("kv_0", "kv_1")
TP = ("tp_0", "tp_1")
KV_TP = ("kv_0", "kv_1", "tp_0", "tp_1")
MESH = pl.DeviceIdType.MESH
EPS = 1e-06
F32 = jnp.float32
BF = jnp.bfloat16
PARTS = ((0, 3), (3, 3), (6, 2))
ORDERS = ("xyz", "yzx", "zxy")
PLANE_ORDERS = ("zy", "yz")


def my_position():
    return dict(
        z=lax.axis_index("kv_0"),
        y=lax.axis_index("kv_1"),
        x=lax.axis_index("tp_0"),
        c=lax.axis_index("tp_1"),
    )


def device_at(at, **moved):
    there = dict(at, **moved)
    return (there["z"], there["y"], there["x"], there["c"])


def plane_offsets():
    return [(dz, dy) for dz in range(4) for dy in range(4) if dz or dy]


def line_offsets():
    return [(dx, dc) for dx in range(4) for dc in range(2) if dx or dc]


def plane_peer(at, dz, dy):
    return device_at(at, z=(at["z"] + dz) % 4, y=(at["y"] + dy) % 4)


def line_peer(at, dx, dc):
    return device_at(at, x=(at["x"] + dx) % 4, c=(at["c"] + dc) % 2)


def meet(peers):
    barrier = pltpu.get_barrier_semaphore()
    for peer in peers:
        pl.semaphore_signal(barrier, inc=1, device_id=peer, device_id_type=MESH)
    pl.semaphore_wait(barrier, len(peers))


def send(src, dst, sems, i, peer):
    copy = pltpu.make_async_remote_copy(
        src_ref=src,
        dst_ref=dst,
        send_sem=sems[0].at[i],
        recv_sem=sems[1].at[i],
        device_id=peer,
        device_id_type=MESH,
    )
    copy.start()
    return copy


def times(a, b, dims=((1,), (1,))):
    return lax.dot_general(a, b, (dims, ((), ())), preferred_element_type=F32)


def row_of(column, rows):
    eye = lax.broadcasted_iota(jnp.int32, (rows, 128), 0) == lax.broadcasted_iota(
        jnp.int32, (rows, 128), 1
    )
    return jnp.sum(jnp.where(eye, column, 0.0), axis=0, keepdims=True)


def column_of(row, rows):
    eye = lax.broadcasted_iota(jnp.int32, (rows, 128), 0) == lax.broadcasted_iota(
        jnp.int32, (rows, 128), 1
    )
    return jnp.sum(jnp.where(eye, row, 0.0), axis=1, keepdims=True)


def picks(place, start, rows):
    want = lax.broadcasted_iota(jnp.int32, (rows, 1024), 0) + start
    return jnp.where(want == place, 1.0, 0.0).astype(BF)


def halves(length):
    return pl.ds(0, length // 2), pl.ds(length // 2, length - length // 2)


def gather_phase(at, bufs, parts, phase, sems, base):
    first = []
    for p, order in enumerate(parts):
        axis = order[phase]
        pre = tuple(at[a] for a in order[:phase:-1])
        m = at[axis]
        up, down = (m + 1) % 4, (m + 3) % 4
        own = bufs[p].at[(*pre, m)]
        i = base + 4 * p
        first.append((
            send(own, own, sems, i, device_at(at, **{axis: up})),
            send(own, own, sems, i + 1, device_at(at, **{axis: down})),
        ))
    second = []
    for p, order in enumerate(parts):
        axis = order[phase]
        pre = tuple(at[a] for a in order[:phase:-1])
        m = at[axis]
        up, down = (m + 1) % 4, (m + 3) % 4
        lo, hi = halves(bufs[p].shape[len(pre) + 1])
        i = base + 4 * p
        first[p][0].wait_recv()
        from_down = bufs[p].at[(*pre, down, lo)]
        a = send(from_down, from_down, sems, i + 2, device_at(at, **{axis: up}))
        first[p][1].wait_recv()
        from_up = bufs[p].at[(*pre, up, hi)]
        b = send(from_up, from_up, sems, i + 3, device_at(at, **{axis: down}))
        second.append((a, b))
    for p in range(len(parts)):
        for copy in first[p]:
            copy.wait_send()
        for copy in second[p]:
            copy.wait()


def add_into(ref, idx, terms):
    total = ref[idx].astype(F32)
    for term in terms:
        total = total + term.astype(F32)
    ref[idx] = total.astype(BF)


def reduce_phase(at, bufs, parts, phase, one_up, one_down, two_up, two_down, sems, base, keep=True):
    early = []
    for p, order in enumerate(parts):
        axis = order[phase]
        pre = tuple(at[a] for a in order[:phase:-1])
        m = at[axis]
        up, down, far = (m + 1) % 4, (m + 3) % 4, (m + 2) % 4
        to_up, to_down = device_at(at, **{axis: up}), device_at(at, **{axis: down})
        lo, hi = halves(bufs[p].shape[len(pre) + 1])
        i = base + 6 * p
        early.append((
            send(bufs[p].at[(*pre, far, lo)], one_up[p], sems, i, to_up),
            send(bufs[p].at[(*pre, far, hi)], one_down[p], sems, i + 1, to_down),
            send(bufs[p].at[(*pre, up, hi)], two_up[p].at[hi], sems, i + 2, to_up),
            send(bufs[p].at[(*pre, down, lo)], two_down[p].at[lo], sems, i + 3, to_down),
        ))
    late = []
    for p, order in enumerate(parts):
        axis = order[phase]
        pre = tuple(at[a] for a in order[:phase:-1])
        m = at[axis]
        up, down = (m + 1) % 4, (m + 3) % 4
        to_up, to_down = device_at(at, **{axis: up}), device_at(at, **{axis: down})
        lo, hi = halves(bufs[p].shape[len(pre) + 1])
        i = base + 6 * p
        early[p][0].wait_recv()
        add_into(bufs[p], (*pre, up, lo), [one_up[p][...]])
        a = send(bufs[p].at[(*pre, up, lo)], two_up[p].at[lo], sems, i + 4, to_up)
        early[p][1].wait_recv()
        add_into(bufs[p], (*pre, down, hi), [one_down[p][...]])
        b = send(bufs[p].at[(*pre, down, hi)], two_down[p].at[hi], sems, i + 5, to_down)
        late.append((a, b))
    sums = []
    for p, order in enumerate(parts):
        axis = order[phase]
        pre = tuple(at[a] for a in order[:phase:-1])
        for copy in early[p][2:]:
            copy.wait_recv()
        for copy in late[p]:
            copy.wait_recv()
        for copy in (*early[p], *late[p]):
            copy.wait_send()
        own = (*pre, at[axis])
        total = bufs[p][own].astype(F32) + two_up[p][...].astype(F32) + two_down[p][...].astype(F32)
        if keep:
            bufs[p][own] = total.astype(BF)
        sums.append(total)
    return sums


def mixer_kernel(
    normed_ref, packed_ref, x_ref, result_ref, gain_ref, gate_ref, wide_ref, narrow_ref,
    out_ref,
    heads, partial, arrived, own_gain, gains, residual_ref, squares, squares_sum, squares_line,
    weights, narrow, total, ga, gb, gc,
    *rest,
):
    (pa, pb, pc), rest = rest[:3], rest[3:]
    receive, rest = rest[:36], rest[36:]
    ypack, yarrive, sends, recvs = rest
    sems = (sends, recvs)
    at = my_position()
    kv = 4 * at["z"] + at["y"]
    tp = 2 * at["x"] + at["c"]
    planes, lines = plane_offsets(), line_offsets()
    meet([plane_peer(at, *d) for d in planes] + [line_peer(at, *d) for d in lines])

    copies = [
        send(normed_ref, heads.at[kv], sems, i, plane_peer(at, *d)) for i, d in enumerate(planes)
    ]
    own_gain[...] = jnp.broadcast_to(
        jnp.concatenate([gain_ref[...], jnp.zeros((1, 96), F32)], axis=1), (8, 128)
    )
    gain_copies = [
        send(own_gain, gains.at[tp], sems, 15 + i, line_peer(at, *d)) for i, d in enumerate(lines)
    ]
    partner = line_peer(at, 0, 1)
    for slot, start in ((0, 80), (1, 96)):
        weights[slot, :, start:128] = jnp.zeros((2, 128 - start, 4096), BF)
        narrow[slot, start:128] = jnp.zeros((128 - start, 4096), BF)
    weights[0, 0, 0:86] = gate_ref[...]
    weights[0, 1, 0:86] = wide_ref[...]
    narrow[0, 0:86] = narrow_ref[...]
    weight_copy = send(weights.at[0, :, 0:96], weights.at[1, :, 0:96], sems, 22, partner)
    narrow_copy = send(narrow.at[0, 0:96], narrow.at[1, 0:96], sems, 23, partner)
    heads[pl.ds(kv, 1)] = normed_ref[...][None]
    gains[pl.ds(tp, 1)] = own_gain[...][None]

    place = packed_ref[0:1, :]

    def chosen(start, rows):
        return picks(place, start, rows)

    for copy in copies:
        copy.wait()
    all_heads = heads[...].reshape(1024, 256)
    for part in range(2):
        live = jnp.dot(chosen(256 * part, 256), all_heads, preferred_element_type=F32).astype(BF)
        partial[4 * part : 4 * part + 4] = (
            jnp.dot(live, result_ref[...], preferred_element_type=F32)
            .astype(BF)
            .reshape(4, 64, 256)
        )
    copies = []
    for i, (dx, dc) in enumerate(lines):
        peer = line_peer(at, dx, dc)
        copies.append(
            send(partial.at[2 * peer[2] + peer[3]], arrived.at[i], sems, 24 + i, peer)
        )
    for copy in gain_copies:
        copy.wait()
    gain = jnp.concatenate([gains[t, 0:1, 0:32] for t in range(8)], axis=1)
    attended = partial[tp].astype(F32)
    for i, copy in enumerate(copies):
        copy.wait()
        attended = attended + arrived[i].astype(F32)
    residual = (x_ref[...].astype(F32) + attended).astype(BF).astype(F32)
    residual_ref[...] = residual
    own_squares = jnp.sum(residual * residual, axis=1, keepdims=True)
    squares[0] = jnp.broadcast_to(row_of(own_squares, 64), (8, 128))
    square_copies = [
        send(squares.at[0], squares.at[1 + i], sems, 31 + i, plane_peer(at, *d))
        for i, d in enumerate(planes)
    ]
    tile = (residual * gain).astype(BF)
    blocks = [tile[16 * i : 16 * i + 16, 128 * h : 128 * h + 128] for h in range(2) for i in range(4)]
    bufs = (ga, gb, gc)
    for p, ((start, count), order) in enumerate(zip(PARTS, ORDERS)):
        idx = tuple(at[a] for a in order[::-1])
        for b in range(count):
            bufs[p][(*idx, b)] = blocks[start + b]
    gather_phase(at, bufs, ORDERS, 0, sems, 46)
    gather_phase(at, bufs, ORDERS, 1, sems, 58)
    for copy in square_copies:
        copy.wait()
    own_sum = jnp.sum(squares[...], axis=0)
    squares_sum[...] = own_sum
    squares_line[pl.ds(at["x"], 1)] = own_sum[None]
    line_copies = [
        send(squares_sum, squares_line.at[at["x"]], sems, 82 + dx - 1, line_peer(at, dx, 0))
        for dx in (1, 2, 3)
    ]
    gather_phase(at, bufs, ORDERS, 2, sems, 70)
    for copy in line_copies:
        copy.wait()
    weight_copy.wait()
    narrow_copy.wait()

    def rows_at(zz, yy):
        a, b, c = ga[zz, yy], gb[:, zz, yy], gc[yy, :, zz]
        v = jnp.concatenate([a, b, c], axis=1)
        return jnp.concatenate(
            [v[:, 0:4].reshape(256, 128), v[:, 4:8].reshape(256, 128)], axis=1
        )

    def widening(k, carry):
        lhs = rows_at(k // 4, k % 4)
        cols = pl.ds(pl.multiple_of(k * 256, 256), 256)
        for core in range(2):
            term = times(lhs, weights[core, :, :, cols].reshape(256, 256))

            @pl.when(k == 0)
            def _():
                total[core] = term

            @pl.when(k > 0)
            def _():
                total[core] += term

        return carry

    lax.fori_loop(0, 16, widening, 0)
    scale = lax.rsqrt(
        jnp.concatenate([column_of(squares_line[g, 0:1, :], 64) for g in range(4)], axis=0)
        / 4096
        + EPS
    )
    hidden = []
    for core in range(2):
        gated = total[core, :, 0:128] * scale
        upward = total[core, :, 128:256] * scale
        hidden.append((gated * jax.nn.sigmoid(gated) * upward).astype(BF))
    hidden = jnp.concatenate(hidden, axis=1)
    pbufs = (pa, pb, pc)

    def narrowing(k, carry):
        cols = pl.ds(pl.multiple_of(k * 256, 256), 256)
        rhs = jnp.concatenate([narrow[0, :, cols], narrow[1, :, cols]], axis=0)
        term = jnp.dot(hidden, rhs, preferred_element_type=F32).astype(BF)
        v = jnp.concatenate(
            [term[:, 0:128].reshape(4, 4, 16, 128), term[:, 128:256].reshape(4, 4, 16, 128)], axis=1
        )
        zz, yy = k // 4, k % 4
        pa[zz, yy] = v[:, 0:3]
        pb[:, zz, yy] = v[:, 3:6]
        pc[yy, :, zz] = v[:, 6:8]
        return carry

    lax.fori_loop(0, 16, narrowing, 0)
    for n, phase in enumerate((2, 1, 0)):
        r = receive[12 * n : 12 * n + 12]
        sums = reduce_phase(
            at, pbufs, ORDERS, phase, r[0:3], r[3:6], r[6:9], r[9:12], sems, 85 + 18 * n, phase > 0
        )
    sums = jnp.concatenate(sums, axis=0)
    mixed = []
    for h in range(2):
        for i in range(4):
            res = residual_ref[16 * i : 16 * i + 16, 128 * h : 128 * h + 128]
            mixed.append((res + sums[4 * h + i]).astype(BF))
    for t in range(8):
        h, lane = t // 4, 32 * (t % 4)
        ypack[t] = jnp.concatenate(
            [mixed[4 * h + i][:, lane : lane + 32] for i in range(4)], axis=1
        )
    copies = []
    for i, (dx, dc) in enumerate(lines):
        peer = line_peer(at, dx, dc)
        copies.append(
            send(ypack.at[2 * peer[2] + peer[3]], yarrive.at[tp], sems, 139 + i, peer)
        )
    yarrive[pl.ds(tp, 1)] = ypack[pl.ds(tp, 1)]
    for copy in copies:
        copy.wait()
    out_ref[...] = yarrive[...]


def mixer(normed, packed, x, result, gain, gate, wide, narrow):
    vmem = pl.BlockSpec(memory_space=pltpu.VMEM)
    counts = [count for _, count in PARTS]
    boxes = [pltpu.VMEM((4, 4, 4, count, 16, 128), BF) for count in counts]
    receive = []
    for phase in (2, 1, 0):
        lead = (4,) * phase
        shapes = [(*lead, count, 16, 128) for count in counts]
        low = [pltpu.VMEM((s[0] // 2, *s[1:]), BF) for s in shapes]
        high = [pltpu.VMEM((s[0] - s[0] // 2, *s[1:]), BF) for s in shapes]
        full = [pltpu.VMEM(s, BF) for s in shapes]
        receive += low + high + full + full
    return pl.pallas_call(
        mixer_kernel,
        out_shape=jax.ShapeDtypeStruct((8, 16, 128), BF),
        in_specs=[vmem] * 8,
        out_specs=vmem,
        scratch_shapes=[
            pltpu.VMEM((16, 64, 256), BF),
            pltpu.VMEM((8, 64, 256), BF),
            pltpu.VMEM((7, 64, 256), BF),
            pltpu.VMEM((8, 128), F32),
            pltpu.VMEM((8, 8, 128), F32),
            pltpu.VMEM((64, 256), F32),
            pltpu.VMEM((16, 8, 128), F32),
            pltpu.VMEM((8, 128), F32),
            pltpu.VMEM((4, 8, 128), F32),
            pltpu.VMEM((2, 2, 128, 4096), BF),
            pltpu.VMEM((2, 128, 4096), BF),
            pltpu.VMEM((2, 256, 256), F32),
            *boxes,
            *boxes,
            *receive,
            pltpu.VMEM((8, 16, 128), BF),
            pltpu.VMEM((8, 16, 128), BF),
            pltpu.SemaphoreType.DMA((146,)),
            pltpu.SemaphoreType.DMA((146,)),
        ],
        compiler_params=pltpu.CompilerParams(
            collective_id=0, has_side_effects=True, vmem_limit_bytes=48 * 1024 * 1024
        ),
        name="mixer",
    )(normed, packed, x, result, gain, gate, wide, narrow)


def spread_kernel(packed_ref, mixed_ref, out_ref):
    place = packed_ref[0:1, :]
    total = jnp.zeros((32, 1024), F32)
    j = lax.broadcasted_iota(jnp.int32, (128, 1024), 0)
    rows = 64 * (j // 16) + j % 16
    for a in range(4):
        chosen = jnp.where(rows + 16 * a == place, 1.0, 0.0).astype(BF)
        piece = mixed_ref[...].reshape(128, 128)[:, 32 * a : 32 * a + 32]
        total = total + times(piece, chosen, ((0,), (0,)))
    out_ref[...] = total.astype(BF)


def spread(packed, mixed):
    vmem = pl.BlockSpec(memory_space=pltpu.VMEM)
    return pl.pallas_call(
        spread_kernel,
        out_shape=jax.ShapeDtypeStruct((32, 1024), BF),
        in_specs=[vmem] * 2,
        out_specs=vmem,
        name="spread",
    )(packed, mixed)


def front_kernel(
    x_ref, lengths_ref, gain_ref, wq_ref, wf_ref, wi_ref, wo_ref,
    z_ref, xt_ref, packed_ref,
    cols, scaled, squares, squares_in, pa, pb, *rest,
):
    receive, (sends, recvs) = rest[:16], rest[16:]
    sems = (sends, recvs)
    at = my_position()
    kv = 4 * at["z"] + at["y"]
    tp = 2 * at["x"] + at["c"]
    planes, lines = plane_offsets(), line_offsets()
    meet([plane_peer(at, *d) for d in planes] + [line_peer(at, *d) for d in lines])
    copies = [
        send(x_ref, cols.at[tp], sems, i, line_peer(at, *d)) for i, d in enumerate(lines)
    ]
    cols[pl.ds(tp, 1)] = x_ref[...][None]
    lengths = jnp.broadcast_to(lengths_ref[...], (8, 128)).astype(F32).astype(BF)
    s = lax.broadcasted_iota(jnp.int32, (128, 1024), 0)
    owner = lax.broadcasted_iota(jnp.int32, (128, 1024), 1) // 8
    start = times(lengths, jnp.where(s < owner, 1.0, 0.0).astype(BF), ((1,), (0,)))
    length = times(lengths, jnp.where(s == owner, 1.0, 0.0).astype(BF), ((1,), (0,)))
    slot = lax.broadcasted_iota(jnp.int32, (8, 1024), 1) % 8
    place = jnp.where(
        slot < length.astype(jnp.int32), start.astype(jnp.int32) + slot, -1
    )
    packed_ref[...] = place
    gain = jnp.concatenate(
        [column_of(gain_ref[:, 0:128], 128), column_of(gain_ref[:, 128:256], 128)], axis=0
    )
    mine = picks(place[0:1, :], 64 * tp, 64)
    for copy in copies:
        copy.wait()
    xt_ref[...] = times(mine, cols[...].reshape(256, 1024)).astype(BF)
    for k in range(8):
        lanes = slice(128 * k, 128 * k + 128)
        v = cols[:, :, lanes].reshape(256, 128).astype(F32)
        scaled[:, lanes] = (v * gain).astype(BF)
        squares[k] = jnp.broadcast_to(jnp.sum(v * v, axis=0, keepdims=True), (8, 128))
    square_copies = []
    for i, (dz, dy) in enumerate(planes):
        peer = plane_peer(at, dz, dy)
        square_copies.append(
            send(squares.at[(4 * peer[0] + peer[1]) // 2], squares_in.at[i], sems, 7 + i, peer)
        )

    def project(a, carry):
        lhs = scaled[:, pl.ds(pl.multiple_of(256 * a, 256), 256)]
        for n, (first, second) in enumerate(((wq_ref, wf_ref), (wi_ref, wo_ref))):
            for half, weight in enumerate((first, second)):
                lanes = slice(256 * half, 256 * half + 256)
                v = times(lhs, weight[...], ((0,), (0,))).astype(BF).reshape(4, 64, 256)
                if n == 0:
                    pa[:, a, :, lanes] = v
                else:
                    pb[a, :, :, lanes] = v
        return carry

    lax.fori_loop(0, 4, project, 0)
    bufs = (pa, pb)
    r = receive
    reduce_phase(at, bufs, PLANE_ORDERS, 1, r[0:2], r[2:4], r[4:6], r[6:8], sems, 22)
    r = receive[8:]
    sums = reduce_phase(
        at, bufs, PLANE_ORDERS, 0, r[0:2], r[2:4], r[4:6], r[6:8], sems, 34, False
    )
    for copy in square_copies:
        copy.wait()
    total = jnp.sum(squares_in[...], axis=0) + squares[kv // 2]
    shift = 64 * (kv % 2)
    eye = lax.broadcasted_iota(jnp.int32, (64, 128), 1) == shift + lax.broadcasted_iota(
        jnp.int32, (64, 128), 0
    )
    own = jnp.sum(jnp.where(eye, total[0:1, :], 0.0), axis=1, keepdims=True)
    scale = lax.rsqrt(own / 4096 + EPS)
    z_ref[:, 0:512] = sums[0] * scale
    z_ref[:, 512:1024] = sums[1] * scale


def front(x, lengths, gain, wq, wf, wi, wo):
    vmem = pl.BlockSpec(memory_space=pltpu.VMEM)
    receive = []
    for phase in (1, 0):
        shape = (*(4,) * phase, 64, 512)
        half = pltpu.VMEM((shape[0] // 2, *shape[1:]), BF)
        receive += [half] * 4 + [pltpu.VMEM(shape, BF)] * 4
    return pl.pallas_call(
        front_kernel,
        out_shape=(
            jax.ShapeDtypeStruct((64, 1024), F32),
            jax.ShapeDtypeStruct((64, 256), BF),
            jax.ShapeDtypeStruct((8, 1024), jnp.int32),
        ),
        in_specs=[vmem] * 7,
        out_specs=(vmem,) * 3,
        scratch_shapes=[
            pltpu.VMEM((8, 32, 1024), BF),
            pltpu.VMEM((256, 1024), BF),
            pltpu.VMEM((8, 8, 128), F32),
            pltpu.VMEM((15, 8, 128), F32),
            pltpu.VMEM((4, 4, 64, 512), BF),
            pltpu.VMEM((4, 4, 64, 512), BF),
            *receive,
            pltpu.SemaphoreType.DMA((46,)),
            pltpu.SemaphoreType.DMA((46,)),
        ],
        compiler_params=pltpu.CompilerParams(
            collective_id=1, has_side_effects=True, vmem_limit_bytes=32 * 1024 * 1024
        ),
        name="front",
    )(x, lengths, gain, wq, wf, wi, wo)


def recurrence_kernel(
    z_ref, bound_ref, shrink_ref, lengths_ref, lane_gain_ref, state_ref,
    normed_ref, new_ref,
    decay, gate, query, output,
):
    step = pl.program_id(0)
    kv = 4 * lax.axis_index("kv_0") + lax.axis_index("kv_1")
    row = lax.broadcasted_iota(jnp.int32, (64, 128), 0)
    lane = lax.broadcasted_iota(jnp.int32, (64, 128), 1)
    length = jnp.sum(
        jnp.where(lane == 8 * kv + row // 8, lengths_ref[...].astype(F32), 0.0),
        axis=1,
        keepdims=True,
    )
    live = (row[:, 0:1] % 8).astype(F32) < length

    @pl.when(step == 0)
    def _():
        bound = bound_ref[...]
        retain = bound + (1.0 - bound) * jax.nn.sigmoid(z_ref[:, 256:512])
        for h in range(2):
            lanes = slice(128 * h, 128 * h + 128)
            shrink = jnp.sum(
                jnp.where(lane[:, 0:64] == row[:, 0:64], shrink_ref[h : h + 1, :], 0.0),
                axis=1,
                keepdims=True,
            )
            kept = jnp.exp(jnp.log(retain[:, lanes]) + shrink)
            decay[:, lanes] = jnp.where(live, kept, 1.0)
            gate[:, lanes] = jnp.where(live, 1.0 - retain[:, lanes], 0.0)
        zq = z_ref[:, 0:256]
        query[...] = zq * jax.nn.sigmoid(zq)

    rows = pl.ds(pl.multiple_of(8 * step, 8), 8)
    for h in range(2):
        lanes = slice(128 * h, 128 * h + 128)
        d, k, q = decay[rows, lanes].T, gate[rows, lanes].T, query[rows, lanes].T
        value = z_ref[rows, 512 + 128 * h : 640 + 128 * h]
        state = state_ref[0, h]
        outs = []
        for j in range(8):
            state = d[:, j : j + 1] * state + k[:, j : j + 1] * value[j : j + 1, :]
            outs.append(jnp.sum(q[:, j : j + 1] * state, axis=0, keepdims=True))
        new_ref[0, h] = state
        output[rows, lanes] = jnp.concatenate(outs, axis=0)

    @pl.when(step == 7)
    def _():
        for h in range(2):
            lanes = slice(128 * h, 128 * h + 128)
            o = output[:, lanes]
            zo = z_ref[:, 768 + 128 * h : 896 + 128 * h]
            o = o * lax.rsqrt(jnp.mean(o * o, axis=1, keepdims=True) + EPS) * lane_gain_ref[...]
            normed_ref[:, lanes] = jnp.where(live, o * (zo * jax.nn.sigmoid(zo)), 0.0).astype(BF)


def recurrence(z, bound, shrink, lengths, lane_gain, state):
    def whole(*shape):
        return pl.BlockSpec(shape, lambda s: (0,) * len(shape))

    one = pl.BlockSpec((1, 2, 128, 128), lambda s: (s, 0, 0, 0))
    return pl.pallas_call(
        recurrence_kernel,
        out_shape=(
            jax.ShapeDtypeStruct((64, 256), BF),
            jax.ShapeDtypeStruct((8, 2, 128, 128), F32),
        ),
        grid=(8,),
        in_specs=[whole(64, 1024), whole(1, 256), whole(2, 64), whole(1, 128), whole(1, 128), one],
        out_specs=(whole(64, 256), one),
        scratch_shapes=[pltpu.VMEM((64, 256), F32)] * 4,
        name="recurrence",
    )(z, bound, shrink, lengths, lane_gain, state)


def local(
    residual_entries,
    fresh_extents,
    memory_matrix,
    initial_rescale_vector,
    probe_matrix,
    retain_matrix,
    content_matrix,
    result_switch_matrix,
    retain_lower_limit,
    extra_shrink_log,
    lane_result_rescale,
    result_matrix,
    later_rescale_vector,
    mixer_switch_matrix,
    widening_matrix,
    narrowing_matrix,
):
    lengths = fresh_extents.reshape(1, 128)
    z, xt, packed = front(
        residual_entries.T,
        lengths,
        initial_rescale_vector.reshape(1, 256),
        probe_matrix,
        retain_matrix,
        content_matrix,
        result_switch_matrix,
    )
    normed, carried = recurrence(
        z,
        retain_lower_limit.reshape(1, 256),
        extra_shrink_log.T,
        lengths,
        lane_result_rescale.reshape(1, 128),
        memory_matrix,
    )
    mixed = mixer(
        normed,
        packed,
        xt,
        result_matrix,
        later_rescale_vector.reshape(1, 32),
        mixer_switch_matrix.T,
        widening_matrix.T,
        narrowing_matrix,
    )
    return (spread(packed, mixed).T, carried)


def solution(mesh):
    torus = Mesh(mesh.devices.reshape(4, 4, 4, 2), ("kv_0", "kv_1", "tp_0", "tp_1"))
    placed = (
        P(None, KV_TP),
        P(),
        P(KV, TP, None, None),
        P(KV),
        P(KV, TP),
        P(KV, TP),
        P(KV, TP),
        P(KV, TP),
        P(TP),
        P(KV, TP),
        P(),
        P(TP, KV),
        P(KV_TP),
        P(None, KV_TP),
        P(None, KV_TP),
        P(KV_TP, None),
    )
    return jax.shard_map(
        local,
        mesh=torus,
        in_specs=placed,
        out_specs=(P(None, KV_TP), P(KV, TP, None, None)),
        check_vma=False,
    )
```

time: 221 us -> 143 us (0.65)
  Pallas kernels: 87.4 us -> 133 us
  waiting for transfers between devices: 40.4 us -> 0 us
  matrix products: 33.5 us -> 0 us
  blocking collectives: 15 us -> 0 us
  between operations: 14.4 us -> 0.72 us
  other arithmetic: 9.85 us -> 0 us
  local copies, waits for them, and re-layouts: 14.3 us -> 8.91 us
  starting transfers between devices: 5.09 us -> 0 us
    pallas_call x1 -> x3, Pallas kernels: 2.03 us -> 48.5 us  [the longest x1 35.1 us: front(): pl.pallas_call(front_kernel, out_shape=(jax.ShapeDtypeStruct((64, 1024),...]
    reduce_scatter x2 -> x0, waiting for transfers between devices: 39 us -> none  [own_rows(): total = lax.psum_scatter(total, axis, scatter_dimension=0, tiled=True)]
    dot_general x12 -> x0, matrix products: 33.5 us -> none  [the longest x8 32.1 us: local(): jnp.einsum('bhd,bhdv->bhv', query[:, position], carried, precision=lax.Pr...]
    all_to_all x1 -> x0, blocking collectives: 15 us -> none  [copy_for_each(): lax.all_to_all(jnp.broadcast_to(x[None], (devices, *x.shape)), axis, 0, 0...]
    all_to_all x1 -> x0, starting transfers between devices: 5.01 us -> none  [sum_at_owner(): pieces = lax.all_to_all(split_up(x, dim, devices), axis, 0, 0, tiled=True)]
    add x1 -> x0, other arithmetic: 4.68 us -> none  [local(): decays[:, position, :, :, None] * carried]
    broadcast_in_dim x3 -> x0, local copies, waits for them, and re-layouts: 2.26 us -> none  [the longest x1 0.95 us: copy_for_each(): jnp.broadcast_to(x[None], (devices, *x.shape))]
    unnamed x37 -> x32, local copies, waits for them, and re-layouts: 7.62 us -> 8.91 us
  transfers between devices with their start and end apart: 3 -> 0, of which waited for: 3 -> 0; matrix products, arithmetic and copies ran while one was open for 2% -> 0% of each run, Pallas kernels for 0% -> 0%
where the time goes in v2:
time: 143 us
  Pallas kernels  133 us (93%)
  local copies, waits for them, and re-layouts  8.91 us (6%)
    pallas_call x1, Pallas kernels, mixer(): pl.pallas_call(mixer_kernel, out_shape=jax.ShapeDtypeStruct((8, 16, 128),...  84.5 us
    pallas_call x1, Pallas kernels, front(): pl.pallas_call(front_kernel, out_shape=(jax.ShapeDtypeStruct((64, 1024),...  35.1 us
    pallas_call x1, Pallas kernels, recurrence(): pl.pallas_call(recurrence_kernel, out_shape=(jax.ShapeDtypeStruct((64, 25...  11.6 us
    unnamed x32, local copies, waits for them, and re-layouts  8.91 us

profile of v2, /device:TPU:1, one launch (start us, length us, event | category | flops | bytes accessed | tf_op | source)
XLA Modules:
  0.0 142.6 jit_solution(524428172213032009)
XLA Ops:
  0.6 0.0 copy-start.13
  0.6 0.0 copy-start.14
  0.7 0.6 copy-done.13
  1.3 0.0 copy-done.14
  1.3 0.0 copy-start.6
  1.3 0.9 copy-done.6
  2.2 0.0 copy-start.7
  2.2 0.9 copy-done.7
  3.1 0.0 copy-start.8
  3.1 0.9 copy-done.8
  4.0 0.0 copy-start.9
  4.0 0.9 copy-done.9
  4.9 0.0 copy-start.11
  5.0 0.8 copy-done.11
  5.8 0.0 copy-start.1
  5.8 35.1 %front.1 = (f32[64,1024]{1,0:T(8,128)S(1)}, bf16[64,256]{1,0:T(8,128)(2,1)S(1)}, s32[8,1024]{1,0:T(8,128)S(1)}) custom-call(bf16[32,1024]{1,0:T(8,128)(2,1)S(1)} %bitcast.12, s32[1,128]{1,0:T(1,128)S(1)} %bitcast.14, f32[1,256]{1,0:T(1,128)S(1)} %bitcast.15, bf16[256,256]{1,0:T(8,128)(2,1)S(1)} %copy-done.6, bf16[256,256]{1,0:T(8,128)(2,1)S(1)} %copy-done.7, ...), custom_call_target="tpu_custom_call" | custom-call | tf_op jit(solution)/shard_map/front/pallas_call | solution.py:520
  40.9 0.0 copy-start.3
  41.0 0.7 copy-done.3
  41.6 0.0 copy-start.4
  41.6 0.0 copy-start
  41.6 0.0 copy-start.10
  41.6 11.6 %recurrence.1 = (bf16[64,256]{1,0:T(8,128)(2,1)}, f32[8,2,128,128]{3,2,1,0:T(8,128)}) custom-call(f32[64,1024]{1,0:T(8,128)} %copy-done.3, f32[1,256]{1,0:T(1,128)} %bitcast.18, f32[2,64]{1,0:T(2,128)} %bitcast.19, s32[1,128]{1,0:T(1,128)} %bitcast.13, f32[1,128]{1,0:T(1,128)} %bitcast.20, f32[8,2,128,128]{3,2,1,0:T(8,128)} %state_ref.1), custom_call_target="tpu_custom_call" | custom-call | tf_op jit(solution)/shard_map/recurrence/pallas_call | solution.py:608
  53.2 0.0 copy-start.15
  53.2 0.0 copy-done.4
  53.2 0.0 copy-done.1
  53.2 0.0 copy-done
  53.3 0.0 copy-done.10
  53.3 0.6 copy-done.15
  53.9 0.0 copy-start.2
  53.9 1.1 copy-done.2
  55.0 0.0 copy-start.12
  55.0 0.8 copy-done.12
  55.8 84.5 %mixer.1.mixed_ref = bf16[8,16,128]{2,1,0:T(8,128)(2,1)S(1)} custom-call(bf16[64,256]{1,0:T(8,128)(2,1)S(1)} %copy-done.12, s32[8,1024]{1,0:T(8,128)S(1)} %get-tuple-element.7.packed_ref, bf16[64,256]{1,0:T(8,128)(2,1)S(1)} %get-tuple-element.10.x_ref, bf16[256,256]{1,0:T(8,128)(2,1)S(1)} %copy-done.10, f32[1,32]{1,0:T(1,128)S(1)} %bitcast.16, ...), custom_call_target="tpu_custom_call" | custom-call | tf_op jit(solution)/shard_map/mixer/pallas_call | solution.py:379
  140.2 0.0 copy-start.5
  140.2 0.6 copy-done.5
  140.8 1.8 %spread.1 = bf16[32,1024]{1,0:T(8,128)(2,1)} custom-call(s32[8,1024]{1,0:T(8,128)} %copy-done.4, bf16[8,16,128]{2,1,0:T(8,128)(2,1)} %copy-done.5), custom_call_target="tpu_custom_call" | custom-call | tf_op jit(solution)/shard_map/spread/pallas_call | solution.py:426
Async XLA Ops:
  0.6 0.7 copy-start.13
  0.6 0.7 copy-start.14
  1.3 0.9 copy-start.6
  2.2 0.9 copy-start.7
  3.1 0.9 copy-start.8
  4.0 0.9 copy-start.9
  4.9 0.8 copy-start.11
  5.8 47.4 %copy-start.1 = (bf16[4096,86]{0,1:T(8,128)(2,1)S(1)}, bf16[4096,86]{0,1:T(8,128)(2,1)}, u32[]{:S(2)}) copy-start(bf16[4096,86]{0,1:T(8,128)(2,1)} %param.30) | copy-start | bytes 2113540
  40.9 0.7 copy-start.3
  41.6 11.6 %copy-start.4 = (s32[8,1024]{1,0:T(8,128)}, s32[8,1024]{1,0:T(8,128)S(1)}, u32[]{:S(2)}) copy-start(s32[8,1024]{1,0:T(8,128)S(1)} %get-tuple-element.7.packed_ref) | copy-start | bytes 98308
  41.6 11.6 %copy-start = (bf16[4096,86]{0,1:T(8,128)(2,1)S(1)}, bf16[4096,86]{0,1:T(8,128)(2,1)}, u32[]{:S(2)}) copy-start(bf16[4096,86]{0,1:T(8,128)(2,1)} %param.29) | copy-start | bytes 2113540
  41.6 11.6 %copy-start.10 = (bf16[256,256]{1,0:T(8,128)(2,1)S(1)}, bf16[256,256]{1,0:T(8,128)(2,1)}, u32[]{:S(2)}) copy-start(bf16[256,256]{1,0:T(8,128)(2,1)} %result_ref.1) | copy-start | bytes 393220
  53.2 0.7 copy-start.15
  53.9 1.1 copy-start.2
  55.0 0.8 copy-start.12
  140.2 0.6 copy-start.5

commit v3 on v2

--- a/solution.py
+++ b/solution.py
@@ -196,12 +196,25 @@
 ):
     (pa, pb, pc), rest = rest[:3], rest[3:]
     receive, rest = rest[:36], rest[36:]
-    ypack, yarrive, sends, recvs = rest
+    ypack, yarrive, result, staged, sends, recvs, local = rest
     sems = (sends, recvs)
     at = my_position()
     kv = 4 * at["z"] + at["y"]
     tp = 2 * at["x"] + at["c"]
     planes, lines = plane_offsets(), line_offsets()
+    for slot, start in ((0, 80), (1, 96)):
+        weights[slot, :, start:128] = jnp.zeros((2, 128 - start, 4096), BF)
+        narrow[slot, start:128] = jnp.zeros((128 - start, 4096), BF)
+    local_copies = []
+    for n, (src, dst) in enumerate((
+        (gate_ref, staged.at[0]),
+        (wide_ref, staged.at[1]),
+        (narrow_ref, staged.at[2]),
+        (result_ref, result),
+    )):
+        copy = pltpu.make_async_copy(src, dst, local.at[n])
+        copy.start()
+        local_copies.append(copy)
     meet([plane_peer(at, *d) for d in planes] + [line_peer(at, *d) for d in lines])
 
     copies = [
@@ -214,12 +227,10 @@
         send(own_gain, gains.at[tp], sems, 15 + i, line_peer(at, *d)) for i, d in enumerate(lines)
     ]
     partner = line_peer(at, 0, 1)
-    for slot, start in ((0, 80), (1, 96)):
-        weights[slot, :, start:128] = jnp.zeros((2, 128 - start, 4096), BF)
-        narrow[slot, start:128] = jnp.zeros((128 - start, 4096), BF)
-    weights[0, 0, 0:86] = gate_ref[...]
-    weights[0, 1, 0:86] = wide_ref[...]
-    narrow[0, 0:86] = narrow_ref[...]
+    for copy in local_copies:
+        copy.wait()
+    weights[0, :, 0:86] = staged[0:2]
+    narrow[0, 0:86] = staged[2]
     weight_copy = send(weights.at[0, :, 0:96], weights.at[1, :, 0:96], sems, 22, partner)
     narrow_copy = send(narrow.at[0, 0:96], narrow.at[1, 0:96], sems, 23, partner)
     heads[pl.ds(kv, 1)] = normed_ref[...][None]
@@ -236,7 +247,7 @@
     for part in range(2):
         live = jnp.dot(chosen(256 * part, 256), all_heads, preferred_element_type=F32).astype(BF)
         partial[4 * part : 4 * part + 4] = (
-            jnp.dot(live, result_ref[...], preferred_element_type=F32)
+            jnp.dot(live, result[...], preferred_element_type=F32)
             .astype(BF)
             .reshape(4, 64, 256)
         )
@@ -292,23 +303,16 @@
             [v[:, 0:4].reshape(256, 128), v[:, 4:8].reshape(256, 128)], axis=1
         )
 
-    def widening(k, carry):
-        lhs = rows_at(k // 4, k % 4)
-        cols = pl.ds(pl.multiple_of(k * 256, 256), 256)
+    total[...] = jnp.zeros_like(total)
+
+    def widening(zz, carry):
+        lhs = jnp.concatenate([rows_at(zz, yy) for yy in range(4)], axis=1)
+        cols = pl.ds(pl.multiple_of(zz * 1024, 1024), 1024)
         for core in range(2):
-            term = times(lhs, weights[core, :, :, cols].reshape(256, 256))
-
-            @pl.when(k == 0)
-            def _():
-                total[core] = term
-
-            @pl.when(k > 0)
-            def _():
-                total[core] += term
-
+            total[core] += times(lhs, weights[core, :, :, cols].reshape(256, 1024))
         return carry
 
-    lax.fori_loop(0, 16, widening, 0)
+    lax.fori_loop(0, 4, widening, 0)
     scale = lax.rsqrt(
         jnp.concatenate([column_of(squares_line[g, 0:1, :], 64) for g in range(4)], axis=0)
         / 4096
@@ -366,6 +370,7 @@
 
 def mixer(normed, packed, x, result, gain, gate, wide, narrow):
     vmem = pl.BlockSpec(memory_space=pltpu.VMEM)
+    far = pl.BlockSpec(memory_space=pltpu.HBM)
     counts = [count for _, count in PARTS]
     boxes = [pltpu.VMEM((4, 4, 4, count, 16, 128), BF) for count in counts]
     receive = []
@@ -379,7 +384,7 @@
     return pl.pallas_call(
         mixer_kernel,
         out_shape=jax.ShapeDtypeStruct((8, 16, 128), BF),
-        in_specs=[vmem] * 8,
+        in_specs=[vmem, vmem, vmem, far, vmem, far, far, far],
         out_specs=vmem,
         scratch_shapes=[
             pltpu.VMEM((16, 64, 256), BF),
@@ -399,11 +404,14 @@
             *receive,
             pltpu.VMEM((8, 16, 128), BF),
             pltpu.VMEM((8, 16, 128), BF),
+            pltpu.VMEM((256, 256), BF),
+            pltpu.VMEM((3, 86, 4096), BF),
             pltpu.SemaphoreType.DMA((146,)),
             pltpu.SemaphoreType.DMA((146,)),
+            pltpu.SemaphoreType.DMA((4,)),
         ],
         compiler_params=pltpu.CompilerParams(
-            collective_id=0, has_side_effects=True, vmem_limit_bytes=48 * 1024 * 1024
+            collective_id=0, has_side_effects=True, vmem_limit_bytes=67043328
         ),
         name="mixer",
     )(normed, packed, x, result, gain, gate, wide, narrow)
@@ -435,19 +443,26 @@
 def front_kernel(
     x_ref, lengths_ref, gain_ref, wq_ref, wf_ref, wi_ref, wo_ref,
     z_ref, xt_ref, packed_ref,
-    cols, scaled, squares, squares_in, pa, pb, *rest,
+    cols, scaled, squares, squares_in, pa, pb, weights, *rest,
 ):
-    receive, (sends, recvs) = rest[:16], rest[16:]
+    receive, (sends, recvs, local) = rest[:16], rest[16:]
     sems = (sends, recvs)
     at = my_position()
     kv = 4 * at["z"] + at["y"]
     tp = 2 * at["x"] + at["c"]
     planes, lines = plane_offsets(), line_offsets()
+    own_copy = pltpu.make_async_copy(x_ref, cols.at[tp], local.at[0])
+    own_copy.start()
+    weight_copies = []
+    for n, ref in enumerate((wq_ref, wf_ref, wi_ref, wo_ref)):
+        copy = pltpu.make_async_copy(ref, weights.at[n], local.at[1 + n])
+        copy.start()
+        weight_copies.append(copy)
     meet([plane_peer(at, *d) for d in planes] + [line_peer(at, *d) for d in lines])
+    own_copy.wait()
     copies = [
-        send(x_ref, cols.at[tp], sems, i, line_peer(at, *d)) for i, d in enumerate(lines)
+        send(cols.at[tp], cols.at[tp], sems, i, line_peer(at, *d)) for i, d in enumerate(lines)
     ]
-    cols[pl.ds(tp, 1)] = x_ref[...][None]
     lengths = jnp.broadcast_to(lengths_ref[...], (8, 128)).astype(F32).astype(BF)
     s = lax.broadcasted_iota(jnp.int32, (128, 1024), 0)
     owner = lax.broadcasted_iota(jnp.int32, (128, 1024), 1) // 8
@@ -479,16 +494,18 @@
 
     def project(a, carry):
         lhs = scaled[:, pl.ds(pl.multiple_of(256 * a, 256), 256)]
-        for n, (first, second) in enumerate(((wq_ref, wf_ref), (wi_ref, wo_ref))):
-            for half, weight in enumerate((first, second)):
+        for n in range(2):
+            for half in range(2):
                 lanes = slice(256 * half, 256 * half + 256)
-                v = times(lhs, weight[...], ((0,), (0,))).astype(BF).reshape(4, 64, 256)
+                v = times(lhs, weights[2 * n + half], ((0,), (0,))).astype(BF).reshape(4, 64, 256)
                 if n == 0:
                     pa[:, a, :, lanes] = v
                 else:
                     pb[a, :, :, lanes] = v
         return carry
 
+    for copy in weight_copies:
+        copy.wait()
     lax.fori_loop(0, 4, project, 0)
     bufs = (pa, pb)
     r = receive
@@ -512,6 +529,7 @@
 
 def front(x, lengths, gain, wq, wf, wi, wo):
     vmem = pl.BlockSpec(memory_space=pltpu.VMEM)
+    far = pl.BlockSpec(memory_space=pltpu.HBM)
     receive = []
     for phase in (1, 0):
         shape = (*(4,) * phase, 64, 512)
@@ -524,7 +542,7 @@
             jax.ShapeDtypeStruct((64, 256), BF),
             jax.ShapeDtypeStruct((8, 1024), jnp.int32),
         ),
-        in_specs=[vmem] * 7,
+        in_specs=[far, vmem, vmem, far, far, far, far],
         out_specs=(vmem,) * 3,
         scratch_shapes=[
             pltpu.VMEM((8, 32, 1024), BF),
@@ -533,23 +551,29 @@
             pltpu.VMEM((15, 8, 128), F32),
             pltpu.VMEM((4, 4, 64, 512), BF),
             pltpu.VMEM((4, 4, 64, 512), BF),
+            pltpu.VMEM((4, 256, 256), BF),
             *receive,
             pltpu.SemaphoreType.DMA((46,)),
             pltpu.SemaphoreType.DMA((46,)),
+            pltpu.SemaphoreType.DMA((5,)),
         ],
         compiler_params=pltpu.CompilerParams(
-            collective_id=1, has_side_effects=True, vmem_limit_bytes=32 * 1024 * 1024
+            collective_id=1, has_side_effects=True, vmem_limit_bytes=67043328
         ),
         name="front",
     )(x, lengths, gain, wq, wf, wi, wo)
 
 
+def split(v):
+    high = v.astype(BF)
+    return high, (v - high.astype(F32)).astype(BF)
+
+
 def recurrence_kernel(
     z_ref, bound_ref, shrink_ref, lengths_ref, lane_gain_ref, state_ref,
     normed_ref, new_ref,
-    decay, gate, query, output,
+    query, kept, gate, output,
 ):
-    step = pl.program_id(0)
     kv = 4 * lax.axis_index("kv_0") + lax.axis_index("kv_1")
     row = lax.broadcasted_iota(jnp.int32, (64, 128), 0)
     lane = lax.broadcasted_iota(jnp.int32, (64, 128), 1)
@@ -559,61 +583,81 @@
         keepdims=True,
     )
     live = (row[:, 0:1] % 8).astype(F32) < length
-
-    @pl.when(step == 0)
-    def _():
-        bound = bound_ref[...]
-        retain = bound + (1.0 - bound) * jax.nn.sigmoid(z_ref[:, 256:512])
+    slot = lax.broadcasted_iota(jnp.int32, (8, 8, 128), 1)
+    for h in range(2):
+        lanes = slice(128 * h, 128 * h + 128)
+        bound = bound_ref[:, lanes]
+        retain = bound + (1.0 - bound) * jax.nn.sigmoid(z_ref[:, 256 + 128 * h : 384 + 128 * h])
+        shrink = jnp.sum(
+            jnp.where(lane[:, 0:64] == row[:, 0:64], shrink_ref[h : h + 1, :], 0.0),
+            axis=1,
+            keepdims=True,
+        )
+        decay = jnp.where(live, jnp.exp(jnp.log(retain) + shrink), 1.0).reshape(8, 8, 128)
+        key = jnp.where(live, 1.0 - retain, 0.0).reshape(8, 8, 128)
+        zq = z_ref[:, lanes]
+        q = (zq * jax.nn.sigmoid(zq)).reshape(8, 8, 128)
+        value = z_ref[:, 512 + 128 * h : 640 + 128 * h].reshape(8, 8, 128)
+        between = q
+        out = jnp.sum(q * key, axis=2, keepdims=True) * value
+        for back in range(1, 8):
+            between = between * (decay if back == 1 else pltpu.roll(decay, back - 1, 1))
+            weight = jnp.sum(between * pltpu.roll(key, back, 1), axis=2, keepdims=True)
+            out = out + jnp.where(slot >= back, weight * pltpu.roll(value, back, 1), 0.0)
+        output[:, lanes] = out.reshape(64, 128)
+        before, after = decay, jnp.where(slot < 7, pltpu.roll(decay, 7, 1), 1.0)
+        for step in (1, 2, 4):
+            before = before * jnp.where(slot >= step, pltpu.roll(before, step, 1), 1.0)
+            after = after * jnp.where(slot + step < 8, pltpu.roll(after, 8 - step, 1), 1.0)
+        query[:, lanes] = (q * before).reshape(64, 128)
+        kept[:, lanes] = before.reshape(64, 128)
+        gate[:, lanes] = (key * after).reshape(64, 128)
+
+    def sequence(n, carry):
+        rows = pl.ds(pl.multiple_of(8 * n, 8), 8)
         for h in range(2):
             lanes = slice(128 * h, 128 * h + 128)
-            shrink = jnp.sum(
-                jnp.where(lane[:, 0:64] == row[:, 0:64], shrink_ref[h : h + 1, :], 0.0),
-                axis=1,
-                keepdims=True,
+            state = state_ref[n, h]
+            s_high, s_low = split(state)
+            q_high, q_low = split(query[rows, lanes])
+            lhs = jnp.concatenate(
+                [
+                    jnp.concatenate([q_high, q_high], axis=1),
+                    jnp.concatenate([q_low, jnp.zeros_like(q_low)], axis=1),
+                ],
+                axis=0,
             )
-            kept = jnp.exp(jnp.log(retain[:, lanes]) + shrink)
-            decay[:, lanes] = jnp.where(live, kept, 1.0)
-            gate[:, lanes] = jnp.where(live, 1.0 - retain[:, lanes], 0.0)
-        zq = z_ref[:, 0:256]
-        query[...] = zq * jax.nn.sigmoid(zq)
-
-    rows = pl.ds(pl.multiple_of(8 * step, 8), 8)
+            o = times(lhs, jnp.concatenate([s_high, s_low], axis=0), ((1,), (0,)))
+            output[rows, lanes] += o[0:8] + o[8:16]
+            k_high, k_low = split(gate[rows, lanes])
+            v_high, v_low = split(z_ref[rows, 512 + 128 * h : 640 + 128 * h])
+            added = times(
+                jnp.concatenate([k_high, k_high, k_low], axis=0),
+                jnp.concatenate([v_high, v_low, v_high], axis=0),
+                ((0,), (0,)),
+            )
+            new_ref[n, h] = column_of(kept[rows, lanes][7:8, :], 128) * state + added
+        return carry
+
+    lax.fori_loop(0, 8, sequence, 0)
     for h in range(2):
         lanes = slice(128 * h, 128 * h + 128)
-        d, k, q = decay[rows, lanes].T, gate[rows, lanes].T, query[rows, lanes].T
-        value = z_ref[rows, 512 + 128 * h : 640 + 128 * h]
-        state = state_ref[0, h]
-        outs = []
-        for j in range(8):
-            state = d[:, j : j + 1] * state + k[:, j : j + 1] * value[j : j + 1, :]
-            outs.append(jnp.sum(q[:, j : j + 1] * state, axis=0, keepdims=True))
-        new_ref[0, h] = state
-        output[rows, lanes] = jnp.concatenate(outs, axis=0)
-
-    @pl.when(step == 7)
-    def _():
-        for h in range(2):
-            lanes = slice(128 * h, 128 * h + 128)
-            o = output[:, lanes]
-            zo = z_ref[:, 768 + 128 * h : 896 + 128 * h]
-            o = o * lax.rsqrt(jnp.mean(o * o, axis=1, keepdims=True) + EPS) * lane_gain_ref[...]
-            normed_ref[:, lanes] = jnp.where(live, o * (zo * jax.nn.sigmoid(zo)), 0.0).astype(BF)
+        o = output[:, lanes]
+        zo = z_ref[:, 768 + 128 * h : 896 + 128 * h]
+        o = o * lax.rsqrt(jnp.mean(o * o, axis=1, keepdims=True) + EPS) * lane_gain_ref[...]
+        normed_ref[:, lanes] = jnp.where(live, o * (zo * jax.nn.sigmoid(zo)), 0.0).astype(BF)
 
 
 def recurrence(z, bound, shrink, lengths, lane_gain, state):
-    def whole(*shape):
-        return pl.BlockSpec(shape, lambda s: (0,) * len(shape))
-
-    one = pl.BlockSpec((1, 2, 128, 128), lambda s: (s, 0, 0, 0))
+    vmem = pl.BlockSpec(memory_space=pltpu.VMEM)
     return pl.pallas_call(
         recurrence_kernel,
         out_shape=(
             jax.ShapeDtypeStruct((64, 256), BF),
             jax.ShapeDtypeStruct((8, 2, 128, 128), F32),
         ),
-        grid=(8,),
-        in_specs=[whole(64, 1024), whole(1, 256), whole(2, 64), whole(1, 128), whole(1, 128), one],
-        out_specs=(whole(64, 256), one),
+        in_specs=[vmem] * 6,
+        out_specs=(vmem, vmem),
         scratch_shapes=[pltpu.VMEM((64, 256), F32)] * 4,
         name="recurrence",
     )(z, bound, shrink, lengths, lane_gain, state)

time: 143 us -> 123 us (0.86)
  Pallas kernels: 133 us -> 122 us
  local copies, waits for them, and re-layouts: 8.91 us -> 0 us
    unnamed x32 -> x0, local copies, waits for them, and re-layouts: 8.91 us -> none
    pallas_call x1, Pallas kernels: 11.6 us -> 4.36 us  [recurrence(): pl.pallas_call(recurrence_kernel, out_shape=(jax.ShapeDtypeStruct((64, 25...]
    pallas_call x1, Pallas kernels: 84.5 us -> 79.3 us  [mixer(): pl.pallas_call(mixer_kernel, out_shape=jax.ShapeDtypeStruct((8, 16, 128),...]
    pallas_call x1, Pallas kernels: 35.1 us -> 36.6 us  [front(): pl.pallas_call(front_kernel, out_shape=(jax.ShapeDtypeStruct((64, 1024),...]
where the time goes in v3:
time: 123 us
  Pallas kernels  122 us (99%)
    pallas_call x1, Pallas kernels, mixer(): pl.pallas_call(mixer_kernel, out_shape=jax.ShapeDtypeStruct((8, 16, 128),...  79.3 us
    pallas_call x1, Pallas kernels, front(): pl.pallas_call(front_kernel, out_shape=(jax.ShapeDtypeStruct((64, 1024),...  36.6 us
    pallas_call x1, Pallas kernels, recurrence(): pl.pallas_call(recurrence_kernel, out_shape=(jax.ShapeDtypeStruct((64, 25...  4.36 us

profile of v3, /device:TPU:1, one launch (start us, length us, event | category | flops | bytes accessed | tf_op | source)
XLA Modules:
  0.0 122.7 jit_solution(5215591827602031031)
XLA Ops:
  0.6 36.6 %front.1 = (f32[64,1024]{1,0:T(8,128)}, bf16[64,256]{1,0:T(8,128)(2,1)}, s32[8,1024]{1,0:T(8,128)}) custom-call(bf16[32,1024]{1,0:T(8,128)(2,1)} %bitcast.13, s32[1,128]{1,0:T(1,128)} %bitcast.14, f32[1,256]{1,0:T(1,128)} %bitcast.16, bf16[256,256]{1,0:T(8,128)(2,1)} %wq_ref.1, bf16[256,256]{1,0:T(8,128)(2,1)} %wf_ref.1, bf16[256,256]{1,0:T(8,128)(2,1)} %wi_ref.1, ...), custom_call_target="tpu_custom_call" | custom-call | tf_op jit(solution)/shard_map/front/pallas_call | solution.py:538
  37.2 4.4 %recurrence.1 = (bf16[64,256]{1,0:T(8,128)(2,1)}, f32[8,2,128,128]{3,2,1,0:T(8,128)}) custom-call(f32[64,1024]{1,0:T(8,128)} %get-tuple-element.8.z_ref, f32[1,256]{1,0:T(1,128)} %bitcast.17, f32[2,64]{1,0:T(2,128)} %bitcast.18, s32[1,128]{1,0:T(1,128)} %bitcast.15, f32[1,128]{1,0:T(1,128)} %bitcast.19, f32[8,2,128,128]{3,2,1,0:T(8,128)} %state_ref.1), custom_call_target="tpu_custom_call" | custom-call | tf_op jit(solution)/shard_map/recurrence/pallas_call | solution.py:653
  41.6 79.3 %mixer.1.mixed_ref = bf16[8,16,128]{2,1,0:T(8,128)(2,1)} custom-call(bf16[64,256]{1,0:T(8,128)(2,1)} %get-tuple-element.9.normed_ref, s32[8,1024]{1,0:T(8,128)} %get-tuple-element.7.packed_ref, bf16[64,256]{1,0:T(8,128)(2,1)} %get-tuple-element.10.x_ref, bf16[256,256]{1,0:T(8,128)(2,1)} %result_ref.1, f32[1,32]{1,0:T(1,128)} %bitcast.20, ...), custom_call_target="tpu_custom_call" | custom-call | tf_op jit(solution)/shard_map/mixer/pallas_call | solution.py:384
  120.9 1.8 %spread.1 = bf16[32,1024]{1,0:T(8,128)(2,1)} custom-call(s32[8,1024]{1,0:T(8,128)} %get-tuple-element.7.packed_ref, bf16[8,16,128]{2,1,0:T(8,128)(2,1)} %mixer.1.mixed_ref), custom_call_target="tpu_custom_call" | custom-call | tf_op jit(solution)/shard_map/spread/pallas_call | solution.py:434

commit v4 on v0

v4 whole, which is shorter than its diff:
```python
import jax
import jax.numpy as jnp
from jax import lax
from jax.experimental import pallas as pl
from jax.experimental.pallas import tpu as pltpu
from jax.sharding import Mesh
from jax.sharding import PartitionSpec as P

KV = ("kv_0", "kv_1")
TP = ("tp_0", "tp_1")
KV_TP = ("kv_0", "kv_1", "tp_0", "tp_1")
MESH = pl.DeviceIdType.MESH
EPS = 1e-06
F32 = jnp.float32
BF = jnp.bfloat16
PARTS = ((0, 3), (3, 3), (6, 2))
ORDERS = ("xyz", "yzx", "zxy")
PLANE_ORDERS = ("zy", "yz")


def my_position():
    return dict(
        z=lax.axis_index("kv_0"),
        y=lax.axis_index("kv_1"),
        x=lax.axis_index("tp_0"),
        c=lax.axis_index("tp_1"),
    )


def device_at(at, **moved):
    there = dict(at, **moved)
    return (there["z"], there["y"], there["x"], there["c"])


def plane_offsets():
    return [(dz, dy) for dz in range(4) for dy in range(4) if dz or dy]


def line_offsets():
    return [(dx, dc) for dx in range(4) for dc in range(2) if dx or dc]


def plane_peer(at, dz, dy):
    return device_at(at, z=(at["z"] + dz) % 4, y=(at["y"] + dy) % 4)


def line_peer(at, dx, dc):
    return device_at(at, x=(at["x"] + dx) % 4, c=(at["c"] + dc) % 2)


def meet(peers):
    barrier = pltpu.get_barrier_semaphore()
    for peer in peers:
        pl.semaphore_signal(barrier, inc=1, device_id=peer, device_id_type=MESH)
    pl.semaphore_wait(barrier, len(peers))


class Sender:
    def __init__(self, sends, recvs):
        self.sends, self.recvs, self.used = sends, recvs, 0

    def __call__(self, src, dst, peer):
        i = self.used
        self.used = i + 1
        return start_copy(src, dst, self.sends.at[i], self.recvs.at[i], peer)


def start_copy(src, dst, send_sem, recv_sem, peer):
    copy = pltpu.make_async_remote_copy(
        src_ref=src,
        dst_ref=dst,
        send_sem=send_sem,
        recv_sem=recv_sem,
        device_id=peer,
        device_id_type=MESH,
    )
    copy.start()
    return copy


def times(a, b, dims=((1,), (1,))):
    return lax.dot_general(a, b, (dims, ((), ())), preferred_element_type=F32)


def row_of(column, rows):
    eye = lax.broadcasted_iota(jnp.int32, (rows, 128), 0) == lax.broadcasted_iota(
        jnp.int32, (rows, 128), 1
    )
    return jnp.sum(jnp.where(eye, column, 0.0), axis=0, keepdims=True)


def column_of(row, rows):
    eye = lax.broadcasted_iota(jnp.int32, (rows, 128), 0) == lax.broadcasted_iota(
        jnp.int32, (rows, 128), 1
    )
    return jnp.sum(jnp.where(eye, row, 0.0), axis=1, keepdims=True)


def picks(place, start, rows):
    want = lax.broadcasted_iota(jnp.int32, (rows, 1024), 0) + start
    return jnp.where(want == place, 1.0, 0.0).astype(BF)


def halves(length):
    return pl.ds(0, length // 2), pl.ds(length // 2, length - length // 2)


def gather_plane(at, bufs, orders, send):
    copies = []
    for p, order in enumerate(orders):
        a, b, c = order
        own = bufs[p].at[at[c], at[b], at[a]]
        for db, da in plane_offsets():
            there = {a: (at[a] + da) % 4, b: (at[b] + db) % 4}
            copies.append(send(own, own, device_at(at, **there)))
    return copies


def gather_line(at, bufs, orders, send):
    first = []
    for p, order in enumerate(orders):
        axis = order[-1]
        m = at[axis]
        own = bufs[p].at[m]
        first.append((
            send(own, own, device_at(at, **{axis: (m + 1) % 4})),
            send(own, own, device_at(at, **{axis: (m + 3) % 4})),
        ))
    second = []
    for p, order in enumerate(orders):
        axis = order[-1]
        m = at[axis]
        up, down = (m + 1) % 4, (m + 3) % 4
        lo, hi = halves(bufs[p].shape[1])
        first[p][0].wait_recv()
        from_down = bufs[p].at[down, lo]
        second.append(send(from_down, from_down, device_at(at, **{axis: up})))
        first[p][1].wait_recv()
        from_up = bufs[p].at[up, hi]
        second.append(send(from_up, from_up, device_at(at, **{axis: down})))
    for pair in first:
        for copy in pair:
            copy.wait_send()
    for copy in second:
        copy.wait()


def add_into(ref, idx, term):
    ref[idx] = (ref[idx].astype(F32) + term.astype(F32)).astype(BF)


def reduce_line(at, bufs, axes, pres, received, send, keep=True):
    early = []
    for p, (axis, pre) in enumerate(zip(axes, pres)):
        one_up, one_down, two_up, two_down = received[p]
        m = at[axis]
        up, down, away = (m + 1) % 4, (m + 3) % 4, (m + 2) % 4
        to_up, to_down = device_at(at, **{axis: up}), device_at(at, **{axis: down})
        lo, hi = halves(bufs[p].shape[len(pre) + 1])
        early.append((
            send(bufs[p].at[(*pre, away, lo)], one_up, to_up),
            send(bufs[p].at[(*pre, away, hi)], one_down, to_down),
            send(bufs[p].at[(*pre, up, hi)], two_up.at[hi], to_up),
            send(bufs[p].at[(*pre, down, lo)], two_down.at[lo], to_down),
        ))
    yield
    late = []
    for p, (axis, pre) in enumerate(zip(axes, pres)):
        one_up, one_down, two_up, two_down = received[p]
        m = at[axis]
        up, down = (m + 1) % 4, (m + 3) % 4
        to_up, to_down = device_at(at, **{axis: up}), device_at(at, **{axis: down})
        lo, hi = halves(bufs[p].shape[len(pre) + 1])
        early[p][0].wait_recv()
        add_into(bufs[p], (*pre, up, lo), one_up[...])
        a = send(bufs[p].at[(*pre, up, lo)], two_up.at[lo], to_up)
        early[p][1].wait_recv()
        add_into(bufs[p], (*pre, down, hi), one_down[...])
        late.append((a, send(bufs[p].at[(*pre, down, hi)], two_down.at[hi], to_down)))
    yield
    sums = []
    for p, (axis, pre) in enumerate(zip(axes, pres)):
        for copy in early[p][2:]:
            copy.wait_recv()
        for copy in late[p]:
            copy.wait_recv()
        for copy in (*early[p], *late[p]):
            copy.wait_send()
        own = (*pre, at[axis])
        total = bufs[p][own].astype(F32)
        for ref in received[p][2:]:
            total = total + ref[...].astype(F32)
        if keep:
            bufs[p][own] = total.astype(BF)
        sums.append(total)
    yield sums


def all_of(steps):
    for result in steps:
        pass
    return result


def reduce_plane(at, bufs, orders, received, send):
    copies = []
    for p, order in enumerate(orders):
        a, b, c = order
        for n, (db, da) in enumerate(plane_offsets()):
            there = {a: (at[a] + da) % 4, b: (at[b] + db) % 4}
            block = bufs[p].at[at[c], there[b], there[a]]
            copies.append(send(block, received[p].at[n], device_at(at, **there)))
    sums = []
    for copy in copies:
        copy.wait()
    for p, order in enumerate(orders):
        a, b, c = order
        total = bufs[p][at[c], at[b], at[a]].astype(F32)
        for n in range(15):
            total = total + received[p][n].astype(F32)
        sums.append(total)
    return sums


def split(v):
    high = v.astype(BF)
    return high, (v - high.astype(F32)).astype(BF)


INPUTS = (
    "x", "lengths", "gain", "wq", "wf", "wi", "wo", "bound", "shrink", "lane_gain", "state",
    "result", "later_gain", "gate", "wide", "narrow",
)
IN_HBM = ("x", "wq", "wf", "wi", "wo", "state", "result", "gate", "wide", "narrow")


def line_shapes(lead, tail, parts):
    shapes = []
    for count in parts:
        shape = (*lead, *((count,) if count else ()), *tail)
        half = shape[0] // 2
        shapes += [(half, *shape[1:]), (shape[0] - half, *shape[1:]), shape, shape]
    return shapes


def scratch():
    counts = [count for _, count in PARTS]
    boxes = [(4, 4, 4, count, 16, 128) for count in counts]
    named = [
        ("cols", (8, 32, 1024), BF),
        ("scaled", (256, 1024), BF),
        ("squares", (8, 8, 128), F32),
        ("squares_in", (15, 8, 128), F32),
        ("front_weights", (4, 256, 256), BF),
        ("pa", (4, 4, 64, 512), BF),
        ("pb", (4, 4, 64, 512), BF),
        ("z", (64, 1024), F32),
        ("query", (64, 256), F32),
        ("kept", (64, 256), F32),
        ("key", (64, 256), F32),
        ("output", (64, 256), F32),
        ("state_in", (8, 2, 128, 128), F32),
        ("state_out", (8, 2, 128, 128), F32),
        ("chosen", (512, 1024), BF),
        ("heads", (16, 64, 256), BF),
        ("partial", (8, 64, 256), BF),
        ("arrived", (7, 64, 256), BF),
        ("own_gain", (8, 128), F32),
        ("gains", (8, 8, 128), F32),
        ("own_rows", (64, 256), F32),
        ("residual", (64, 256), F32),
        ("later_squares", (16, 8, 128), F32),
        ("squares_sum", (8, 128), F32),
        ("squares_line", (4, 8, 128), F32),
        ("weights", (2, 2, 128, 4096), BF),
        ("narrows", (2, 128, 4096), BF),
        ("staged", (3, 86, 4096), BF),
        ("result_in", (256, 256), BF),
        ("total", (2, 256, 256), F32),
        ("ypack", (8, 16, 128), BF),
        ("yarrive", (8, 16, 128), BF),
    ]
    groups = [
        ("gathered", boxes),
        ("terms", boxes),
        ("front_one", line_shapes((4, 64), (512,), (0, 0))),
        ("front_two", line_shapes((64,), (512,), (0, 0))),
        ("mixer_line", line_shapes((4, 4), (16, 128), counts)),
        ("mixer_plane", [(15, count, 16, 128) for count in counts]),
    ]
    flat = [pltpu.VMEM(shape, kind) for _, shape, kind in named]
    for _, shapes in groups:
        flat += [pltpu.VMEM(shape, BF) for shape in shapes]
    return named, groups, flat


def layer_kernel(*refs):
    named, groups, flat = scratch()
    ref = dict(zip(INPUTS, refs))
    mixed_out, state_result = refs[len(INPUTS) : len(INPUTS) + 2]
    rest = refs[len(INPUTS) + 2 :]
    ref.update(zip(["_" + name for name, _, _ in named], rest))
    rest = rest[len(named) :]
    group = {}
    for name, shapes in groups:
        group[name], rest = rest[: len(shapes)], rest[len(shapes) :]
    sends, recvs, local = rest
    send = Sender(sends, recvs)
    at = my_position()
    kv = 4 * at["z"] + at["y"]
    tp = 2 * at["x"] + at["c"]
    planes, lines = plane_offsets(), line_offsets()
    fours = lambda refs: [refs[i : i + 4] for i in range(0, len(refs), 4)]

    def fetch(n, src, dst):
        copy = pltpu.make_async_copy(src, dst, local.at[n])
        copy.start()
        return copy

    cols = ref["_cols"]
    x_copy = fetch(0, ref["x"], cols.at[tp])
    front_copies = [
        fetch(1 + n, ref[name], ref["_front_weights"].at[n])
        for n, name in enumerate(("wq", "wf", "wi", "wo"))
    ]
    weight_copies = [
        fetch(5 + n, ref[name], ref["_staged"].at[n])
        for n, name in enumerate(("gate", "wide", "narrow"))
    ]
    state_copy = fetch(8, ref["state"], ref["_state_in"])
    result_copy = fetch(9, ref["result"], ref["_result_in"])
    meet([plane_peer(at, *d) for d in planes] + [line_peer(at, *d) for d in lines])

    x_copy.wait()
    copies = [send(cols.at[tp], cols.at[tp], line_peer(at, *d)) for d in lines]
    own_gain, gains = ref["_own_gain"], ref["_gains"]
    own_gain[...] = jnp.broadcast_to(
        jnp.concatenate([ref["later_gain"][...], jnp.zeros((1, 96), F32)], axis=1), (8, 128)
    )
    gain_copies = [send(own_gain, gains.at[tp], line_peer(at, *d)) for d in lines]
    gains[pl.ds(tp, 1)] = own_gain[...][None]

    lengths = jnp.broadcast_to(ref["lengths"][...], (8, 128)).astype(F32).astype(BF)
    s = lax.broadcasted_iota(jnp.int32, (128, 1024), 0)
    owner = lax.broadcasted_iota(jnp.int32, (128, 1024), 1) // 8
    start = times(lengths, jnp.where(s < owner, 1.0, 0.0).astype(BF), ((1,), (0,)))
    length = times(lengths, jnp.where(s == owner, 1.0, 0.0).astype(BF), ((1,), (0,)))
    slot = lax.broadcasted_iota(jnp.int32, (8, 1024), 1) % 8
    place = jnp.where(slot < length.astype(jnp.int32), start.astype(jnp.int32) + slot, -1)[0:1]
    for part in range(4):
        ref["_chosen"][128 * part : 128 * part + 128] = picks(place, 128 * part, 128)
    gain = jnp.concatenate(
        [column_of(ref["gain"][:, 0:128], 128), column_of(ref["gain"][:, 128:256], 128)], axis=0
    )
    weights, narrows, staged = ref["_weights"], ref["_narrows"], ref["_staged"]
    for n, first in ((0, 80), (1, 96)):
        weights[n, :, first:128] = jnp.zeros((2, 128 - first, 4096), BF)
        narrows[n, first:128] = jnp.zeros((128 - first, 4096), BF)
    for copy in weight_copies:
        copy.wait()
    weights[0, :, 0:86] = staged[0:2]
    narrows[0, 0:86] = staged[2]

    for copy in copies:
        copy.wait()
    partner = line_peer(at, 0, 1)
    weight_sends = [
        send(weights.at[0, :, 0:96], weights.at[1, :, 0:96], partner),
        send(narrows.at[0, 0:96], narrows.at[1, 0:96], partner),
    ]
    scaled, squares = ref["_scaled"], ref["_squares"]
    for k in range(8):
        lanes = slice(128 * k, 128 * k + 128)
        v = cols[:, :, lanes].reshape(256, 128).astype(F32)
        scaled[:, lanes] = (v * gain).astype(BF)
        squares[k] = jnp.broadcast_to(jnp.sum(v * v, axis=0, keepdims=True), (8, 128))
    for copy in front_copies:
        copy.wait()
    pa, pb = ref["_pa"], ref["_pb"]

    def project(n):
        def body(a, carry):
            lhs = scaled[:, pl.ds(pl.multiple_of(256 * a, 256), 256)]
            for half in range(2):
                lanes = slice(256 * half, 256 * half + 256)
                weight = ref["_front_weights"][2 * n + half]
                v = times(lhs, weight, ((0,), (0,))).astype(BF).reshape(4, 64, 256)
                if n == 0:
                    pa[:, a, :, lanes] = v
                else:
                    pb[a, :, :, lanes] = v
            return carry

        lax.fori_loop(0, 4, body, 0)

    one, two = fours(group["front_one"]), fours(group["front_two"])
    project(0)
    steps_a = reduce_line(at, (pa,), ("y",), ((),), one[0:1], send)
    next(steps_a)
    project(1)
    steps_b = reduce_line(at, (pb,), ("z",), ((),), one[1:2], send)
    next(steps_b)
    square_copies = []
    for i, (dz, dy) in enumerate(planes):
        peer = plane_peer(at, dz, dy)
        block = squares.at[(4 * peer[0] + peer[1]) // 2]
        square_copies.append(send(block, ref["_squares_in"].at[i], peer))
    ref["_own_rows"][...] = times(picks(place, 64 * tp, 64), cols[...].reshape(256, 1024))
    next(steps_a)
    next(steps_b)
    next(steps_a)
    steps_a = reduce_line(at, (pa,), ("z",), ((at["y"],),), two[0:1], send, False)
    next(steps_a)
    next(steps_b)
    steps_b = reduce_line(at, (pb,), ("y",), ((at["z"],),), two[1:2], send, False)
    next(steps_b)
    row = lax.broadcasted_iota(jnp.int32, (64, 128), 0)
    lane = lax.broadcasted_iota(jnp.int32, (64, 128), 1)
    length = jnp.sum(
        jnp.where(lane == 8 * kv + row // 8, ref["lengths"][...].astype(F32), 0.0),
        axis=1,
        keepdims=True,
    )
    live = (row[:, 0:1] % 8).astype(F32) < length
    for copy in square_copies:
        copy.wait()
    total = jnp.sum(ref["_squares_in"][...], axis=0) + squares[kv // 2]
    own = jnp.sum(
        jnp.where(lane == 64 * (kv % 2) + row, total[0:1, :], 0.0), axis=1, keepdims=True
    )
    scale = lax.rsqrt(own / 4096 + EPS)
    next(steps_a)
    next(steps_b)
    z = ref["_z"]
    z[:, 0:512] = next(steps_a)[0] * scale
    z[:, 512:1024] = next(steps_b)[0] * scale

    query, kept, keys, output = ref["_query"], ref["_kept"], ref["_key"], ref["_output"]
    slot = lax.broadcasted_iota(jnp.int32, (8, 8, 128), 1)
    for h in range(2):
        lanes = slice(128 * h, 128 * h + 128)
        bound = ref["bound"][:, lanes]
        retain = bound + (1.0 - bound) * jax.nn.sigmoid(z[:, 256 + 128 * h : 384 + 128 * h])
        shrink = jnp.sum(
            jnp.where(lane[:, 0:64] == row[:, 0:64], ref["shrink"][h : h + 1, :], 0.0),
            axis=1,
            keepdims=True,
        )
        decay = jnp.where(live, jnp.exp(jnp.log(retain) + shrink), 1.0).reshape(8, 8, 128)
        key = jnp.where(live, 1.0 - retain, 0.0).reshape(8, 8, 128)
        zq = z[:, lanes]
        q = (zq * jax.nn.sigmoid(zq)).reshape(8, 8, 128)
        value = z[:, 512 + 128 * h : 640 + 128 * h].reshape(8, 8, 128)
        between = q
        out = jnp.sum(q * key, axis=2, keepdims=True) * value
        for back in range(1, 8):
            between = between * (decay if back == 1 else pltpu.roll(decay, back - 1, 1))
            weight = jnp.sum(between * pltpu.roll(key, back, 1), axis=2, keepdims=True)
            out = out + jnp.where(slot >= back, weight * pltpu.roll(value, back, 1), 0.0)
        output[:, lanes] = out.reshape(64, 128)
        before, after = decay, jnp.where(slot < 7, pltpu.roll(decay, 7, 1), 1.0)
        for step in (1, 2, 4):
            before = before * jnp.where(slot >= step, pltpu.roll(before, step, 1), 1.0)
            after = after * jnp.where(slot + step < 8, pltpu.roll(after, 8 - step, 1), 1.0)
        query[:, lanes] = (q * before).reshape(64, 128)
        kept[:, lanes] = before.reshape(64, 128)
        keys[:, lanes] = (key * after).reshape(64, 128)
    state_copy.wait()
    state_in, state_out = ref["_state_in"], ref["_state_out"]

    def read_state(n, carry):
        rows = pl.ds(pl.multiple_of(8 * n, 8), 8)
        for h in range(2):
            lanes = slice(128 * h, 128 * h + 128)
            s_high, s_low = split(state_in[n, h])
            q_high, q_low = split(query[rows, lanes])
            lhs = jnp.concatenate(
                [
                    jnp.concatenate([q_high, q_high], axis=1),
                    jnp.concatenate([q_low, jnp.zeros_like(q_low)], axis=1),
                ],
                axis=0,
            )
            o = times(lhs, jnp.concatenate([s_high, s_low], axis=0), ((1,), (0,)))
            output[rows, lanes] += o[0:8] + o[8:16]
        return carry

    lax.fori_loop(0, 8, read_state, 0)
    heads = ref["_heads"]
    for h in range(2):
        lanes = slice(128 * h, 128 * h + 128)
        o = output[:, lanes]
        zo = z[:, 768 + 128 * h : 896 + 128 * h]
        o = o * lax.rsqrt(jnp.mean(o * o, axis=1, keepdims=True) + EPS) * ref["lane_gain"][...]
        heads[kv, :, lanes] = jnp.where(live, o * (zo * jax.nn.sigmoid(zo)), 0.0).astype(BF)
    copies = [send(heads.at[kv], heads.at[kv], plane_peer(at, *d)) for d in planes]

    def write_state(n, carry):
        rows = pl.ds(pl.multiple_of(8 * n, 8), 8)
        for h in range(2):
            lanes = slice(128 * h, 128 * h + 128)
            k_high, k_low = split(keys[rows, lanes])
            v_high, v_low = split(z[rows, 512 + 128 * h : 640 + 128 * h])
            added = times(
                jnp.concatenate([k_high, k_high, k_low], axis=0),
                jnp.concatenate([v_high, v_low, v_high], axis=0),
                ((0,), (0,)),
            )
            state_out[n, h] = column_of(kept[rows, lanes][7:8, :], 128) * state_in[n, h] + added
        return carry

    lax.fori_loop(0, 8, write_state, 0)
    new_copy = fetch(10, state_out, state_result)
    result_copy.wait()
    for copy in gain_copies:
        copy.wait()
    gain = jnp.concatenate([gains[t, 0:1, 0:32] for t in range(8)], axis=1)
    for copy in copies:
        copy.wait()

    partial, arrived, result = ref["_partial"], ref["_arrived"], ref["_result_in"]
    all_heads = heads[...].reshape(1024, 256)
    for part in range(2):
        picked = ref["_chosen"][256 * part : 256 * part + 256]
        packed = times(picked, all_heads, ((1,), (0,))).astype(BF)
        partial[4 * part : 4 * part + 4] = (
            times(packed, result[...], ((1,), (0,))).astype(BF).reshape(4, 64, 256)
        )
    copies = []
    for i, (dx, dc) in enumerate(lines):
        peer = line_peer(at, dx, dc)
        copies.append(send(partial.at[2 * peer[2] + peer[3]], arrived.at[i], peer))
    attended = partial[tp].astype(F32)
    for i, copy in enumerate(copies):
        copy.wait()
        attended = attended + arrived[i].astype(F32)
    residual = (ref["_own_rows"][...] + attended).astype(BF).astype(F32)
    tile = (residual * gain).astype(BF)
    blocks = [
        tile[16 * i : 16 * i + 16, 128 * h : 128 * h + 128] for h in range(2) for i in range(4)
    ]
    gathered = group["gathered"]
    for p, ((first, count), order) in enumerate(zip(PARTS, ORDERS)):
        idx = tuple(at[a] for a in order[::-1])
        for b in range(count):
            gathered[p][(*idx, b)] = blocks[first + b]
    copies = gather_plane(at, gathered, ORDERS, send)
    ref["_residual"][...] = residual
    later = ref["_later_squares"]
    own_squares = jnp.sum(residual * residual, axis=1, keepdims=True)
    later[0] = jnp.broadcast_to(row_of(own_squares, 64), (8, 128))
    square_copies = [
        send(later.at[0], later.at[1 + i], plane_peer(at, *d)) for i, d in enumerate(planes)
    ]
    for copy in copies:
        copy.wait()
    for copy in square_copies:
        copy.wait()
    squares_sum, squares_line = ref["_squares_sum"], ref["_squares_line"]
    own_sum = jnp.sum(later[...], axis=0)
    squares_sum[...] = own_sum
    squares_line[pl.ds(at["x"], 1)] = own_sum[None]
    line_copies = [
        send(squares_sum, squares_line.at[at["x"]], line_peer(at, dx, 0)) for dx in (1, 2, 3)
    ]
    gather_line(at, gathered, ORDERS, send)
    for copy in (*line_copies, *weight_sends):
        copy.wait()

    ga, gb, gc = gathered
    total = ref["_total"]

    def rows_at(zz, yy):
        v = jnp.concatenate([ga[zz, yy], gb[:, zz, yy], gc[yy, :, zz]], axis=1)
        return jnp.concatenate(
            [v[:, 0:4].reshape(256, 128), v[:, 4:8].reshape(256, 128)], axis=1
        )

    total[...] = jnp.zeros_like(total)

    def widening(zz, carry):
        lhs = jnp.concatenate([rows_at(zz, yy) for yy in range(4)], axis=1)
        cols = pl.ds(pl.multiple_of(zz * 1024, 1024), 1024)
        for core in range(2):
            total[core] += times(lhs, weights[core, :, :, cols].reshape(256, 1024))
        return carry

    lax.fori_loop(0, 4, widening, 0)
    scale = lax.rsqrt(
        jnp.concatenate([column_of(squares_line[g, 0:1, :], 64) for g in range(4)], axis=0)
        / 4096
        + EPS
    )
    hidden = []
    for core in range(2):
        gated = total[core, :, 0:128] * scale
        upward = total[core, :, 128:256] * scale
        hidden.append((gated * jax.nn.sigmoid(gated) * upward).astype(BF))
    hidden = jnp.concatenate(hidden, axis=1)
    ta, tb, tc = group["terms"]

    def narrowing(k, carry):
        cols = pl.ds(pl.multiple_of(k * 256, 256), 256)
        rhs = jnp.concatenate([narrows[0, :, cols], narrows[1, :, cols]], axis=0)
        term = times(hidden, rhs, ((1,), (0,))).astype(BF)
        v = jnp.concatenate(
            [term[:, 0:128].reshape(4, 4, 16, 128), term[:, 128:256].reshape(4, 4, 16, 128)], axis=1
        )
        zz, yy = k // 4, k % 4
        ta[zz, yy] = v[:, 0:3]
        tb[:, zz, yy] = v[:, 3:6]
        tc[yy, :, zz] = v[:, 6:8]
        return carry

    lax.fori_loop(0, 16, narrowing, 0)
    all_of(
        reduce_line(
            at, group["terms"], [order[-1] for order in ORDERS], ((),) * 3,
            fours(group["mixer_line"]), send,
        )
    )
    sums = reduce_plane(at, group["terms"], ORDERS, group["mixer_plane"], send)
    sums = jnp.concatenate(sums, axis=0)

    mixed = []
    for h in range(2):
        for i in range(4):
            res = ref["_residual"][16 * i : 16 * i + 16, 128 * h : 128 * h + 128]
            mixed.append((res + sums[4 * h + i]).astype(BF))
    ypack, yarrive = ref["_ypack"], ref["_yarrive"]
    for t in range(8):
        h, first = t // 4, 32 * (t % 4)
        ypack[t] = jnp.concatenate(
            [mixed[4 * h + i][:, first : first + 32] for i in range(4)], axis=1
        )
    copies = []
    for dx, dc in lines:
        peer = line_peer(at, dx, dc)
        copies.append(send(ypack.at[2 * peer[2] + peer[3]], yarrive.at[tp], peer))
    yarrive[pl.ds(tp, 1)] = ypack[pl.ds(tp, 1)]
    for copy in copies:
        copy.wait()
    spread = jnp.zeros((32, 1024), F32)
    j = lax.broadcasted_iota(jnp.int32, (128, 1024), 0)
    rows = 64 * (j // 16) + j % 16
    for a in range(4):
        chosen = jnp.where(rows + 16 * a == place, 1.0, 0.0).astype(BF)
        piece = yarrive[...].reshape(128, 128)[:, 32 * a : 32 * a + 32]
        spread = spread + times(piece, chosen, ((0,), (0,)))
    mixed_out[...] = spread.astype(BF)
    new_copy.wait()
    assert send.used <= sends.shape[0]


def layer(*arguments):
    vmem = pl.BlockSpec(memory_space=pltpu.VMEM)
    far = pl.BlockSpec(memory_space=pltpu.HBM)
    copies = 260
    return pl.pallas_call(
        layer_kernel,
        out_shape=(
            jax.ShapeDtypeStruct((32, 1024), BF),
            jax.ShapeDtypeStruct((8, 2, 128, 128), F32),
        ),
        in_specs=[far if name in IN_HBM else vmem for name in INPUTS],
        out_specs=(vmem, far),
        scratch_shapes=[
            *scratch()[2],
            pltpu.SemaphoreType.DMA((copies,)),
            pltpu.SemaphoreType.DMA((copies,)),
            pltpu.SemaphoreType.DMA((11,)),
        ],
        compiler_params=pltpu.CompilerParams(
            collective_id=0, has_side_effects=True, vmem_limit_bytes=67043328
        ),
        name="layer",
    )(*arguments)


def local(
    residual_entries,
    fresh_extents,
    memory_matrix,
    initial_rescale_vector,
    probe_matrix,
    retain_matrix,
    content_matrix,
    result_switch_matrix,
    retain_lower_limit,
    extra_shrink_log,
    lane_result_rescale,
    result_matrix,
    later_rescale_vector,
    mixer_switch_matrix,
    widening_matrix,
    narrowing_matrix,
):
    mixed, carried = layer(
        residual_entries.T,
        fresh_extents.reshape(1, 128),
        initial_rescale_vector.reshape(1, 256),
        probe_matrix,
        retain_matrix,
        content_matrix,
        result_switch_matrix,
        retain_lower_limit.reshape(1, 256),
        extra_shrink_log.T,
        lane_result_rescale.reshape(1, 128),
        memory_matrix,
        result_matrix,
        later_rescale_vector.reshape(1, 32),
        mixer_switch_matrix.T,
        widening_matrix.T,
        narrowing_matrix,
    )
    return (mixed.T, carried)


def solution(mesh):
    torus = Mesh(mesh.devices.reshape(4, 4, 4, 2), ("kv_0", "kv_1", "tp_0", "tp_1"))
    placed = (
        P(None, KV_TP),
        P(),
        P(KV, TP, None, None),
        P(KV),
        P(KV, TP),
        P(KV, TP),
        P(KV, TP),
        P(KV, TP),
        P(TP),
        P(KV, TP),
        P(),
        P(TP, KV),
        P(KV_TP),
        P(None, KV_TP),
        P(None, KV_TP),
        P(KV_TP, None),
    )
    return jax.shard_map(
        local,
        mesh=torus,
        in_specs=placed,
        out_specs=(P(None, KV_TP), P(KV, TP, None, None)),
        check_vma=False,
    )
```

time: 367 us -> 107 us (0.29)
  waiting for transfers between devices: 163 us -> 0 us
  Pallas kernels: 0 us -> 102 us
  blocking collectives: 94.5 us -> 0 us
  matrix products: 34.5 us -> 0 us
  other arithmetic: 22.3 us -> 0 us
  local copies, waits for them, and re-layouts: 24.8 us -> 3.77 us
  between operations: 14.2 us -> 0.65 us
  starting transfers between devices: 11.6 us -> 0 us
    pallas_call x0 -> x1, Pallas kernels: none -> 102 us  [layer(): pl.pallas_call(layer_kernel, out_shape=(jax.ShapeDtypeStruct((32, 1024),...]
    all_gather x1 -> x0, waiting for transfers between devices: 65.2 us -> none  [local(): piece = lax.all_gather(second_in, KV_TP, axis=1, tiled=True)]
    all_to_all x4 -> x0, blocking collectives: 65.1 us -> none  [the longest x2 36.3 us: sent_and_summed(): pieces = lax.all_to_all(split_up(x, dim, devices), axis, 0, 0, tiled=True)]
    all_to_all x2 -> x0, waiting for transfers between devices: 59.3 us -> none  [the longest x1 53.2 us: sum_in_two_steps(): lax.all_to_all(nearer.astype(jnp.bfloat16), far, split_axis=0, concat_axi...]
    reduce_scatter x2 -> x0, waiting for transfers between devices: 38.3 us -> none  [own_rows(): total = lax.psum_scatter(total, axis, scatter_dimension=0, tiled=True)]
    dot_general x15 -> x0, matrix products: 34.5 us -> none  [the longest x8 15.1 us: local(): jnp.einsum('bhd,bhdv->bhv', query[:, position], carried, precision=lax.Pr...]
    psum x4 -> x0, blocking collectives: 29.4 us -> none  [one_axis_at_a_time(): return functools.reduce(lax.psum, axes, x)]
    reduce_sum x7 -> x0, other arithmetic: 12.4 us -> none  [the longest x2 9.14 us: sent_and_summed(): return jnp.sum(pieces.astype(jnp.float32), axis=0)]
  transfers between devices with their start and end apart: 5 -> 0, of which waited for: 5 -> 0; matrix products, arithmetic and copies ran while one was open for 0% -> 0% of each run, Pallas kernels for 0% -> 0%
where the time goes in v4:
time: 107 us
  Pallas kernels  102 us (95%)
  local copies, waits for them, and re-layouts  3.77 us (4%)
    pallas_call x1, Pallas kernels, layer(): pl.pallas_call(layer_kernel, out_shape=(jax.ShapeDtypeStruct((32, 1024),...  102 us
    unnamed x2, local copies, waits for them, and re-layouts  3.77 us

profile of v4, /device:TPU:1, one launch (start us, length us, event | category | flops | bytes accessed | tf_op | source)
XLA Modules:
  0.0 106.9 jit_solution(985609333553692548)
XLA Ops:
  0.6 102.5 %layer.1 = (bf16[32,1024]{1,0:T(8,128)(2,1)}, f32[8,2,128,128]{3,2,1,0:T(8,128)}) custom-call(bf16[32,1024]{1,0:T(8,128)(2,1)} %bitcast.12, s32[1,128]{1,0:T(1,128)} %bitcast.17, f32[1,256]{1,0:T(1,128)} %bitcast.14, bf16[256,256]{1,0:T(8,128)(2,1)} %refs_3_.1, bf16[256,256]{1,0:T(8,128)(2,1)} %refs_4_.1, bf16[256,256]{1,0:T(8,128)(2,1)} %refs_5_.1, ...), custom_call_target="tpu_custom_call" | custom-call | tf_op jit(solution)/shard_map/layer/pallas_call | solution.py:659
  103.1 1.5 %copy.20 = bf16[1024,32]{0,1:T(8,128)(2,1)} copy(bf16[1024,32]{0,1:T(8,128)(2,1)} %bitcast.13) | data formatting | bytes 131072
  104.6 2.3 %copy.21 = f32[8,2,128,128]{3,2,1,0:T(8,128)} copy(f32[8,2,128,128]{3,2,1,0:T(8,128)} %get-tuple-element.9) | data formatting | bytes 2097152

commit v5 on v4

--- a/solution.py
+++ b/solution.py
@@ -1,3 +1,5 @@
+import functools
+
 import jax
 import jax.numpy as jnp
 from jax import lax
@@ -106,19 +108,21 @@
 
 
 def gather_plane(at, bufs, orders, send):
-    copies = []
+    copies = [[] for _ in orders]
     for p, order in enumerate(orders):
         a, b, c = order
         own = bufs[p].at[at[c], at[b], at[a]]
         for db, da in plane_offsets():
             there = {a: (at[a] + da) % 4, b: (at[b] + db) % 4}
-            copies.append(send(own, own, device_at(at, **there)))
+            copies[p].append(send(own, own, device_at(at, **there)))
     return copies
 
 
-def gather_line(at, bufs, orders, send):
+def gather_line(at, bufs, orders, ready, send):
     first = []
     for p, order in enumerate(orders):
+        for copy in ready[p]:
+            copy.wait_recv()
         axis = order[-1]
         m = at[axis]
         own = bufs[p].at[m]
@@ -126,6 +130,7 @@
             send(own, own, device_at(at, **{axis: (m + 1) % 4})),
             send(own, own, device_at(at, **{axis: (m + 3) % 4})),
         ))
+    yield
     second = []
     for p, order in enumerate(orders):
         axis = order[-1]
@@ -138,18 +143,19 @@
         first[p][1].wait_recv()
         from_up = bufs[p].at[up, hi]
         second.append(send(from_up, from_up, device_at(at, **{axis: down})))
-    for pair in first:
-        for copy in pair:
+    for part in (*ready, *first):
+        for copy in part:
             copy.wait_send()
     for copy in second:
         copy.wait()
+    yield
 
 
 def add_into(ref, idx, term):
     ref[idx] = (ref[idx].astype(F32) + term.astype(F32)).astype(BF)
 
 
-def reduce_line(at, bufs, axes, pres, received, send, keep=True):
+def reduce_line(at, bufs, axes, pres, received, send, keep=True, after=None):
     early = []
     for p, (axis, pre) in enumerate(zip(axes, pres)):
         one_up, one_down, two_up, two_down = received[p]
@@ -184,8 +190,6 @@
             copy.wait_recv()
         for copy in late[p]:
             copy.wait_recv()
-        for copy in (*early[p], *late[p]):
-            copy.wait_send()
         own = (*pre, at[axis])
         total = bufs[p][own].astype(F32)
         for ref in received[p][2:]:
@@ -193,31 +197,35 @@
         if keep:
             bufs[p][own] = total.astype(BF)
         sums.append(total)
+        if after:
+            after(p)
+    for p in range(len(axes)):
+        for copy in (*early[p], *late[p]):
+            copy.wait_send()
     yield sums
 
 
-def all_of(steps):
-    for result in steps:
-        pass
-    return result
-
-
-def reduce_plane(at, bufs, orders, received, send):
+def reduce_torus(at, bufs, orders, line_received, plane_received, send):
     copies = []
-    for p, order in enumerate(orders):
-        a, b, c = order
+
+    def to_plane(p):
+        a, b, c = orders[p]
+        copies.append([])
         for n, (db, da) in enumerate(plane_offsets()):
             there = {a: (at[a] + da) % 4, b: (at[b] + db) % 4}
             block = bufs[p].at[at[c], there[b], there[a]]
-            copies.append(send(block, received[p].at[n], device_at(at, **there)))
+            copies[p].append(send(block, plane_received[p].at[n], device_at(at, **there)))
+
+    axes = [order[-1] for order in orders]
+    for _ in reduce_line(at, bufs, axes, ((),) * 3, line_received, send, True, to_plane):
+        pass
     sums = []
-    for copy in copies:
-        copy.wait()
     for p, order in enumerate(orders):
         a, b, c = order
         total = bufs[p][at[c], at[b], at[a]].astype(F32)
-        for n in range(15):
-            total = total + received[p][n].astype(F32)
+        for n, copy in enumerate(copies[p]):
+            copy.wait()
+            total = total + plane_received[p][n].astype(F32)
         sums.append(total)
     return sums
 
@@ -248,10 +256,10 @@
     boxes = [(4, 4, 4, count, 16, 128) for count in counts]
     named = [
         ("cols", (8, 32, 1024), BF),
-        ("scaled", (256, 1024), BF),
+        ("scaled", (1024, 256), BF),
         ("squares", (8, 8, 128), F32),
         ("squares_in", (15, 8, 128), F32),
-        ("front_weights", (4, 256, 256), BF),
+        ("front_weights", (2, 256, 512), BF),
         ("pa", (4, 4, 64, 512), BF),
         ("pb", (4, 4, 64, 512), BF),
         ("z", (64, 1024), F32),
@@ -262,7 +270,7 @@
         ("state_in", (8, 2, 128, 128), F32),
         ("state_out", (8, 2, 128, 128), F32),
         ("chosen", (512, 1024), BF),
-        ("heads", (16, 64, 256), BF),
+        ("heads", (16, 2, 64, 128), BF),
         ("partial", (8, 64, 256), BF),
         ("arrived", (7, 64, 256), BF),
         ("own_gain", (8, 128), F32),
@@ -297,14 +305,14 @@
 def layer_kernel(*refs):
     named, groups, flat = scratch()
     ref = dict(zip(INPUTS, refs))
-    mixed_out, state_result = refs[len(INPUTS) : len(INPUTS) + 2]
-    rest = refs[len(INPUTS) + 2 :]
+    mixed_out, place_out, state_result = refs[len(INPUTS) : len(INPUTS) + 3]
+    rest = refs[len(INPUTS) + 3 :]
     ref.update(zip(["_" + name for name, _, _ in named], rest))
     rest = rest[len(named) :]
     group = {}
     for name, shapes in groups:
         group[name], rest = rest[: len(shapes)], rest[len(shapes) :]
-    sends, recvs, local = rest
+    sends, recvs, local, ready = rest
     send = Sender(sends, recvs)
     at = my_position()
     kv = 4 * at["z"] + at["y"]
@@ -320,7 +328,7 @@
     cols = ref["_cols"]
     x_copy = fetch(0, ref["x"], cols.at[tp])
     front_copies = [
-        fetch(1 + n, ref[name], ref["_front_weights"].at[n])
+        fetch(1 + n, ref[name], ref["_front_weights"].at[n // 2, :, 256 * (n % 2) : 256 * (n % 2) + 256])
         for n, name in enumerate(("wq", "wf", "wi", "wo"))
     ]
     weight_copies = [
@@ -329,10 +337,19 @@
     ]
     state_copy = fetch(8, ref["state"], ref["_state_in"])
     result_copy = fetch(9, ref["result"], ref["_result_in"])
-    meet([plane_peer(at, *d) for d in planes] + [line_peer(at, *d) for d in lines])
+    turns = (1, 2, 3)
+    meet(
+        [line_peer(at, *d) for d in lines]
+        + [plane_peer(at, dz, 0) for dz in turns]
+        + [plane_peer(at, 0, dy) for dy in turns]
+    )
+    for dy in turns:
+        pl.semaphore_signal(ready, inc=1, device_id=plane_peer(at, 0, dy), device_id_type=MESH)
 
     x_copy.wait()
-    copies = [send(cols.at[tp], cols.at[tp], line_peer(at, *d)) for d in lines]
+    partner = line_peer(at, 0, 1)
+    far_copies = [send(cols.at[tp], cols.at[tp], line_peer(at, dx, 0)) for dx in turns]
+    near_copies = [send(cols.at[tp], cols.at[tp], partner)]
     own_gain, gains = ref["_own_gain"], ref["_gains"]
     own_gain[...] = jnp.broadcast_to(
         jnp.concatenate([ref["later_gain"][...], jnp.zeros((1, 96), F32)], axis=1), (8, 128)
@@ -346,7 +363,9 @@
     start = times(lengths, jnp.where(s < owner, 1.0, 0.0).astype(BF), ((1,), (0,)))
     length = times(lengths, jnp.where(s == owner, 1.0, 0.0).astype(BF), ((1,), (0,)))
     slot = lax.broadcasted_iota(jnp.int32, (8, 1024), 1) % 8
-    place = jnp.where(slot < length.astype(jnp.int32), start.astype(jnp.int32) + slot, -1)[0:1]
+    place = jnp.where(slot < length.astype(jnp.int32), start.astype(jnp.int32) + slot, -1)
+    place_out[...] = place
+    place = place[0:1]
     for part in range(4):
         ref["_chosen"][128 * part : 128 * part + 128] = picks(place, 128 * part, 128)
     gain = jnp.concatenate(
@@ -361,9 +380,12 @@
     weights[0, :, 0:86] = staged[0:2]
     narrows[0, 0:86] = staged[2]
 
-    for copy in copies:
-        copy.wait()
-    partner = line_peer(at, 0, 1)
+    for dx, copy in zip(turns, far_copies):
+        copy.wait()
+        came = 2 * ((at["x"] + 4 - dx) % 4) + at["c"]
+        near_copies.append(send(cols.at[came], cols.at[came], partner))
+    for copy in near_copies:
+        copy.wait()
     weight_sends = [
         send(weights.at[0, :, 0:96], weights.at[1, :, 0:96], partner),
         send(narrows.at[0, 0:96], narrows.at[1, 0:96], partner),
@@ -372,7 +394,7 @@
     for k in range(8):
         lanes = slice(128 * k, 128 * k + 128)
         v = cols[:, :, lanes].reshape(256, 128).astype(F32)
-        scaled[:, lanes] = (v * gain).astype(BF)
+        scaled[lanes, :] = (v * gain).T.astype(BF)
         squares[k] = jnp.broadcast_to(jnp.sum(v * v, axis=0, keepdims=True), (8, 128))
     for copy in front_copies:
         copy.wait()
@@ -380,15 +402,12 @@
 
     def project(n):
         def body(a, carry):
-            lhs = scaled[:, pl.ds(pl.multiple_of(256 * a, 256), 256)]
-            for half in range(2):
-                lanes = slice(256 * half, 256 * half + 256)
-                weight = ref["_front_weights"][2 * n + half]
-                v = times(lhs, weight, ((0,), (0,))).astype(BF).reshape(4, 64, 256)
-                if n == 0:
-                    pa[:, a, :, lanes] = v
-                else:
-                    pb[a, :, :, lanes] = v
+            lhs = scaled[pl.ds(pl.multiple_of(256 * a, 256), 256), :]
+            v = times(lhs, ref["_front_weights"][n], ((1,), (0,))).astype(BF).reshape(4, 64, 512)
+            if n == 0:
+                pa[:, a] = v
+            else:
+                pb[a] = v
             return carry
 
         lax.fori_loop(0, 4, body, 0)
@@ -400,6 +419,7 @@
     project(1)
     steps_b = reduce_line(at, (pb,), ("z",), ((),), one[1:2], send)
     next(steps_b)
+    pl.semaphore_wait(ready, 3)
     square_copies = []
     for i, (dz, dy) in enumerate(planes):
         peer = plane_peer(at, dz, dy)
@@ -437,6 +457,25 @@
 
     query, kept, keys, output = ref["_query"], ref["_kept"], ref["_key"], ref["_output"]
     slot = lax.broadcasted_iota(jnp.int32, (8, 8, 128), 1)
+    state_in, state_out, heads = ref["_state_in"], ref["_state_out"], ref["_heads"]
+
+    def read_state(h, n, carry):
+        rows = pl.ds(pl.multiple_of(8 * n, 8), 8)
+        lanes = slice(128 * h, 128 * h + 128)
+        s_high, s_low = split(state_in[n, h])
+        q_high, q_low = split(query[rows, lanes])
+        lhs = jnp.concatenate(
+            [
+                jnp.concatenate([q_high, q_high], axis=1),
+                jnp.concatenate([q_low, jnp.zeros_like(q_low)], axis=1),
+            ],
+            axis=0,
+        )
+        o = times(lhs, jnp.concatenate([s_high, s_low], axis=0), ((1,), (0,)))
+        output[rows, lanes] += o[0:8] + o[8:16]
+        return carry
+
+    copies = []
     for h in range(2):
         lanes = slice(128 * h, 128 * h + 128)
         bound = ref["bound"][:, lanes]
@@ -465,36 +504,15 @@
         query[:, lanes] = (q * before).reshape(64, 128)
         kept[:, lanes] = before.reshape(64, 128)
         keys[:, lanes] = (key * after).reshape(64, 128)
-    state_copy.wait()
-    state_in, state_out = ref["_state_in"], ref["_state_out"]
-
-    def read_state(n, carry):
-        rows = pl.ds(pl.multiple_of(8 * n, 8), 8)
-        for h in range(2):
-            lanes = slice(128 * h, 128 * h + 128)
-            s_high, s_low = split(state_in[n, h])
-            q_high, q_low = split(query[rows, lanes])
-            lhs = jnp.concatenate(
-                [
-                    jnp.concatenate([q_high, q_high], axis=1),
-                    jnp.concatenate([q_low, jnp.zeros_like(q_low)], axis=1),
-                ],
-                axis=0,
-            )
-            o = times(lhs, jnp.concatenate([s_high, s_low], axis=0), ((1,), (0,)))
-            output[rows, lanes] += o[0:8] + o[8:16]
-        return carry
-
-    lax.fori_loop(0, 8, read_state, 0)
-    heads = ref["_heads"]
-    for h in range(2):
-        lanes = slice(128 * h, 128 * h + 128)
+        if h == 0:
+            state_copy.wait()
+        lax.fori_loop(0, 8, functools.partial(read_state, h), 0, unroll=2)
         o = output[:, lanes]
         zo = z[:, 768 + 128 * h : 896 + 128 * h]
         o = o * lax.rsqrt(jnp.mean(o * o, axis=1, keepdims=True) + EPS) * ref["lane_gain"][...]
-        heads[kv, :, lanes] = jnp.where(live, o * (zo * jax.nn.sigmoid(zo)), 0.0).astype(BF)
-    copies = [send(heads.at[kv], heads.at[kv], plane_peer(at, *d)) for d in planes]
-
+        heads[kv, h] = jnp.where(live, o * (zo * jax.nn.sigmoid(zo)), 0.0).astype(BF)
+        own = heads.at[kv, h]
+        copies += [send(own, own, plane_peer(at, *d)) for d in planes]
     def write_state(n, carry):
         rows = pl.ds(pl.multiple_of(8 * n, 8), 8)
         for h in range(2):
@@ -519,7 +537,7 @@
         copy.wait()
 
     partial, arrived, result = ref["_partial"], ref["_arrived"], ref["_result_in"]
-    all_heads = heads[...].reshape(1024, 256)
+    all_heads = jnp.concatenate([heads[:, h].reshape(1024, 128) for h in range(2)], axis=1)
     for part in range(2):
         picked = ref["_chosen"][256 * part : 256 * part + 256]
         packed = times(picked, all_heads, ((1,), (0,))).astype(BF)
@@ -552,8 +570,8 @@
     square_copies = [
         send(later.at[0], later.at[1 + i], plane_peer(at, *d)) for i, d in enumerate(planes)
     ]
-    for copy in copies:
-        copy.wait()
+    steps = gather_line(at, gathered, ORDERS, copies, send)
+    next(steps)
     for copy in square_copies:
         copy.wait()
     squares_sum, squares_line = ref["_squares_sum"], ref["_squares_line"]
@@ -563,7 +581,7 @@
     line_copies = [
         send(squares_sum, squares_line.at[at["x"]], line_peer(at, dx, 0)) for dx in (1, 2, 3)
     ]
-    gather_line(at, gathered, ORDERS, send)
+    next(steps)
     for copy in (*line_copies, *weight_sends):
         copy.wait()
 
@@ -599,28 +617,30 @@
     hidden = jnp.concatenate(hidden, axis=1)
     ta, tb, tc = group["terms"]
 
-    def narrowing(k, carry):
-        cols = pl.ds(pl.multiple_of(k * 256, 256), 256)
+    def narrowing(zz, carry):
+        cols = pl.ds(pl.multiple_of(zz * 1024, 1024), 1024)
         rhs = jnp.concatenate([narrows[0, :, cols], narrows[1, :, cols]], axis=0)
         term = times(hidden, rhs, ((1,), (0,))).astype(BF)
-        v = jnp.concatenate(
-            [term[:, 0:128].reshape(4, 4, 16, 128), term[:, 128:256].reshape(4, 4, 16, 128)], axis=1
-        )
-        zz, yy = k // 4, k % 4
-        ta[zz, yy] = v[:, 0:3]
-        tb[:, zz, yy] = v[:, 3:6]
-        tc[yy, :, zz] = v[:, 6:8]
+        for yy in range(4):
+            v = jnp.concatenate(
+                [
+                    term[:, 256 * yy + 128 * h : 256 * yy + 128 * h + 128].reshape(4, 4, 16, 128)
+                    for h in range(2)
+                ],
+                axis=1,
+            )
+            ta[zz, yy] = v[:, 0:3]
+            tb[:, zz, yy] = v[:, 3:6]
+            tc[yy, :, zz] = v[:, 6:8]
         return carry
 
-    lax.fori_loop(0, 16, narrowing, 0)
-    all_of(
-        reduce_line(
-            at, group["terms"], [order[-1] for order in ORDERS], ((),) * 3,
-            fours(group["mixer_line"]), send,
-        )
-    )
-    sums = reduce_plane(at, group["terms"], ORDERS, group["mixer_plane"], send)
-    sums = jnp.concatenate(sums, axis=0)
+    lax.fori_loop(0, 4, narrowing, 0)
+    sums = jnp.concatenate(
+        reduce_torus(
+            at, group["terms"], ORDERS, fours(group["mixer_line"]), group["mixer_plane"], send
+        ),
+        axis=0,
+    )
 
     mixed = []
     for h in range(2):
@@ -640,14 +660,7 @@
     yarrive[pl.ds(tp, 1)] = ypack[pl.ds(tp, 1)]
     for copy in copies:
         copy.wait()
-    spread = jnp.zeros((32, 1024), F32)
-    j = lax.broadcasted_iota(jnp.int32, (128, 1024), 0)
-    rows = 64 * (j // 16) + j % 16
-    for a in range(4):
-        chosen = jnp.where(rows + 16 * a == place, 1.0, 0.0).astype(BF)
-        piece = yarrive[...].reshape(128, 128)[:, 32 * a : 32 * a + 32]
-        spread = spread + times(piece, chosen, ((0,), (0,)))
-    mixed_out[...] = spread.astype(BF)
+    mixed_out[...] = yarrive[...]
     new_copy.wait()
     assert send.used <= sends.shape[0]
 
@@ -655,26 +668,62 @@
 def layer(*arguments):
     vmem = pl.BlockSpec(memory_space=pltpu.VMEM)
     far = pl.BlockSpec(memory_space=pltpu.HBM)
-    copies = 260
+    copies = 280
     return pl.pallas_call(
         layer_kernel,
         out_shape=(
-            jax.ShapeDtypeStruct((32, 1024), BF),
+            jax.ShapeDtypeStruct((8, 16, 128), BF),
+            jax.ShapeDtypeStruct((8, 1024), jnp.int32),
             jax.ShapeDtypeStruct((8, 2, 128, 128), F32),
         ),
         in_specs=[far if name in IN_HBM else vmem for name in INPUTS],
-        out_specs=(vmem, far),
+        out_specs=(vmem, vmem, far),
         scratch_shapes=[
             *scratch()[2],
             pltpu.SemaphoreType.DMA((copies,)),
             pltpu.SemaphoreType.DMA((copies,)),
             pltpu.SemaphoreType.DMA((11,)),
+            pltpu.SemaphoreType.REGULAR,
         ],
         compiler_params=pltpu.CompilerParams(
             collective_id=0, has_side_effects=True, vmem_limit_bytes=67043328
         ),
         name="layer",
     )(*arguments)
+
+
+def finish_kernel(packed_ref, place_ref, state_ref, mixed_ref, new_ref, held, sems):
+    take = pltpu.make_async_copy(state_ref, held, sems.at[0])
+    take.start()
+    j = lax.broadcasted_iota(jnp.int32, (128, 1024), 0)
+    rows = 64 * (j // 16) + j % 16 - place_ref[0:1, :]
+    packed = packed_ref[...].reshape(128, 128)
+    mixed = jnp.zeros((32, 1024), F32)
+    for a in range(4):
+        chosen = jnp.where(rows == -16 * a, 1.0, 0.0).astype(BF)
+        mixed = mixed + times(packed[:, 32 * a : 32 * a + 32], chosen, ((0,), (0,)))
+    take.wait()
+    give = pltpu.make_async_copy(held, new_ref, sems.at[1])
+    give.start()
+    mixed_ref[...] = mixed.astype(BF)
+    give.wait()
+
+
+def finish(packed, place, state):
+    vmem = pl.BlockSpec(memory_space=pltpu.VMEM)
+    far = pl.BlockSpec(memory_space=pltpu.HBM)
+    return pl.pallas_call(
+        finish_kernel,
+        out_shape=(
+            jax.ShapeDtypeStruct((32, 1024), BF),
+            jax.ShapeDtypeStruct((8, 2, 128, 128), F32),
+        ),
+        in_specs=[vmem, vmem, far],
+        out_specs=(vmem, far),
+        scratch_shapes=[pltpu.VMEM((8, 2, 128, 128), F32), pltpu.SemaphoreType.DMA((2,))],
+        compiler_params=pltpu.CompilerParams(vmem_limit_bytes=67043328),
+        name="finish",
+    )(packed, place, state)
 
 
 def local(
@@ -695,7 +744,7 @@
     widening_matrix,
     narrowing_matrix,
 ):
-    mixed, carried = layer(
+    packed, place, new_state = layer(
         residual_entries.T,
         fresh_extents.reshape(1, 128),
         initial_rescale_vector.reshape(1, 256),
@@ -713,6 +762,7 @@
         widening_matrix.T,
         narrowing_matrix,
     )
+    mixed, carried = finish(packed, place, new_state)
     return (mixed.T, carried)
 
 

time: 107 us -> 101 us (0.944)
  local copies, waits for them, and re-layouts: 3.77 us -> 0 us
    unnamed x2 -> x0, local copies, waits for them, and re-layouts: 3.77 us -> none
    pallas_call x1 -> x2, Pallas kernels: 102 us -> 101 us  [the longest x1 97 us: layer(): pl.pallas_call(layer_kernel, out_shape=(jax.ShapeDtypeStruct((8, 16, 128)...]
where the time goes in v5:
time: 101 us
  Pallas kernels  101 us (100%)
    pallas_call x1, Pallas kernels, layer(): pl.pallas_call(layer_kernel, out_shape=(jax.ShapeDtypeStruct((8, 16, 128)...  97 us
    pallas_call x1, Pallas kernels, finish(): pl.pallas_call(finish_kernel, out_shape=(jax.ShapeDtypeStruct((32, 1024),...  3.62 us

profile of v5, /device:TPU:1, one launch (start us, length us, event | category | flops | bytes accessed | tf_op | source)
XLA Modules:
  0.0 101.2 jit_solution(13572438132616078666)
XLA Ops:
  0.6 97.0 %layer.1 = (bf16[8,16,128]{2,1,0:T(8,128)(2,1)}, s32[8,1024]{1,0:T(8,128)}, f32[8,2,128,128]{3,2,1,0:T(8,128)}) custom-call(bf16[32,1024]{1,0:T(8,128)(2,1)} %bitcast.12, s32[1,128]{1,0:T(1,128)} %bitcast.16, f32[1,256]{1,0:T(1,128)} %bitcast.13, bf16[256,256]{1,0:T(8,128)(2,1)} %refs_3_.1, bf16[256,256]{1,0:T(8,128)(2,1)} %refs_4_.1, ...), custom_call_target="tpu_custom_call" | custom-call | tf_op jit(solution)/shard_map/layer/pallas_call | solution.py:672
  97.6 3.6 %finish.1 = (bf16[32,1024]{1,0:T(8,128)(2,1)}, f32[8,2,128,128]{3,2,1,0:T(8,128)}) custom-call(bf16[8,16,128]{2,1,0:T(8,128)(2,1)} %get-tuple-element.7.packed_ref, s32[8,1024]{1,0:T(8,128)} %get-tuple-element.8.place_ref, f32[8,2,128,128]{3,2,1,0:T(8,128)} %get-tuple-element.9.state_ref), custom_call_target="tpu_custom_call" | custom-call | tf_op jit(solution)/shard_map/finish/pallas_call | solution.py:715

commit v6 on v5

--- a/solution.py
+++ b/solution.py
@@ -17,7 +17,7 @@
 BF = jnp.bfloat16
 PARTS = ((0, 3), (3, 3), (6, 2))
 ORDERS = ("xyz", "yzx", "zxy")
-PLANE_ORDERS = ("zy", "yz")
+ROWS = (0, 1, 3, 2)
 
 
 def my_position():
@@ -50,10 +50,11 @@
     return device_at(at, x=(at["x"] + dx) % 4, c=(at["c"] + dc) % 2)
 
 
-def meet(peers):
+def meet(peers, meanwhile):
     barrier = pltpu.get_barrier_semaphore()
     for peer in peers:
         pl.semaphore_signal(barrier, inc=1, device_id=peer, device_id_type=MESH)
+    meanwhile()
     pl.semaphore_wait(barrier, len(peers))
 
 
@@ -108,42 +109,39 @@
 
 
 def gather_plane(at, bufs, orders, send):
-    copies = [[] for _ in orders]
-    for p, order in enumerate(orders):
-        a, b, c = order
-        own = bufs[p].at[at[c], at[b], at[a]]
-        for db, da in plane_offsets():
-            there = {a: (at[a] + da) % 4, b: (at[b] + db) % 4}
-            copies[p].append(send(own, own, device_at(at, **there)))
+    copies = [{} for _ in orders]
+    for db in ROWS:
+        for p, order in enumerate(orders):
+            a, b, c = order
+            own = bufs[p].at[at[c], at[b], at[a]]
+            for da in range(4):
+                if db or da:
+                    there = {a: (at[a] + da) % 4, b: (at[b] + db) % 4}
+                    copies[p][db, da] = send(own, own, device_at(at, **there))
     return copies
 
 
-def gather_line(at, bufs, orders, ready, send):
-    first = []
-    for p, order in enumerate(orders):
-        for copy in ready[p]:
-            copy.wait_recv()
-        axis = order[-1]
-        m = at[axis]
-        own = bufs[p].at[m]
-        first.append((
-            send(own, own, device_at(at, **{axis: (m + 1) % 4})),
-            send(own, own, device_at(at, **{axis: (m + 3) % 4})),
-        ))
+def gather_line(at, bufs, orders, plane, send):
+    first = {}
+    for db in ROWS:
+        for p, (a, b, c) in enumerate(orders):
+            for da in range(4):
+                if db or da:
+                    plane[p][db, da].wait_recv()
+            own = bufs[p].at[at[c], (at[b] + 4 - db) % 4]
+            first[p, db] = tuple(
+                send(own, own, device_at(at, **{c: (at[c] + turn) % 4})) for turn in (1, 3)
+            )
     yield
     second = []
-    for p, order in enumerate(orders):
-        axis = order[-1]
-        m = at[axis]
-        up, down = (m + 1) % 4, (m + 3) % 4
-        lo, hi = halves(bufs[p].shape[1])
-        first[p][0].wait_recv()
-        from_down = bufs[p].at[down, lo]
-        second.append(send(from_down, from_down, device_at(at, **{axis: up})))
-        first[p][1].wait_recv()
-        from_up = bufs[p].at[up, hi]
-        second.append(send(from_up, from_up, device_at(at, **{axis: down})))
-    for part in (*ready, *first):
+    for db in ROWS:
+        for p, (a, b, c) in enumerate(orders):
+            for copy in first[p, db]:
+                copy.wait_recv()
+            turn = 1 if db in (0, 2) else 3
+            came = bufs[p].at[(at[c] + 4 - turn) % 4, (at[b] + 4 - db) % 4]
+            second.append(send(came, came, device_at(at, **{c: (at[c] + turn) % 4})))
+    for part in (*[part.values() for part in plane], *first.values()):
         for copy in part:
             copy.wait_send()
     for copy in second:
@@ -206,27 +204,71 @@
 
 
 def reduce_torus(at, bufs, orders, line_received, plane_received, send):
-    copies = []
-
-    def to_plane(p):
+    early, late, plane = {}, {}, {}
+    lo, hi = pl.ds(0, 2), pl.ds(2, 2)
+
+    def row(p, db):
         a, b, c = orders[p]
-        copies.append([])
-        for n, (db, da) in enumerate(plane_offsets()):
-            there = {a: (at[a] + da) % 4, b: (at[b] + db) % 4}
-            block = bufs[p].at[at[c], there[b], there[a]]
-            copies[p].append(send(block, plane_received[p].at[n], device_at(at, **there)))
-
-    axes = [order[-1] for order in orders]
-    for _ in reduce_line(at, bufs, axes, ((),) * 3, line_received, send, True, to_plane):
-        pass
+        m = at[c]
+        return c, m, (m + 1) % 4, (m + 3) % 4, (at[b] + db) % 4
+
+    def begin(db):
+        for p in range(len(orders)):
+            c, m, up, down, r = row(p, db)
+            one_up, one_down, two_up, two_down = line_received[p]
+            to_up, to_down = device_at(at, **{c: up}), device_at(at, **{c: down})
+            away = (m + 2) % 4
+            early[p, db] = (
+                send(bufs[p].at[away, r, lo], one_up.at[db], to_up),
+                send(bufs[p].at[away, r, hi], one_down.at[db], to_down),
+                send(bufs[p].at[up, r, hi], two_up.at[db, hi], to_up),
+                send(bufs[p].at[down, r, lo], two_down.at[db, lo], to_down),
+            )
+
+    def go_on(db):
+        for p in range(len(orders)):
+            c, m, up, down, r = row(p, db)
+            one_up, one_down, two_up, two_down = line_received[p]
+            to_up, to_down = device_at(at, **{c: up}), device_at(at, **{c: down})
+            early[p, db][0].wait_recv()
+            add_into(bufs[p], (up, r, lo), one_up[db])
+            first = send(bufs[p].at[up, r, lo], two_up.at[db, lo], to_up)
+            early[p, db][1].wait_recv()
+            add_into(bufs[p], (down, r, hi), one_down[db])
+            late[p, db] = (first, send(bufs[p].at[down, r, hi], two_down.at[db, hi], to_down))
+
+    def end(db):
+        for p, (a, b, c) in enumerate(orders):
+            _, m, up, down, r = row(p, db)
+            two_up, two_down = line_received[p][2:]
+            for copy in (*early[p, db][2:], *late[p, db]):
+                copy.wait_recv()
+            total = bufs[p][m, r].astype(F32) + two_up[db].astype(F32) + two_down[db].astype(F32)
+            bufs[p][m, r] = total.astype(BF)
+            for da in range(4):
+                if db or da:
+                    n = 4 * db + da - 1
+                    there = {a: (at[a] + da) % 4, b: r}
+                    block = bufs[p].at[m, r, there[a]]
+                    plane[p, n] = send(block, plane_received[p].at[n], device_at(at, **there))
+
+    rows = ROWS[::-1]
+    for db in rows:
+        begin(db)
+    for db in rows:
+        go_on(db)
+    for db in rows:
+        end(db)
     sums = []
-    for p, order in enumerate(orders):
-        a, b, c = order
+    for p, (a, b, c) in enumerate(orders):
         total = bufs[p][at[c], at[b], at[a]].astype(F32)
-        for n, copy in enumerate(copies[p]):
-            copy.wait()
+        for n in range(14, -1, -1):
+            plane[p, n].wait_recv()
             total = total + plane_received[p][n].astype(F32)
         sums.append(total)
+    for copies in (*early.values(), *late.values(), plane.values()):
+        for copy in copies:
+            copy.wait_send()
     return sums
 
 
@@ -239,13 +281,19 @@
     "x", "lengths", "gain", "wq", "wf", "wi", "wo", "bound", "shrink", "lane_gain", "state",
     "result", "later_gain", "gate", "wide", "narrow",
 )
-IN_HBM = ("x", "wq", "wf", "wi", "wo", "state", "result", "gate", "wide", "narrow")
-
-
-def line_shapes(lead, tail, parts):
+SMALL = (
+    ("lengths", (1, 128), jnp.int32),
+    ("gain", (1, 256), F32),
+    ("bound", (1, 256), F32),
+    ("shrink", (2, 64), F32),
+    ("lane_gain", (1, 128), F32),
+    ("later_gain", (1, 32), F32),
+)
+
+
+def line_shapes(shape, count):
     shapes = []
-    for count in parts:
-        shape = (*lead, *((count,) if count else ()), *tail)
+    for _ in range(count):
         half = shape[0] // 2
         shapes += [(half, *shape[1:]), (shape[0] - half, *shape[1:]), shape, shape]
     return shapes
@@ -255,13 +303,14 @@
     counts = [count for _, count in PARTS]
     boxes = [(4, 4, 4, count, 16, 128) for count in counts]
     named = [
+        *[("small_" + name, shape, kind) for name, shape, kind in SMALL],
         ("cols", (8, 32, 1024), BF),
         ("scaled", (1024, 256), BF),
         ("squares", (8, 8, 128), F32),
         ("squares_in", (15, 8, 128), F32),
-        ("front_weights", (2, 256, 512), BF),
-        ("pa", (4, 4, 64, 512), BF),
-        ("pb", (4, 4, 64, 512), BF),
+        ("front_weights", (4, 256, 256), BF),
+        ("pa", (2, 4, 4, 64, 256), BF),
+        ("pb", (2, 4, 4, 64, 256), BF),
         ("z", (64, 1024), F32),
         ("query", (64, 256), F32),
         ("kept", (64, 256), F32),
@@ -291,9 +340,12 @@
     groups = [
         ("gathered", boxes),
         ("terms", boxes),
-        ("front_one", line_shapes((4, 64), (512,), (0, 0))),
-        ("front_two", line_shapes((64,), (512,), (0, 0))),
-        ("mixer_line", line_shapes((4, 4), (16, 128), counts)),
+        ("front_one", line_shapes((4, 64, 256), 4)),
+        ("front_two", [(3, 64, 256)] * 4),
+        (
+            "mixer_line",
+            [(4, n, count, 16, 128) for count in counts for n in (2, 2, 4, 4)],
+        ),
         ("mixer_plane", [(15, count, 16, 128) for count in counts]),
     ]
     flat = [pltpu.VMEM(shape, kind) for _, shape, kind in named]
@@ -326,9 +378,14 @@
         return copy
 
     cols = ref["_cols"]
+    small_copies = [
+        fetch(11 + n, ref[name], ref["_small_" + name]) for n, (name, _, _) in enumerate(SMALL)
+    ]
+    for name, _, _ in SMALL:
+        ref[name] = ref["_small_" + name]
     x_copy = fetch(0, ref["x"], cols.at[tp])
     front_copies = [
-        fetch(1 + n, ref[name], ref["_front_weights"].at[n // 2, :, 256 * (n % 2) : 256 * (n % 2) + 256])
+        fetch(1 + n, ref[name], ref["_front_weights"].at[n])
         for n, name in enumerate(("wq", "wf", "wi", "wo"))
     ]
     weight_copies = [
@@ -337,11 +394,23 @@
     ]
     state_copy = fetch(8, ref["state"], ref["_state_in"])
     result_copy = fetch(9, ref["result"], ref["_result_in"])
+    weights, narrows, staged = ref["_weights"], ref["_narrows"], ref["_staged"]
+
+    def pad_weights():
+        for n, first in ((0, 80), (1, 96)):
+            weights[n, :, first:128] = jnp.zeros((2, 128 - first, 4096), BF)
+            narrows[n, first:128] = jnp.zeros((128 - first, 4096), BF)
+        for copy in weight_copies:
+            copy.wait()
+        weights[0, :, 0:86] = staged[0:2]
+        narrows[0, 0:86] = staged[2]
+
     turns = (1, 2, 3)
     meet(
         [line_peer(at, *d) for d in lines]
         + [plane_peer(at, dz, 0) for dz in turns]
-        + [plane_peer(at, 0, dy) for dy in turns]
+        + [plane_peer(at, 0, dy) for dy in turns],
+        pad_weights,
     )
     for dy in turns:
         pl.semaphore_signal(ready, inc=1, device_id=plane_peer(at, 0, dy), device_id_type=MESH)
@@ -350,6 +419,8 @@
     partner = line_peer(at, 0, 1)
     far_copies = [send(cols.at[tp], cols.at[tp], line_peer(at, dx, 0)) for dx in turns]
     near_copies = [send(cols.at[tp], cols.at[tp], partner)]
+    for copy in small_copies:
+        copy.wait()
     own_gain, gains = ref["_own_gain"], ref["_gains"]
     own_gain[...] = jnp.broadcast_to(
         jnp.concatenate([ref["later_gain"][...], jnp.zeros((1, 96), F32)], axis=1), (8, 128)
@@ -371,54 +442,42 @@
     gain = jnp.concatenate(
         [column_of(ref["gain"][:, 0:128], 128), column_of(ref["gain"][:, 128:256], 128)], axis=0
     )
-    weights, narrows, staged = ref["_weights"], ref["_narrows"], ref["_staged"]
-    for n, first in ((0, 80), (1, 96)):
-        weights[n, :, first:128] = jnp.zeros((2, 128 - first, 4096), BF)
-        narrows[n, first:128] = jnp.zeros((128 - first, 4096), BF)
-    for copy in weight_copies:
-        copy.wait()
-    weights[0, :, 0:86] = staged[0:2]
-    narrows[0, 0:86] = staged[2]
-
     for dx, copy in zip(turns, far_copies):
         copy.wait()
         came = 2 * ((at["x"] + 4 - dx) % 4) + at["c"]
         near_copies.append(send(cols.at[came], cols.at[came], partner))
     for copy in near_copies:
         copy.wait()
-    weight_sends = [
-        send(weights.at[0, :, 0:96], weights.at[1, :, 0:96], partner),
-        send(narrows.at[0, 0:96], narrows.at[1, 0:96], partner),
-    ]
     scaled, squares = ref["_scaled"], ref["_squares"]
     for k in range(8):
         lanes = slice(128 * k, 128 * k + 128)
         v = cols[:, :, lanes].reshape(256, 128).astype(F32)
-        scaled[lanes, :] = (v * gain).T.astype(BF)
+        scaled[lanes, :] = (v * gain).astype(BF).T
         squares[k] = jnp.broadcast_to(jnp.sum(v * v, axis=0, keepdims=True), (8, 128))
     for copy in front_copies:
         copy.wait()
     pa, pb = ref["_pa"], ref["_pb"]
 
-    def project(n):
+    chunks = ((0, pa.at[0], "yz"), (1, pb.at[0], "zy"), (2, pa.at[1], "yz"), (3, pb.at[1], "zy"))
+    one, two = fours(group["front_one"]), group["front_two"]
+
+    def project(n, terms, order):
         def body(a, carry):
             lhs = scaled[pl.ds(pl.multiple_of(256 * a, 256), 256), :]
-            v = times(lhs, ref["_front_weights"][n], ((1,), (0,))).astype(BF).reshape(4, 64, 512)
-            if n == 0:
-                pa[:, a] = v
+            v = times(lhs, ref["_front_weights"][n], ((1,), (0,))).astype(BF).reshape(4, 64, 256)
+            if order == "yz":
+                terms[:, a] = v
             else:
-                pb[a] = v
+                terms[a] = v
             return carry
 
         lax.fori_loop(0, 4, body, 0)
 
-    one, two = fours(group["front_one"]), fours(group["front_two"])
-    project(0)
-    steps_a = reduce_line(at, (pa,), ("y",), ((),), one[0:1], send)
-    next(steps_a)
-    project(1)
-    steps_b = reduce_line(at, (pb,), ("z",), ((),), one[1:2], send)
-    next(steps_b)
+    lines_one = []
+    for n, terms, order in chunks:
+        project(n, terms, order)
+        lines_one.append(reduce_line(at, (terms,), order[0], ((),), one[n : n + 1], send))
+        next(lines_one[n])
     pl.semaphore_wait(ready, 3)
     square_copies = []
     for i, (dz, dy) in enumerate(planes):
@@ -426,14 +485,17 @@
         block = squares.at[(4 * peer[0] + peer[1]) // 2]
         square_copies.append(send(block, ref["_squares_in"].at[i], peer))
     ref["_own_rows"][...] = times(picks(place, 64 * tp, 64), cols[...].reshape(256, 1024))
-    next(steps_a)
-    next(steps_b)
-    next(steps_a)
-    steps_a = reduce_line(at, (pa,), ("z",), ((at["y"],),), two[0:1], send, False)
-    next(steps_a)
-    next(steps_b)
-    steps_b = reduce_line(at, (pb,), ("y",), ((at["z"],),), two[1:2], send, False)
-    next(steps_b)
+    for step in lines_one:
+        next(step)
+    second = []
+    for n, terms, order in chunks:
+        next(lines_one[n])
+        here, axis = at[order[0]], order[1]
+        second.append([])
+        for turn in turns:
+            there = (at[axis] + turn) % 4
+            peer = device_at(at, **{axis: there})
+            second[n].append(send(terms.at[here, there], two[n].at[turn - 1], peer))
     row = lax.broadcasted_iota(jnp.int32, (64, 128), 0)
     lane = lax.broadcasted_iota(jnp.int32, (64, 128), 1)
     length = jnp.sum(
@@ -449,11 +511,18 @@
         jnp.where(lane == 64 * (kv % 2) + row, total[0:1, :], 0.0), axis=1, keepdims=True
     )
     scale = lax.rsqrt(own / 4096 + EPS)
-    next(steps_a)
-    next(steps_b)
     z = ref["_z"]
-    z[:, 0:512] = next(steps_a)[0] * scale
-    z[:, 512:1024] = next(steps_b)[0] * scale
+    for n, terms, order in chunks:
+        total = terms[at[order[0]], at[order[1]]].astype(F32)
+        for i, copy in enumerate(second[n]):
+            copy.wait()
+            total = total + two[n][i].astype(F32)
+        z[:, 256 * n : 256 * n + 256] = total * scale
+
+    weight_sends = [
+        send(weights.at[0, :, 0:96], weights.at[1, :, 0:96], partner),
+        send(narrows.at[0, 0:96], narrows.at[1, 0:96], partner),
+    ]
 
     query, kept, keys, output = ref["_query"], ref["_kept"], ref["_key"], ref["_output"]
     slot = lax.broadcasted_iota(jnp.int32, (8, 8, 128), 1)
@@ -668,7 +737,7 @@
 def layer(*arguments):
     vmem = pl.BlockSpec(memory_space=pltpu.VMEM)
     far = pl.BlockSpec(memory_space=pltpu.HBM)
-    copies = 280
+    copies = 400
     return pl.pallas_call(
         layer_kernel,
         out_shape=(
@@ -676,13 +745,13 @@
             jax.ShapeDtypeStruct((8, 1024), jnp.int32),
             jax.ShapeDtypeStruct((8, 2, 128, 128), F32),
         ),
-        in_specs=[far if name in IN_HBM else vmem for name in INPUTS],
+        in_specs=[far] * len(INPUTS),
         out_specs=(vmem, vmem, far),
         scratch_shapes=[
             *scratch()[2],
             pltpu.SemaphoreType.DMA((copies,)),
             pltpu.SemaphoreType.DMA((copies,)),
-            pltpu.SemaphoreType.DMA((11,)),
+            pltpu.SemaphoreType.DMA((17,)),
             pltpu.SemaphoreType.REGULAR,
         ],
         compiler_params=pltpu.CompilerParams(
@@ -692,25 +761,38 @@
     )(*arguments)
 
 
-def finish_kernel(packed_ref, place_ref, state_ref, mixed_ref, new_ref, held, sems):
-    take = pltpu.make_async_copy(state_ref, held, sems.at[0])
-    take.start()
+def finish_kernel(packed_ref, place_ref, state_ref, mixed_ref, new_ref, held, packed, place, out, sems):
+    takes = []
+    for n, (src, dst) in enumerate(((packed_ref, packed), (place_ref, place))):
+        takes.append(pltpu.make_async_copy(src, dst, sems.at[n]))
+        takes[n].start()
+    for n in range(4):
+        half = pl.ds(2 * n, 2)
+        takes.append(pltpu.make_async_copy(state_ref.at[half], held.at[half], sems.at[2 + n]))
+        takes[2 + n].start()
+    takes[0].wait()
+    takes[1].wait()
     j = lax.broadcasted_iota(jnp.int32, (128, 1024), 0)
-    rows = 64 * (j // 16) + j % 16 - place_ref[0:1, :]
-    packed = packed_ref[...].reshape(128, 128)
+    rows = 64 * (j // 16) + j % 16 - place[0:1, :]
+    gives = []
     mixed = jnp.zeros((32, 1024), F32)
     for a in range(4):
+        takes[2 + a].wait()
+        half = pl.ds(2 * a, 2)
+        gives.append(pltpu.make_async_copy(held.at[half], new_ref.at[half], sems.at[6 + a]))
+        gives[a].start()
         chosen = jnp.where(rows == -16 * a, 1.0, 0.0).astype(BF)
-        mixed = mixed + times(packed[:, 32 * a : 32 * a + 32], chosen, ((0,), (0,)))
-    take.wait()
-    give = pltpu.make_async_copy(held, new_ref, sems.at[1])
+        piece = packed[...].reshape(128, 128)[:, 32 * a : 32 * a + 32]
+        mixed = mixed + times(piece, chosen, ((0,), (0,)))
+    out[...] = mixed.astype(BF)
+    give = pltpu.make_async_copy(out, mixed_ref, sems.at[10])
     give.start()
-    mixed_ref[...] = mixed.astype(BF)
+    for copy in gives:
+        copy.wait()
     give.wait()
 
 
 def finish(packed, place, state):
-    vmem = pl.BlockSpec(memory_space=pltpu.VMEM)
     far = pl.BlockSpec(memory_space=pltpu.HBM)
     return pl.pallas_call(
         finish_kernel,
@@ -718,9 +800,15 @@
             jax.ShapeDtypeStruct((32, 1024), BF),
             jax.ShapeDtypeStruct((8, 2, 128, 128), F32),
         ),
-        in_specs=[vmem, vmem, far],
-        out_specs=(vmem, far),
-        scratch_shapes=[pltpu.VMEM((8, 2, 128, 128), F32), pltpu.SemaphoreType.DMA((2,))],
+        in_specs=[far] * 3,
+        out_specs=(far, far),
+        scratch_shapes=[
+            pltpu.VMEM((8, 2, 128, 128), F32),
+            pltpu.VMEM((8, 16, 128), BF),
+            pltpu.VMEM((8, 1024), jnp.int32),
+            pltpu.VMEM((32, 1024), BF),
+            pltpu.SemaphoreType.DMA((11,)),
+        ],
         compiler_params=pltpu.CompilerParams(vmem_limit_bytes=67043328),
         name="finish",
     )(packed, place, state)

time: 101 us -> 96.2 us (0.952)
  Pallas kernels: 101 us -> 95.4 us
    pallas_call x1, Pallas kernels: 97 us -> 93 us  [layer(): pl.pallas_call(layer_kernel, out_shape=(jax.ShapeDtypeStruct((8, 16, 128)...]
    pallas_call x1, Pallas kernels: 3.62 us -> 2.42 us  [finish(): pl.pallas_call(finish_kernel, out_shape=(jax.ShapeDtypeStruct((32, 1024),...]
where the time goes in v6:
time: 96.2 us; the launch traced here: 96.1 us
  Pallas kernels  95.4 us (99%)
    pallas_call x1, Pallas kernels, layer(): pl.pallas_call(layer_kernel, out_shape=(jax.ShapeDtypeStruct((8, 16, 128)...  93 us
    pallas_call x1, Pallas kernels, finish(): pl.pallas_call(finish_kernel, out_shape=(jax.ShapeDtypeStruct((32, 1024),...  2.42 us

profile of v6, /device:TPU:1, one launch (start us, length us, event | category | flops | bytes accessed | tf_op | source)
XLA Modules:
  0.0 96.1 jit_solution(18434138284614790117)
XLA Ops:
  0.6 93.0 %layer.1 = (bf16[8,16,128]{2,1,0:T(8,128)(2,1)}, s32[8,1024]{1,0:T(8,128)}, f32[8,2,128,128]{3,2,1,0:T(8,128)}) custom-call(bf16[32,1024]{1,0:T(8,128)(2,1)} %bitcast.12, s32[1,128]{1,0:T(1,128)} %bitcast.16, f32[1,256]{1,0:T(1,128)} %bitcast.13, bf16[256,256]{1,0:T(8,128)(2,1)} %refs_3_.1, bf16[256,256]{1,0:T(8,128)(2,1)} %refs_4_.1, ...), custom_call_target="tpu_custom_call" | custom-call | tf_op jit(solution)/shard_map/layer/pallas_call | solution.py:741
  93.7 2.4 %finish.1 = (bf16[32,1024]{1,0:T(8,128)(2,1)}, f32[8,2,128,128]{3,2,1,0:T(8,128)}) custom-call(bf16[8,16,128]{2,1,0:T(8,128)(2,1)} %get-tuple-element.7.packed_ref, s32[8,1024]{1,0:T(8,128)} %get-tuple-element.8.place_ref, f32[8,2,128,128]{3,2,1,0:T(8,128)} %get-tuple-element.9.state_ref), custom_call_target="tpu_custom_call" | custom-call | tf_op jit(solution)/shard_map/finish/pallas_call | solution.py:797

commit v7 on v6

--- a/solution.py
+++ b/solution.py
@@ -130,17 +130,24 @@
                     plane[p][db, da].wait_recv()
             own = bufs[p].at[at[c], (at[b] + 4 - db) % 4]
             first[p, db] = tuple(
-                send(own, own, device_at(at, **{c: (at[c] + turn) % 4})) for turn in (1, 3)
+                send(own, own, device_at(at, **{c: (at[c] + turn) % 4}))
+                for turn in ((1, 3, 2) if db == 2 else (1, 3))
             )
     yield
     second = []
-    for db in ROWS:
+    for db, parts in ((0, ((1, 0, 4),)), (1, ((3, 0, 4),)), (3, ((1, 0, 2), (3, 2, 2)))):
         for p, (a, b, c) in enumerate(orders):
             for copy in first[p, db]:
                 copy.wait_recv()
-            turn = 1 if db in (0, 2) else 3
-            came = bufs[p].at[(at[c] + 4 - turn) % 4, (at[b] + 4 - db) % 4]
-            second.append(send(came, came, device_at(at, **{c: (at[c] + turn) % 4})))
+            for turn, start, size in parts:
+                came = bufs[p].at[
+                    (at[c] + 4 - turn) % 4, (at[b] + 4 - db) % 4, pl.ds(start, size)
+                ]
+                second.append(send(came, came, device_at(at, **{c: (at[c] + turn) % 4})))
+    yield
+    for p in range(len(orders)):
+        for copy in first[p, 2]:
+            copy.wait_recv()
     for part in (*[part.values() for part in plane], *first.values()):
         for copy in part:
             copy.wait_send()
@@ -410,7 +417,7 @@
         [line_peer(at, *d) for d in lines]
         + [plane_peer(at, dz, 0) for dz in turns]
         + [plane_peer(at, 0, dy) for dy in turns],
-        pad_weights,
+        lambda: None,
     )
     for dy in turns:
         pl.semaphore_signal(ready, inc=1, device_id=plane_peer(at, 0, dy), device_id_type=MESH)
@@ -442,6 +449,7 @@
     gain = jnp.concatenate(
         [column_of(ref["gain"][:, 0:128], 128), column_of(ref["gain"][:, 128:256], 128)], axis=0
     )
+    pad_weights()
     for dx, copy in zip(turns, far_copies):
         copy.wait()
         came = 2 * ((at["x"] + 4 - dx) % 4) + at["c"]
@@ -478,6 +486,8 @@
         project(n, terms, order)
         lines_one.append(reduce_line(at, (terms,), order[0], ((),), one[n : n + 1], send))
         next(lines_one[n])
+    for step in lines_one:
+        next(step)
     pl.semaphore_wait(ready, 3)
     square_copies = []
     for i, (dz, dy) in enumerate(planes):
@@ -485,8 +495,6 @@
         block = squares.at[(4 * peer[0] + peer[1]) // 2]
         square_copies.append(send(block, ref["_squares_in"].at[i], peer))
     ref["_own_rows"][...] = times(picks(place, 64 * tp, 64), cols[...].reshape(256, 1024))
-    for step in lines_one:
-        next(step)
     second = []
     for n, terms, order in chunks:
         next(lines_one[n])
@@ -622,6 +630,12 @@
         copy.wait()
         attended = attended + arrived[i].astype(F32)
     residual = (ref["_own_rows"][...] + attended).astype(BF).astype(F32)
+    later = ref["_later_squares"]
+    own_squares = jnp.sum(residual * residual, axis=1, keepdims=True)
+    later[0] = jnp.broadcast_to(row_of(own_squares, 64), (8, 128))
+    square_copies = [
+        send(later.at[0], later.at[1 + i], plane_peer(at, *d)) for i, d in enumerate(planes)
+    ]
     tile = (residual * gain).astype(BF)
     blocks = [
         tile[16 * i : 16 * i + 16, 128 * h : 128 * h + 128] for h in range(2) for i in range(4)
@@ -633,12 +647,6 @@
             gathered[p][(*idx, b)] = blocks[first + b]
     copies = gather_plane(at, gathered, ORDERS, send)
     ref["_residual"][...] = residual
-    later = ref["_later_squares"]
-    own_squares = jnp.sum(residual * residual, axis=1, keepdims=True)
-    later[0] = jnp.broadcast_to(row_of(own_squares, 64), (8, 128))
-    square_copies = [
-        send(later.at[0], later.at[1 + i], plane_peer(at, *d)) for i, d in enumerate(planes)
-    ]
     steps = gather_line(at, gathered, ORDERS, copies, send)
     next(steps)
     for copy in square_copies:
@@ -651,19 +659,24 @@
         send(squares_sum, squares_line.at[at["x"]], line_peer(at, dx, 0)) for dx in (1, 2, 3)
     ]
     next(steps)
+    total = ref["_total"]
+    total[...] = jnp.zeros_like(total)
     for copy in (*line_copies, *weight_sends):
         copy.wait()
+    scale = lax.rsqrt(
+        jnp.concatenate([column_of(squares_line[g, 0:1, :], 64) for g in range(4)], axis=0)
+        / 4096
+        + EPS
+    )
+    next(steps)
 
     ga, gb, gc = gathered
-    total = ref["_total"]
 
     def rows_at(zz, yy):
         v = jnp.concatenate([ga[zz, yy], gb[:, zz, yy], gc[yy, :, zz]], axis=1)
         return jnp.concatenate(
             [v[:, 0:4].reshape(256, 128), v[:, 4:8].reshape(256, 128)], axis=1
         )
-
-    total[...] = jnp.zeros_like(total)
 
     def widening(zz, carry):
         lhs = jnp.concatenate([rows_at(zz, yy) for yy in range(4)], axis=1)
@@ -673,11 +686,6 @@
         return carry
 
     lax.fori_loop(0, 4, widening, 0)
-    scale = lax.rsqrt(
-        jnp.concatenate([column_of(squares_line[g, 0:1, :], 64) for g in range(4)], axis=0)
-        / 4096
-        + EPS
-    )
     hidden = []
     for core in range(2):
         gated = total[core, :, 0:128] * scale

time: 96.2 us -> 95.1 us (0.989)
  Pallas kernels: 95.4 us -> 94.3 us
    pallas_call x1, Pallas kernels: 93 us -> 91.9 us  [layer(): pl.pallas_call(layer_kernel, out_shape=(jax.ShapeDtypeStruct((8, 16, 128)...]
where the time goes in v7:
time: 95.1 us; the launch traced here: 94.9 us
  Pallas kernels  94.3 us (99%)
    pallas_call x1, Pallas kernels, layer(): pl.pallas_call(layer_kernel, out_shape=(jax.ShapeDtypeStruct((8, 16, 128)...  91.9 us
    pallas_call x1, Pallas kernels, finish(): pl.pallas_call(finish_kernel, out_shape=(jax.ShapeDtypeStruct((32, 1024),...  2.42 us

profile of v7, /device:TPU:1, one launch (start us, length us, event | category | flops | bytes accessed | tf_op | source)
XLA Modules:
  0.0 94.9 jit_solution(3884669942421415378)
XLA Ops:
  0.6 91.9 %layer.1 = (bf16[8,16,128]{2,1,0:T(8,128)(2,1)}, s32[8,1024]{1,0:T(8,128)}, f32[8,2,128,128]{3,2,1,0:T(8,128)}) custom-call(bf16[32,1024]{1,0:T(8,128)(2,1)} %bitcast.12, s32[1,128]{1,0:T(1,128)} %bitcast.16, f32[1,256]{1,0:T(1,128)} %bitcast.13, bf16[256,256]{1,0:T(8,128)(2,1)} %refs_3_.1, bf16[256,256]{1,0:T(8,128)(2,1)} %refs_4_.1, ...), custom_call_target="tpu_custom_call" | custom-call | tf_op jit(solution)/shard_map/layer/pallas_call | solution.py:749
  92.5 2.4 %finish.1 = (bf16[32,1024]{1,0:T(8,128)(2,1)}, f32[8,2,128,128]{3,2,1,0:T(8,128)}) custom-call(bf16[8,16,128]{2,1,0:T(8,128)(2,1)} %get-tuple-element.7.packed_ref, s32[8,1024]{1,0:T(8,128)} %get-tuple-element.8.place_ref, f32[8,2,128,128]{3,2,1,0:T(8,128)} %get-tuple-element.9.state_ref), custom_call_target="tpu_custom_call" | custom-call | tf_op jit(solution)/shard_map/finish/pallas_call | solution.py:805

commit v8 on v7

--- a/solution.py
+++ b/solution.py
@@ -479,7 +479,7 @@
                 terms[a] = v
             return carry
 
-        lax.fori_loop(0, 4, body, 0)
+        lax.fori_loop(0, 4, body, 0, unroll=True)
 
     lines_one = []
     for n, terms, order in chunks:
@@ -583,7 +583,7 @@
         keys[:, lanes] = (key * after).reshape(64, 128)
         if h == 0:
             state_copy.wait()
-        lax.fori_loop(0, 8, functools.partial(read_state, h), 0, unroll=2)
+        lax.fori_loop(0, 8, functools.partial(read_state, h), 0, unroll=8)
         o = output[:, lanes]
         zo = z[:, 768 + 128 * h : 896 + 128 * h]
         o = o * lax.rsqrt(jnp.mean(o * o, axis=1, keepdims=True) + EPS) * ref["lane_gain"][...]
@@ -621,14 +621,22 @@
         partial[4 * part : 4 * part + 4] = (
             times(packed, result[...], ((1,), (0,))).astype(BF).reshape(4, 64, 256)
         )
+    other = 1 - at["c"]
+    near = [send(partial.at[2 * ((at["x"] + dx) % 4) + other], arrived.at[dx], partner) for dx in (2, 1, 3, 0)]
     copies = []
-    for i, (dx, dc) in enumerate(lines):
-        peer = line_peer(at, dx, dc)
-        copies.append(send(partial.at[2 * peer[2] + peer[3]], arrived.at[i], peer))
-    attended = partial[tp].astype(F32)
-    for i, copy in enumerate(copies):
-        copy.wait()
-        attended = attended + arrived[i].astype(F32)
+    for dx, copy in zip((2, 1, 3, 0), near):
+        copy.wait_recv()
+        own = 2 * ((at["x"] + dx) % 4) + at["c"]
+        both = partial[own].astype(F32) + arrived[dx].astype(F32)
+        if dx:
+            partial[own] = both.astype(BF)
+            copies.append(send(partial.at[own], arrived.at[3 + dx], line_peer(at, dx, 0)))
+    attended = both
+    for dx, copy in zip((2, 1, 3), copies):
+        copy.wait()
+        attended = attended + arrived[3 + dx].astype(F32)
+    for copy in near:
+        copy.wait_send()
     residual = (ref["_own_rows"][...] + attended).astype(BF).astype(F32)
     later = ref["_later_squares"]
     own_squares = jnp.sum(residual * residual, axis=1, keepdims=True)
@@ -685,7 +693,7 @@
             total[core] += times(lhs, weights[core, :, :, cols].reshape(256, 1024))
         return carry
 
-    lax.fori_loop(0, 4, widening, 0)
+    lax.fori_loop(0, 4, widening, 0, unroll=2)
     hidden = []
     for core in range(2):
         gated = total[core, :, 0:128] * scale
@@ -711,7 +719,7 @@
             tc[yy, :, zz] = v[:, 6:8]
         return carry
 
-    lax.fori_loop(0, 4, narrowing, 0)
+    lax.fori_loop(0, 4, narrowing, 0, unroll=2)
     sums = jnp.concatenate(
         reduce_torus(
             at, group["terms"], ORDERS, fours(group["mixer_line"]), group["mixer_plane"], send

time: 95.1 us -> 93.2 us (0.980)
  Pallas kernels: 94.3 us -> 92.4 us
    pallas_call x1, Pallas kernels: 91.9 us -> 90 us  [layer(): pl.pallas_call(layer_kernel, out_shape=(jax.ShapeDtypeStruct((8, 16, 128)...]
where the time goes in v8:
time: 93.2 us; the launch traced here: 93.1 us
  Pallas kernels  92.4 us (99%)
    pallas_call x1, Pallas kernels, layer(): pl.pallas_call(layer_kernel, out_shape=(jax.ShapeDtypeStruct((8, 16, 128)...  90 us
    pallas_call x1, Pallas kernels, finish(): pl.pallas_call(finish_kernel, out_shape=(jax.ShapeDtypeStruct((32, 1024),...  2.42 us

profile of v8, /device:TPU:1, one launch (start us, length us, event | category | flops | bytes accessed | tf_op | source)
XLA Modules:
  0.0 93.1 jit_solution(6257380790283194311)
XLA Ops:
  0.6 90.0 %layer.1 = (bf16[8,16,128]{2,1,0:T(8,128)(2,1)}, s32[8,1024]{1,0:T(8,128)}, f32[8,2,128,128]{3,2,1,0:T(8,128)}) custom-call(bf16[32,1024]{1,0:T(8,128)(2,1)} %bitcast.12, s32[1,128]{1,0:T(1,128)} %bitcast.16, f32[1,256]{1,0:T(1,128)} %bitcast.13, bf16[256,256]{1,0:T(8,128)(2,1)} %refs_3_.1, bf16[256,256]{1,0:T(8,128)(2,1)} %refs_4_.1, ...), custom_call_target="tpu_custom_call" | custom-call | tf_op jit(solution)/shard_map/layer/pallas_call | solution.py:757
  90.7 2.4 %finish.1 = (bf16[32,1024]{1,0:T(8,128)(2,1)}, f32[8,2,128,128]{3,2,1,0:T(8,128)}) custom-call(bf16[8,16,128]{2,1,0:T(8,128)(2,1)} %get-tuple-element.7.packed_ref, s32[8,1024]{1,0:T(8,128)} %get-tuple-element.8.place_ref, f32[8,2,128,128]{3,2,1,0:T(8,128)} %get-tuple-element.9.state_ref), custom_call_target="tpu_custom_call" | custom-call | tf_op jit(solution)/shard_map/finish/pallas_call | solution.py:813
